TPU v7x, 32 devices: a whole 2x2x4 slice. The times are simulated.
32 devices in a mesh: ep: 16 (over z, y, x), tp: 2 (over core).
Axes of the slice: x: 2, y: 2, z: 4, core: 2. Of those that a mesh axis runs over, the one named last changes fastest.
Arguments:
- tokens: bfloat16 [256, 2048], P(('ep', 'tp')), may hold values from -6 to 6
- mix_gain: float32 [2048], replicated, may hold values from 0.1 to 1.9
- w_query: bfloat16 [2048, 16, 128], P(None, 'tp', 'ep'), may hold values from -0.125 to 0.125
- w_key: bfloat16 [2048, 16, 128], P(None, 'tp', 'ep'), may hold values from -0.125 to 0.125
- w_value: bfloat16 [2048, 16, 128], P(None, 'tp', 'ep'), may hold values from -0.125 to 0.125
- w_zgate: bfloat16 [2048, 16, 128], P(None, 'tp', 'ep'), may hold values from -0.125 to 0.125
- w_beta: bfloat16 [2048, 16], P(None, 'tp'), may hold values from -0.125 to 0.125
- w_decay: bfloat16 [2048, 16], P(None, 'tp'), may hold values from -0.125 to 0.125
- decay_rate: float32 [16], P('tp'), may hold values from 0.5 to 8
- decay_bias: float32 [16], P('tp'), may hold values from -3 to 0
- head_gain: float32 [128], replicated, may hold values from 0.1 to 1.9
- state: float32 [256, 16, 128, 128], P('ep', 'tp'), may hold values from -1.5 to 1.5
- w_out: bfloat16 [2048, 2048], P('tp', 'ep'), may hold values from -0.125 to 0.125
- moe_gain: float32 [2048], replicated, may hold values from 0.1 to 1.9
- dense_mix: bfloat16 [2048], replicated, may hold values from -0.125 to 0.125
- dense_gate: bfloat16 [2048, 4096], P(None, ('ep', 'tp')), may hold values from -0.125 to 0.125
- dense_up: bfloat16 [2048, 4096], P(None, ('ep', 'tp')), may hold values from -0.125 to 0.125
- dense_down: bfloat16 [4096, 2048], P(('ep', 'tp')), may hold values from -0.09375 to 0.09375
- expert_gate: bfloat16 [16, 2048, 1024], P('ep', None, 'tp'), may hold values from -0.125 to 0.125
- expert_up: bfloat16 [16, 2048, 1024], P('ep', None, 'tp'), may hold values from -0.125 to 0.125
- expert_down: bfloat16 [16, 1024, 2048], P('ep', 'tp'), may hold values from -0.1875 to 0.1875
- expert_ids: int32 [256, 4], replicated, may hold values from 0 to 15, as said below
- route_weight: float32 [256, 4], replicated, may hold values from 0.1 to 1
Outputs:
- layer_out: bfloat16 [256, 2048], P(('ep', 'tp'))
- new_state: float32 [256, 16, 128, 128], P('ep', 'tp')
Inputs may be any that keep to these rules, and one draw needn't show every extreme that they name: `expert_ids`: the 4 experts of a row are distinct and lie in one group of 8 consecutive ids. In each aligned block of 16 rows (the rows of one index of ep) no expert is named by more than 8 rows, and at most 16 rows pick one group.
All inputs are finite; a program needn't handle non-finite values.
Results may differ from a plain program's by a relative error of at most 0.012.
Values may be sent and summed in bfloat16 or wider, within the bound.
No kernel may reach another device: no remote copies, remote signals or barrier semaphores. Data moves between devices by JAX's collectives and lax.ppermute only.
A program may use at most 128 MiB of HBM per device.

v0:
```python
import jax
import jax.numpy as jnp
from jax import lax
from jax.sharding import PartitionSpec as P

EPG = 8


EPS = 1e-06


def rms_scale(values, gain):
    return values * lax.rsqrt(jnp.mean(values * values, axis=-1, keepdims=True) + EPS) * gain


def unit_rows(values):
    return values * lax.rsqrt(jnp.sum(values * values, axis=-1, keepdims=True) + EPS)


def body(
    tokens,
    mix_gain,
    w_query,
    w_key,
    w_value,
    w_zgate,
    w_beta,
    w_decay,
    decay_rate,
    decay_bias,
    head_gain,
    state,
    w_out,
    moe_gain,
    dense_mix,
    dense_gate,
    dense_up,
    dense_down,
    expert_gate,
    expert_up,
    expert_down,
    expert_ids,
    route_weight,
):
    ep_count = lax.axis_size("ep")
    tp_count = lax.axis_size("tp")
    group_idx = lax.axis_index("ep")
    own_rows = tokens.shape[0]
    tok_float = tokens.astype(jnp.float32)
    normed = rms_scale(tok_float, mix_gain).astype(jnp.bfloat16)
    rows_all = lax.all_gather(normed, ("ep", "tp"), axis=0, tiled=True)
    total_rows = rows_all.shape[0]
    seq_group = total_rows // ep_count
    w_cat = jnp.stack([w_query, w_key, w_value, w_zgate], axis=1)
    model_width = w_cat.shape[0]
    local_heads = w_cat.shape[2]
    head_slice = w_cat.shape[3]
    projected = jnp.dot(
        rows_all, w_cat.reshape(model_width, -1), preferred_element_type=jnp.float32
    )
    projected = projected.astype(jnp.bfloat16).reshape(total_rows, 4, local_heads, head_slice)
    by_heads = lax.all_to_all(projected, "ep", split_axis=0, concat_axis=3, tiled=True).astype(
        jnp.float32
    )
    head_size = by_heads.shape[3]
    query = unit_rows(jax.nn.silu(by_heads[:, 0])) * head_size ** (-0.5)
    key_vec = unit_rows(jax.nn.silu(by_heads[:, 1]))
    value = jax.nn.silu(by_heads[:, 2])
    gate_in = by_heads[:, 3]
    seq_rows = lax.dynamic_slice_in_dim(rows_all, group_idx * seq_group, seq_group, 0)
    beta_rate = jax.nn.sigmoid(jnp.dot(seq_rows, w_beta, preferred_element_type=jnp.float32))
    decay_in = jnp.dot(seq_rows, w_decay, preferred_element_type=jnp.float32)
    retain = jnp.exp(-decay_rate * jax.nn.softplus(decay_in + decay_bias))
    recalled = jnp.einsum("shkv,shk->shv", state, key_vec, precision=lax.Precision.HIGHEST)
    correction = value - retain[..., None] * recalled
    new_state = (
        retain[..., None, None] * state
        + (beta_rate[..., None] * key_vec)[..., :, None] * correction[..., None, :]
    )
    readout = jnp.einsum("shkv,shk->shv", new_state, query, precision=lax.Precision.HIGHEST)
    gated = rms_scale(readout, head_gain) * jax.nn.silu(gate_in)
    gated = gated.astype(jnp.bfloat16).reshape(seq_group, local_heads * head_size)
    partial_value = jnp.dot(
        lax.all_gather(gated, "ep", axis=0, tiled=True), w_out, preferred_element_type=jnp.float32
    )
    partial_value = partial_value.reshape(ep_count, tp_count, own_rows, partial_value.shape[1])
    partial_value = lax.psum_scatter(
        partial_value.astype(jnp.bfloat16), "tp", scatter_dimension=1, tiled=True
    ).astype(jnp.float32)
    mixed = (
        lax.all_to_all(
            partial_value.astype(jnp.bfloat16), "ep", split_axis=0, concat_axis=3, tiled=True
        )
        .astype(partial_value.dtype)
        .reshape(own_rows, -1)
    )
    resid = tok_float + mixed
    moe_in = rms_scale(resid, moe_gain).astype(jnp.bfloat16)
    moe_all = lax.all_gather(moe_in, ("ep", "tp"), axis=0, tiled=True)
    dense_hidden = (
        jax.nn.silu(jnp.dot(moe_all, dense_gate, preferred_element_type=jnp.float32))
        * jnp.dot(moe_all, dense_up, preferred_element_type=jnp.float32)
    ).astype(jnp.bfloat16)
    mix_factor = jax.nn.sigmoid(jnp.dot(moe_all, dense_mix, preferred_element_type=jnp.float32))
    top_count = expert_ids.shape[1]
    group_count = ep_count // EPG
    group_cap = min(seq_group, 2 * seq_group // group_count)
    capacity = (group_cap * top_count + EPG - 1) // EPG
    slot_count = ep_count * capacity
    positions = jnp.arange(total_rows, dtype=jnp.int32)
    block_idx = positions // seq_group
    matched = expert_ids == group_idx
    routed = jnp.any(matched, axis=1).astype(jnp.int32)
    weight = jnp.sum(jnp.where(matched, route_weight, 0.0), axis=1)
    rank_in = jnp.cumsum(routed.reshape(-1, seq_group), axis=1).reshape(-1) - routed
    slot_idx = block_idx * capacity + rank_in
    slot_iota = jnp.arange(slot_count, dtype=jnp.int32)
    matches = (slot_idx[None, :] == slot_iota[:, None]) & (routed[None, :] > 0)
    source = jnp.sum(jnp.where(matches, positions[None, :], 0), axis=1)
    picked = jnp.take(moe_all, source, axis=0)
    expert_hidden = (
        jax.nn.silu(jnp.dot(picked, expert_gate[0], preferred_element_type=jnp.float32))
        * jnp.dot(picked, expert_up[0], preferred_element_type=jnp.float32)
    ).astype(jnp.bfloat16)
    expert_out = jnp.dot(expert_hidden, expert_down[0], preferred_element_type=jnp.float32)
    slot_clip = jnp.minimum(slot_idx, slot_count - 1)
    moe_total = lax.psum_scatter(
        jnp.dot(dense_hidden, dense_down, preferred_element_type=jnp.float32) * mix_factor[:, None]
        + weight[:, None] * jnp.take(expert_out, slot_clip, axis=0),
        ("ep", "tp"),
        scatter_dimension=0,
        tiled=True,
    )
    layer_out = (resid + moe_total).astype(jnp.bfloat16)
    return (layer_out, new_state)


def solution(mesh):
    placed = (
        P(("ep", "tp"), None),
        P(),
        P(None, "tp", "ep"),
        P(None, "tp", "ep"),
        P(None, "tp", "ep"),
        P(None, "tp", "ep"),
        P(None, "tp"),
        P(None, "tp"),
        P("tp"),
        P("tp"),
        P(),
        P("ep", "tp", None, None),
        P("tp", "ep"),
        P(),
        P(),
        P(None, ("ep", "tp")),
        P(None, ("ep", "tp")),
        P(("ep", "tp"), None),
        P("ep", None, "tp"),
        P("ep", None, "tp"),
        P("ep", "tp", None),
        P(),
        P(),
    )
    return jax.shard_map(
        body,
        mesh=mesh,
        in_specs=placed,
        out_specs=(P(("ep", "tp"), None), P("ep", "tp", None, None)),
        check_vma=False,
    )
```

profile of v0, /device:TPU:0, one launch (start us, length us, event | category | flops | bytes accessed | tf_op | source)
XLA Modules:
  0.0 411.6 jit_solution(2718276647418501136)
XLA Ops:
  7.2 0.0 all-gather.3.cloned.1.call-start
  7.2 1.0 fusion.31
  8.3 1.5 fusion.33
  9.7 0.0 all-gather.3.cloned.1.call-update
  9.8 0.7 neg.38
  10.4 1.3 pad_maximum_fusion
  11.7 56.1 %all-gather.3.cloned.1.call-done = bf16[256,2048]{1,0:T(8,128)(2,1)} async-done(((bf16[8,2048]{1,0:T(8,128)(2,1)}), bf16[256,2048]{1,0:T(8,128)(2,1)}) %all-gather.3.cloned.1.call-update) | async-done | bytes 1048592 | tf_op jit(solution)/shard_map/all_gather | solution.py:51
  67.8 1.7 convolution_convert_fusion
  69.5 3.7 copy.52
  73.2 4.0 reshape.258
  77.2 4.6 %all-to-all-start = ((bf16[16,2,2048]{2,1,0:T(2,128)(2,1)}), bf16[16,2,2048]{2,1,0:T(2,128)(2,1)S(1)}, u32[]{:S(2)}, u32[]{:S(2)}) async-start(bf16[16,2,2048]{2,1,0:T(2,128)(2,1)} %reshape.258), calls=%async_computation | async-start | bytes 262144 | tf_op jit(solution)/shard_map/all_to_all | solution.py:62
  81.8 0.0 all-reduce.3.cloned.1.call-start
  81.9 1.0 fusion.18
  82.9 0.1 copy.51
  83.0 1.0 fusion.53
  84.0 0.1 copy.50
  84.0 5.6 %all-to-all-done = bf16[16,2,2048]{2,1,0:T(2,128)(2,1)S(1)} async-done(((bf16[16,2,2048]{2,1,0:T(2,128)(2,1)}), bf16[16,2,2048]{2,1,0:T(2,128)(2,1)S(1)}, u32[]{:S(2)}, u32[]{:S(2)}) %all-to-all-start) | async-done | bytes 131104 | tf_op jit(solution)/shard_map/all_to_all | solution.py:62
  89.7 3.4 reshape.259
  93.1 2.7 copy.53
  95.8 1.9 reshape.231
  97.7 2.5 copy.73
  100.2 1.1 fusion.70
  101.3 1.2 copy.66
  102.5 0.1 multiply_reduce_fusion.3
  102.7 1.2 copy.67
  103.9 0.2 copy.68
  104.1 0.1 multiply_reduce_fusion.2
  104.2 0.1 multiply_multiply_fusion
  104.3 0.1 broadcast_multiply_fusion.1
  104.4 9.4 %fusion.71 = f32[16,8,1,128]{3,2,1,0:T(1,128)S(1)} fusion(f32[16,8,128,1]{2,3,1,0:T(1,128)S(1)} %bitcast.153, f32[16,8,128,128]{3,2,1,0:T(8,128)} %param.34), kind=kOutput, calls=%fused_computation.123 | convolution fusion | flops 25165824 | bytes 8519680 | tf_op jit(solution)/shard_map/shkv,shk->shv/dot_general | solution.py:74
  113.8 0.1 fusion.44
  113.9 5.7 %multiply_add_fusion = f32[16,8,128,128]{3,2,1,0:T(8,128)S(1)} fusion(f32[16,8,128,128]{3,2,1,0:T(8,128)} %param.34, f32[16,8,128]{2,1,0:T(8,128)S(1)} %fusion.44, f32[16,8,128]{2,1,0:T(8,128)S(1)} %get-tuple-element.6, f32[16,8]{1,0:T(8,128)S(1)} %copy.50), kind=kLoop, calls=%fused_computation.2 | loop fusion | flops 6291456 | bytes 16908800 | tf_op jit(solution)/shard_map/add | solution.py:77
  119.6 7.2 %fusion.72 = f32[16,8,1,128]{3,2,1,0:T(1,128)S(1)} fusion(f32[16,8,128,128]{3,2,1,0:T(8,128)S(1)} %multiply_add_fusion, f32[16,8,128,1]{2,3,1,0:T(1,128)S(1)} %bitcast.152), kind=kOutput, calls=%fused_computation.124 | convolution fusion | flops 25165824 | bytes 8519680 | tf_op jit(solution)/shard_map/shkv,shk->shv/dot_general | solution.py:80
  126.8 0.1 multiply_reduce_fusion.1
  126.9 0.2 copy.69
  127.1 0.1 fusion.49
  127.2 40.5 %all_gather.10 = bf16[256,1024]{1,0:T(8,128)(2,1)S(1)} all-gather(bf16[16,1024]{1,0:T(8,128)(2,1)S(1)} %bitcast.159), channel_id=1, replica_groups=mesh['ep'=16,'tp'=2] {'ep'}, dimensions={0}, use_global_device_ids=true | all-gather | bytes 557056 | tf_op jit(solution)/shard_map/all_gather | solution.py:84
  167.7 0.9 convolution_convert_fusion.1
  168.6 0.0 all-reduce.3.cloned.1.call-update
  168.6 0.0 all-gather.5.cloned.1.call-start
  168.7 0.6 dynamic-slice
  169.3 13.1 %all-reduce.3.cloned.1.call-done = bf16[16,2,8,128]{3,2,1,0:T(8,128)(2,1)} async-done(((bf16[16,2,8,128]{3,2,1,0:T(8,128)(2,1)}), bf16[16,2,8,128]{3,2,1,0:T(8,128)(2,1)}) %all-reduce.3.cloned.1.call-update) | async-done | bytes 65552
  182.4 1.4 constant_dynamic-slice_fusion
  183.8 14.0 %all_to_all.8 = bf16[16,1,8,128]{3,2,1,0:T(8,128)(2,1)S(1)} all-to-all(bf16[16,1,8,128]{3,2,1,0:T(8,128)(2,1)S(1)} %constant_dynamic-slice_fusion), channel_id=1, replica_groups=mesh['ep'=16,'tp'=2] {'ep'}, dimensions={0} | all-to-all | bytes 65536 | tf_op jit(solution)/shard_map/all_to_all | solution.py:91
  197.8 0.1 multiply_reduce_fusion
  198.0 0.7 multiply_convert_fusion
  198.6 0.0 all-gather.5.cloned.1.call-update
  198.7 0.3 reduce-scatter.3.cloned.1.call-start
  199.0 0.1 reshape.229
  199.1 0.2 reduce_window_sum.11
  199.3 0.1 reshape.225
  199.3 0.1 reshape.226
  199.5 0.1 select_reduce_fusion
  199.7 49.3 %all-gather.5.cloned.1.call-done = bf16[256,2048]{1,0:T(8,128)(2,1)} async-done(((bf16[8,2048]{1,0:T(8,128)(2,1)}), bf16[256,2048]{1,0:T(8,128)(2,1)}) %all-gather.5.cloned.1.call-update) | async-done | bytes 1048592 | tf_op jit(solution)/shard_map/all_gather | solution.py:99
  249.0 1.7 fusion.74
  250.7 1.7 gather_fusion
  252.4 2.2 fusion.5
  254.7 2.6 fusion.1
  257.3 2.7 gather_fusion.1
  260.0 1.9 fusion.73
  261.9 4.1 fusion
  266.0 0.0 reduce-scatter.3.cloned.1.call-update
  266.0 137.6 %reduce-scatter.3.cloned.1.call-done = f32[8,2048]{1,0:T(8,128)} async-done(((f32[256,2048]{1,0:T(8,128)}), f32[8,2048]{1,0:T(8,128)}) %reduce-scatter.3.cloned.1.call-update) | async-done | bytes 65552 | tf_op jit(solution)/shard_map/reduce_scatter | solution.py:127
  403.6 1.5 add_convert_fusion
  (47 shorter events, 0.3 us)
Async XLA Ops:
  7.2 247.5 %copy-start = (bf16[1,512,2048]{2,1,0:T(8,128)(2,1)S(1)}, bf16[1,512,2048]{2,1,0:T(8,128)(2,1)}, u32[]{:S(2)}) copy-start(bf16[1,512,2048]{2,1,0:T(8,128)(2,1)} %param.43) | copy-start | bytes 6291460
  7.2 60.6 %all-gather.3.cloned.1.call-start = ((), (), s32[]{:S(2)}) async-start(), calls=%async_computation.3 | async-start | bytes 1081344 | tf_op jit(solution)/shard_map/all_gather | solution.py:51
  69.5 12.4 %copy-start.6 = (bf16[2048,8]{0,1:T(8,128)(2,1)S(1)}, bf16[2048,8]{0,1:T(8,128)(2,1)}, u32[]{:S(2)}) copy-start(bf16[2048,8]{0,1:T(8,128)(2,1)} %param.29) | copy-start | bytes 98308
  69.5 13.4 %copy-start.12 = (bf16[2048,8]{0,1:T(8,128)(2,1)S(1)}, bf16[2048,8]{0,1:T(8,128)(2,1)}, u32[]{:S(2)}) copy-start(bf16[2048,8]{0,1:T(8,128)(2,1)} %param.30) | copy-start | bytes 98308
  69.5 13.4 %copy-start.13 = (f32[8]{0:T(128)S(1)}, f32[8]{0:T(128)}, u32[]{:S(2)}) copy-start(f32[8]{0:T(128)} %param.32) | copy-start | bytes 100
  77.2 12.4 %all-to-all-start = ((bf16[16,2,2048]{2,1,0:T(2,128)(2,1)}), bf16[16,2,2048]{2,1,0:T(2,128)(2,1)S(1)}, u32[]{:S(2)}, u32[]{:S(2)}) async-start(bf16[16,2,2048]{2,1,0:T(2,128)(2,1)} %reshape.258), calls=%async_computation | async-start | bytes 262144 | tf_op jit(solution)/shard_map/all_to_all | solution.py:62
  81.8 100.5 %all-reduce.3.cloned.1.call-start = ((), (), s32[]{:S(2)}) async-start(), calls=%async_computation.6 | async-start | bytes 131072
  119.5 7.2 %copy-start.3 = (f32[16,8,128,128]{3,2,1,0:T(8,128)}, f32[16,8,128,128]{3,2,1,0:T(8,128)S(1)}, u32[]{:S(2)}) copy-start(f32[16,8,128,128]{3,2,1,0:T(8,128)S(1)} %multiply_add_fusion) | copy-start | bytes 25165828
  119.6 7.6 %copy-start.11 = (f32[128]{0:T(128)S(1)}, f32[128]{0:T(128)}, u32[]{:S(2)}) copy-start(f32[128]{0:T(128)} %param.33) | copy-start | bytes 1540
  119.6 48.1 %copy-start.5 = (bf16[1024,128]{1,0:T(8,128)(2,1)S(1)}, bf16[1024,128]{1,0:T(8,128)(2,1)}, u32[]{:S(2)}) copy-start(bf16[1024,128]{1,0:T(8,128)(2,1)} %param.35) | copy-start | bytes 786436
  126.8 41.9 %copy-start.14 = (u32[32]{0:T(128)S(1)}, u32[32]{0:T(128)}, u32[]{:S(2)}) copy-start(u32[32]{0:T(128)} %constant.108) | copy-start | bytes 388
  126.8 71.0 %copy-start.4 = (bf16[8,2048]{1,0:T(8,128)(2,1)S(1)}, bf16[8,2048]{1,0:T(8,128)(2,1)}, u32[]{:S(2)}) copy-start(bf16[8,2048]{1,0:T(8,128)(2,1)} %param.23) | copy-start | bytes 98308
  126.8 71.2 %copy-start.7 = (f32[2048]{0:T(1024)S(1)}, f32[2048]{0:T(1024)}, u32[]{:S(2)}) copy-start(f32[2048]{0:T(1024)} %param.36) | copy-start | bytes 24580
  126.8 72.2 %copy-start.9 = (f32[256,4]{0,1:T(4,128)S(1)}, f32[256,4]{0,1:T(4,128)}, u32[]{:S(2)}) copy-start(f32[256,4]{0,1:T(4,128)} %param.45) | copy-start | bytes 12292
  126.8 72.2 %copy-start.10 = (s32[256,4]{0,1:T(4,128)S(1)}, s32[256,4]{0,1:T(4,128)}, u32[]{:S(2)}) copy-start(s32[256,4]{0,1:T(4,128)} %param.44) | copy-start | bytes 12292
  126.8 72.6 %copy-start.8 = (bf16[2048]{0:T(1024)(128)(2,1)S(1)}, bf16[2048]{0:T(1024)(128)(2,1)}, u32[]{:S(2)}) copy-start(bf16[2048]{0:T(1024)(128)(2,1)} %param.37) | copy-start | bytes 12292
  168.6 80.3 %all-gather.5.cloned.1.call-start = ((), (), s32[]{:S(2)}) async-start(), calls=%async_computation.4 | async-start | bytes 1081344 | tf_op jit(solution)/shard_map/all_gather | solution.py:99
  198.7 204.9 %reduce-scatter.3.cloned.1.call-start = ((), (), s32[]{:S(2)}) async-start(), calls=%async_computation.5 | async-start | bytes 2162688 | tf_op jit(solution)/shard_map/reduce_scatter | solution.py:127
  249.0 1.7 copy-start.1
  260.0 1.9 copy-start.2
Sparse Core Ops, SparseCore 0:
  11.4 56.3 all-gather.2
  168.8 13.5 all-reduce.2
  198.8 50.1 all-gather.4
  266.1 137.4 reduce-scatter.2
where the time goes:
time: 413 us; the launch traced here: 412 us
  waiting for transfers between devices  262 us (63%)
  blocking collectives  54.5 us (13%)
  matrix products  33.7 us (8%)
  local copies, waits for them, and re-layouts  29.1 us (7%)
  between operations  14.1 us (3%)
  other arithmetic  13.5 us (3%)
  starting transfers between devices  4.98 us (1%)
    reduce_scatter x1, waiting for transfers between devices, body(): lax.psum_scatter(jnp.dot(dense_hidden, dense_down, preferred_element_type...  138 us
    all_gather x1, waiting for transfers between devices, body(): rows_all = lax.all_gather(normed, ('ep', 'tp'), axis=0, tiled=True)  56.1 us
    all_gather x1, waiting for transfers between devices, body(): moe_all = lax.all_gather(moe_in, ('ep', 'tp'), axis=0, tiled=True)  49.3 us
    all_gather x1, blocking collectives, body(): lax.all_gather(gated, 'ep', axis=0, tiled=True)  40.5 us
    all_to_all x1, blocking collectives, body(): lax.all_to_all(partial_value.astype(jnp.bfloat16), 'ep', split_axis=0, co...  14 us
    unnamed x5, waiting for transfers between devices  13.2 us
    unnamed x40, local copies, waits for them, and re-layouts  12.4 us
    dot_general x1, matrix products, body(): jnp.einsum('shkv,shk->shv', state, key_vec, precision=lax.Precision.HIGHEST)  9.38 us
  transfers between devices with their start and end apart: 5, of which 5 were waited for; matrix products, arithmetic and copies ran while one was open for 1% of the time, Pallas kernels for 0%

commit v1 on v0

v1 whole, which is shorter than its diff:
```python
import functools

import jax
import jax.numpy as jnp
from jax import lax
from jax.experimental import pallas as pl
from jax.experimental.pallas import tpu as pltpu
from jax.sharding import PartitionSpec as P

EPS = 1e-06
AXES = ("ep", "tp")
F32 = jnp.float32
BF16 = jnp.bfloat16
VM = pltpu.VMEM
SM = pltpu.SMEM


def call(kernel, out_shape, operands, scratch=(), smem=(0,), limit=None, grid=None, in_specs=None, out_specs=None, name=None):
    if in_specs is None:
        in_specs = [pl.BlockSpec(memory_space=SM if i in smem else VM) for i in range(len(operands))]
    extra = {} if grid is None else {"grid": grid}
    if out_specs is None:
        out_specs = jax.tree.map(lambda _: pl.BlockSpec(memory_space=VM), out_shape)
    return pl.pallas_call(
        kernel,
        out_shape=out_shape,
        in_specs=in_specs,
        out_specs=out_specs,
        scratch_shapes=list(scratch),
        compiler_params=pltpu.CompilerParams(vmem_limit_bytes=limit),
        name=name,
        **extra,
    )(*operands)


def digits_of(count):
    bits = count.bit_length() - 1
    found = []
    while bits > 0:
        width = 2 if bits >= 2 else 1
        bits -= width
        found.append((bits, 1 << width))
    return found


def masks_of(digits):
    cur = [0]
    for shift, radix in digits[:-1]:
        cur = [(d << shift) | m for d in range(radix) for m in cur]
    shift, radix = digits[-1]
    return [[(d << shift) | m for m in cur] for d in range(radix)]


def exchange(value, mask, swap=0):
    ep_count, tp_count = lax.axis_size("ep"), lax.axis_size("tp")
    pairs = [
        (e * tp_count + t, (e ^ mask) * tp_count + (t ^ swap)) for e in range(ep_count) for t in range(tp_count)
    ]
    return lax.ppermute(value, AXES, pairs)


def gather_xor(piece, digits):
    cur = piece[None]
    for shift, radix in digits[:-1]:
        cur = jnp.concatenate([cur] + [exchange(cur, d << shift) for d in range(1, radix)], axis=0)
    shift, radix = digits[-1]
    return [cur] + [exchange(cur, d << shift) for d in range(1, radix)]


def scale_rows(values, gain):
    return values * lax.rsqrt(jnp.mean(values * values, axis=-1, keepdims=True) + EPS) * gain


def norm_kernel(masks, where, *refs):
    pieces, gain, out = refs[: len(masks)], refs[-2], refs[-1]
    me = where[0]
    for ref, row in zip(pieces, masks):
        for j, mask in enumerate(row):
            out[me ^ mask] = scale_rows(ref[j].astype(F32), gain[...]).astype(BF16)


def project_kernel(where, own, other, wq, wk, wv, wz, out, stacked):
    par = where[1]
    rows, each = wq.shape[0], own.shape[1]
    for p, ref in enumerate((wq, wk, wv, wz)):
        stacked[p * rows : (p + 1) * rows, :] = ref[...]
    for side, ref in ((par, own), (1 - par, other)):
        x = ref[...].reshape(-1, ref.shape[2])
        y = lax.dot_general(x, stacked[...], (((1,), (1,)), ((), ())), preferred_element_type=F32)
        out[:, side] = y.reshape(ref.shape[0], each, -1).astype(BF16)


def rates_kernel(where, own, other, wb, wd, rate, bias, beta, retain):
    me, par = where[0], where[1]
    each = own.shape[1]
    for side, ref in ((par, own), (1 - par, other)):
        x = ref[me]
        b = lax.dot_general(x, wb[...], (((1,), (1,)), ((), ())), preferred_element_type=F32)
        d = lax.dot_general(x, wd[...], (((1,), (1,)), ((), ())), preferred_element_type=F32)
        d = d + bias[...]
        soft = jnp.maximum(d, 0.0) + jnp.log1p(jnp.exp(-jnp.abs(d)))
        beta[side] = 1.0 / (1.0 + jnp.exp(-b))
        retain[side] = jnp.exp(-rate[...] * soft)


def silu(x):
    return x / (1.0 + jnp.exp(-x))


def state_kernel(heads, beta, retain, cols, gain, state, gated, new_state, rows, qt, kt, reads):
    step = pl.program_id(0)
    seqs = pl.num_programs(0)
    size = state.shape[3]

    @pl.when(step == 0)
    def _():
        table = cols[...]
        width = table.shape[1]
        count = table.shape[0] // gated.shape[0]
        piece = width // (4 * heads)
        lane = lax.broadcasted_iota(jnp.int32, (table.shape[0], size), 1)
        src = lax.broadcasted_iota(jnp.int32, (table.shape[0], size), 0)
        keep = (lane // piece) == (src // gated.shape[0])
        pick_lane = lax.broadcasted_iota(jnp.int32, (width, size), 1) % piece
        pick_row = lax.broadcasted_iota(jnp.int32, (width, size), 0)
        for p in range(4):
            for h in range(heads):
                pick = jnp.where(pick_row == pick_lane + (p * heads + h) * piece, 1.0, 0.0).astype(BF16)
                spread = jnp.dot(table, pick, preferred_element_type=F32)
                spread = jnp.where(keep, spread, 0.0).reshape(count, gated.shape[0], size)
                rows[p, pl.ds(h, gated.shape[0], stride=heads), :] = jnp.sum(spread, axis=0)
        q = silu(rows[0])
        q = q * lax.rsqrt(jnp.sum(q * q, axis=-1, keepdims=True) + EPS) * size ** (-0.5)
        qt[...] = q.T
        k = silu(rows[1])
        k = k * lax.rsqrt(jnp.sum(k * k, axis=-1, keepdims=True) + EPS)
        kt[...] = k.T
        rows[2] = silu(rows[2])
        rows[3] = silu(rows[3])

    lanes = qt.shape[1]
    back = lax.rem(lanes - step * heads, lanes)
    q_cols = pltpu.roll(qt[...], back, 1)
    k_cols = pltpu.roll(kt[...], back, 1)
    first = pl.multiple_of(step * heads, heads)
    values = rows[2, pl.ds(first, heads), :]
    gates = rows[3, pl.ds(first, heads), :]
    found = []
    for h in range(heads):
        keep_rate = retain[step, h]
        write_rate = beta[step, h]
        old = state[0, h]
        k_wide = jnp.broadcast_to(k_cols[:, h : h + 1], (size, size))
        q_wide = jnp.broadcast_to(q_cols[:, h : h + 1], (size, size))
        recalled = jnp.sum(old * k_wide, axis=0, keepdims=True)
        change = write_rate * (values[h : h + 1, :] - keep_rate * recalled)
        new = keep_rate * old + k_wide * change
        new_state[0, h] = new
        found.append(jnp.sum(new * q_wide, axis=0, keepdims=True))
    read = jnp.concatenate(found, axis=0)
    reads[pl.ds(first, heads), :] = scale_rows(read, gain[...]) * gates

    @pl.when(step == seqs - 1)
    def _():
        for h in range(heads):
            gated[:, h * size : (h + 1) * size] = reads[pl.ds(h, gated.shape[0], stride=heads), :].astype(BF16)


def mix_kernel(masks, where, *refs):
    pieces, weight, out = refs[: len(masks)], refs[-2], refs[-1]
    me, par = where[0], where[1]
    each = out.shape[2]
    for ref, row in zip(pieces, masks):
        x = ref[...].reshape(-1, ref.shape[2])
        y = jnp.dot(x, weight[...], preferred_element_type=F32)
        y = y.reshape(len(row), 2, each, -1).astype(BF16)
        for j, mask in enumerate(row):
            for side in range(2):
                out[side ^ par, me ^ mask] = y[j, side]


def resid_kernel(masks, where, *refs):
    count = len(masks)
    tokens, mixed, gain = refs[:count], refs[count:-4], refs[-4]
    moe, own, resid = refs[-3:]
    me = where[0]
    each = own.shape[0]
    for ref, row in zip(tokens, masks):
        for j, mask in enumerate(row):
            at = pl.multiple_of((me ^ mask) * each, each)
            resid[pl.ds(at, each), :] = ref[j].astype(F32)
    if len(mixed) == 1:
        resid[...] = resid[...] + mixed[0][...].astype(F32)
    for ref, row in zip(mixed, masks if len(mixed) > 1 else ()):
        for j, mask in enumerate(row):
            width = ref.shape[2]
            at = pl.ds(pl.multiple_of((me ^ mask) * width, width), width)
            resid[:, at] = resid[:, at] + ref[j].astype(F32)
    moe[...] = scale_rows(resid[...], gain[...]).astype(BF16)
    own[...] = resid[pl.ds(pl.multiple_of(me * each, each), each), :]


def expert_kernel(rows_in, route, mix, d_gate, d_up, d_down, e_gate, e_up, e_down, out):
    x = rows_in[...]
    dot = functools.partial(jnp.dot, preferred_element_type=F32)
    hidden = (silu(dot(x, e_gate[...])) * dot(x, e_up[...])).astype(BF16)
    dense = (silu(dot(x, d_gate[...])) * dot(x, d_up[...])).astype(BF16)
    factor = jnp.sum(x.astype(F32) * mix[...].astype(F32), axis=1, keepdims=True)
    factor = 1.0 / (1.0 + jnp.exp(-factor))
    out[...] = (route[...] * dot(hidden, e_down[...]) + factor * dot(dense, d_down[...])).astype(out.dtype)


def fold_kernel(masks, where, own, other, *outs):
    me = where[0]
    each = outs[0].shape[1]
    for out, row in zip(outs, masks):
        for j, mask in enumerate(row):
            at = pl.ds(pl.multiple_of((me ^ mask) * each, each), each)
            out[j] = (own[at, :].astype(F32) + other[at, :].astype(F32)).astype(BF16)


def sum_kernel(parts, *refs):
    outs = refs[parts:]
    for i, out in enumerate(outs):
        total = refs[0][i].astype(F32)
        for ref in refs[1:parts]:
            total = total + ref[i].astype(F32)
        out[...] = total.astype(out.dtype)


def last_kernel(resid, *refs):
    total = refs[0][...].astype(F32)
    for ref in refs[1:-1]:
        total = total + ref[...].astype(F32)
    refs[-1][...] = (resid[...] + total).astype(refs[-1].dtype)


def body(
    tokens,
    mix_gain,
    w_query,
    w_key,
    w_value,
    w_zgate,
    w_beta,
    w_decay,
    decay_rate,
    decay_bias,
    head_gain,
    state,
    w_out,
    moe_gain,
    dense_mix,
    dense_gate,
    dense_up,
    dense_down,
    expert_gate,
    expert_up,
    expert_down,
    expert_ids,
    route_weight,
):
    ep_count = lax.axis_size("ep")
    me, par = lax.axis_index("ep"), lax.axis_index("tp")
    where = jnp.stack([me, par]).astype(jnp.int32)
    digits = digits_of(ep_count)
    masks = masks_of(digits)
    each, width = tokens.shape
    seqs, heads, size = state.shape[:3]
    half = ep_count * each
    sds = jax.ShapeDtypeStruct

    tok_pieces = gather_xor(tokens, digits)
    normed = call(
        functools.partial(norm_kernel, masks),
        sds((ep_count, each, width), BF16),
        [where, *tok_pieces, mix_gain[None]],
        name="norm",
    )
    normed_other = exchange(normed, 0, 1)

    flat = [w.transpose(1, 2, 0).reshape(-1, width) for w in (w_query, w_key, w_value, w_zgate)]
    columns = 4 * flat[0].shape[0]
    projected = call(
        project_kernel,
        sds((ep_count, 2, each, columns), BF16),
        [where, normed, normed_other, *flat],
        scratch=[VM((columns, width), BF16)],
        name="project",
    )
    by_seq = lax.all_to_all(projected, "ep", split_axis=0, concat_axis=0, tiled=True)
    beta, retain = call(
        rates_kernel,
        (sds((2, each, heads), F32), sds((2, each, heads), F32)),
        [where, normed, normed_other, w_beta.T, w_decay.T, decay_rate[None], decay_bias[None]],
        name="rates",
    )

    whole = lambda shape: pl.BlockSpec(shape, lambda i: (0,) * len(shape))
    blocked = pl.BlockSpec((1, heads, size, size), lambda i: (i, 0, 0, 0))
    gated, new_state = call(
        functools.partial(state_kernel, heads),
        (sds((seqs, heads * size), BF16), sds(state.shape, F32)),
        [
            beta.reshape(seqs, heads),
            retain.reshape(seqs, heads),
            by_seq.reshape(ep_count * seqs, columns),
            head_gain[None],
            state,
        ],
        scratch=[
            VM((4, seqs * heads, size), F32),
            VM((size, seqs * heads), F32),
            VM((size, seqs * heads), F32),
            VM((seqs * heads, size), F32),
        ],
        grid=(seqs,),
        in_specs=[
            pl.BlockSpec(memory_space=SM),
            pl.BlockSpec(memory_space=SM),
            whole((ep_count * seqs, columns)),
            whole((1, size)),
            blocked,
        ],
        out_specs=(whole((seqs, heads * size)), blocked),
        name="state",
    )

    gated_pieces = gather_xor(gated, digits)
    out_cols = w_out.shape[1]
    mixed = call(
        functools.partial(mix_kernel, masks),
        sds((2, ep_count, each, out_cols), BF16),
        [where, *gated_pieces, w_out],
        name="mix",
    )
    mixed = (mixed[0].astype(F32) + exchange(mixed[1], 0, 1).astype(F32)).astype(BF16).reshape(half, out_cols)
    mixed_pieces = gather_xor(mixed, digits)
    if out_cols % 128:
        order = jnp.argsort(me ^ jnp.array([m for row in masks for m in row], jnp.int32))
        blocks = jnp.take(jnp.concatenate(mixed_pieces, axis=0), order, axis=0)
        mixed_pieces = [blocks.transpose(1, 0, 2).reshape(half, width)]
    moe_in, resid = call(
        functools.partial(resid_kernel, masks),
        (sds((half, width), BF16), sds((each, width), F32)),
        [where, *tok_pieces, *mixed_pieces, moe_gain[None]],
        scratch=[VM((half, width), F32)],
        name="resid",
    )
    moe_other = exchange(moe_in, 0, 1)

    chosen = jnp.sum(jnp.where(expert_ids == me, route_weight, 0.0), axis=1).reshape(ep_count, 2, each)
    route = lax.dynamic_index_in_dim(chosen, par, 1, False).reshape(half, 1)
    route_other = lax.dynamic_index_in_dim(chosen, 1 - par, 1, False).reshape(half, 1)
    weights = [dense_mix[None], dense_gate, dense_up, dense_down, expert_gate[0], expert_up[0], expert_down[0]]
    run = lambda x, r, dt, name: call(expert_kernel, sds((half, width), dt), [x, r, *weights], smem=(), name=name)
    part_own = run(moe_in, route, F32, "experts_own")
    part_other = run(moe_other, route_other, BF16, "experts_other")

    prev = len(masks[0])
    parts = call(
        functools.partial(fold_kernel, masks),
        tuple(sds((prev, each, width), BF16) for _ in masks),
        [where, part_own, exchange(part_other, 0, 1)],
        name="fold",
    )
    for level in range(len(digits) - 1, 0, -1):
        shift, radix = digits[level]
        got = [parts[0]] + [exchange(parts[d], d << shift) for d in range(1, radix)]
        nxt = digits[level - 1][1]
        got = [g.reshape(nxt, -1, width) for g in got]
        parts = call(
            functools.partial(sum_kernel, len(got)),
            tuple(sds(got[0].shape[1:], BF16) for _ in range(nxt)),
            got,
            smem=(),
            name=f"sum{level}",
        )
    shift, radix = digits[0]
    got = [parts[0]] + [exchange(parts[d], d << shift) for d in range(1, radix)]
    layer_out = call(last_kernel, sds((each, width), BF16), [resid, *got], smem=(), name="last")
    return (layer_out, new_state)


def solution(mesh):
    placed = (
        P(("ep", "tp"), None),
        P(),
        P(None, "tp", "ep"),
        P(None, "tp", "ep"),
        P(None, "tp", "ep"),
        P(None, "tp", "ep"),
        P(None, "tp"),
        P(None, "tp"),
        P("tp"),
        P("tp"),
        P(),
        P("ep", "tp", None, None),
        P("tp", "ep"),
        P(),
        P(),
        P(None, ("ep", "tp")),
        P(None, ("ep", "tp")),
        P(("ep", "tp"), None),
        P("ep", None, "tp"),
        P("ep", None, "tp"),
        P("ep", "tp", None),
        P(),
        P(),
    )
    return jax.shard_map(
        body,
        mesh=mesh,
        in_specs=placed,
        out_specs=(P(("ep", "tp"), None), P("ep", "tp", None, None)),
        check_vma=False,
    )
```

time: 413 us -> 141 us (0.34)
  waiting for transfers between devices: 262 us -> 42.1 us
  blocking collectives: 54.5 us -> 0 us
  Pallas kernels: 0 us -> 46.7 us
  matrix products: 33.7 us -> 0 us
  starting transfers between devices: 4.98 us -> 37.5 us
  local copies, waits for them, and re-layouts: 29.1 us -> 9.71 us
  between operations: 14.1 us -> 0.79 us
  other arithmetic: 13.5 us -> 3.02 us
    reduce_scatter x1 -> x0, waiting for transfers between devices: 138 us -> none  [body(): lax.psum_scatter(jnp.dot(dense_hidden, dense_down, preferred_element_type...]
    all_gather x2 -> x0, waiting for transfers between devices: 105 us -> none  [the longest x1 56.1 us: body(): rows_all = lax.all_gather(normed, ('ep', 'tp'), axis=0, tiled=True)]
    pallas_call x0 -> x11, Pallas kernels: none -> 46.7 us  [call(): pl.pallas_call(kernel, out_shape=out_shape, in_specs=in_specs, out_specs=...]
    all_gather x1 -> x0, blocking collectives: 40.5 us -> none  [body(): lax.all_gather(gated, 'ep', axis=0, tiled=True)]
    ppermute x0 -> x28, waiting for transfers between devices: none -> 36.4 us  [exchange(): return lax.ppermute(value, AXES, pairs)]
    dot_general x11 -> x0, matrix products: 33.7 us -> none  [the longest x1 9.38 us: body(): jnp.einsum('shkv,shk->shv', state, key_vec, precision=lax.Precision.HIGHEST)]
    ppermute x0 -> x28, starting transfers between devices: none -> 33.4 us  [exchange(): return lax.ppermute(value, AXES, pairs)]
    all_to_all x1 -> x0, blocking collectives: 14 us -> none  [body(): lax.all_to_all(partial_value.astype(jnp.bfloat16), 'ep', split_axis=0, co...]
  transfers between devices with their start and end apart: 5 -> 29, of which waited for: 5 -> 22; matrix products, arithmetic and copies ran while one was open for 1% -> 2% of each run, Pallas kernels for 0% -> 6%
where the time goes in v1:
time: 141 us; the launch traced here: 140 us
  Pallas kernels  46.7 us (33%)
  waiting for transfers between devices  42.1 us (30%)
  starting transfers between devices  37.5 us (27%)
  local copies, waits for them, and re-layouts  9.71 us (7%)
  other arithmetic  3.02 us (2%)
    pallas_call x11, Pallas kernels, call(): pl.pallas_call(kernel, out_shape=out_shape, in_specs=in_specs, out_specs=...  46.7 us
    ppermute x28, waiting for transfers between devices, exchange(): return lax.ppermute(value, AXES, pairs)  36.4 us
    ppermute x28, starting transfers between devices, exchange(): return lax.ppermute(value, AXES, pairs)  33.4 us
    unnamed x50, local copies, waits for them, and re-layouts  6.77 us
    all_to_all x1, waiting for transfers between devices, body(): lax.all_to_all(projected, 'ep', split_axis=0, concat_axis=0, tiled=True)  5.72 us
    all_to_all x1, starting transfers between devices, body(): lax.all_to_all(projected, 'ep', split_axis=0, concat_axis=0, tiled=True)  4.17 us
  transfers between devices with their start and end apart: 29, of which 22 were waited for; matrix products, arithmetic and copies ran while one was open for 2% of the time, Pallas kernels for 6%

profile of v1, /device:TPU:0, one launch (start us, length us, event | category | flops | bytes accessed | tf_op | source)
XLA Modules:
  0.0 139.9 jit_solution(15980793239015700736)
XLA Ops:
  0.6 5.1 %collective-permute-start.2 = (bf16[1,8,2048]{2,1,0:T(8,128)(2,1)}, bf16[1,8,2048]{2,1,0:T(8,128)(2,1)S(1)}, u32[]{:S(2)}, u32[]{:S(2)}) collective-permute-start(bf16[1,8,2048]{2,1,0:T(8,128)(2,1)} %bitcast.51), channel_id=1, source_target_pairs={{0,24},{1,25},{2,26},{3,27},{4,28},{5,29},{6,30},{7,31},{8,16},{9,... | collective-permute-start | bytes 98312 | tf_op jit(solution)/shard_map/ppermute | solution.py:59
  5.8 0.6 collective-permute-start
  6.4 1.5 %collective-permute-done.2 = bf16[1,8,2048]{2,1,0:T(8,128)(2,1)S(1)} collective-permute-done((bf16[1,8,2048]{2,1,0:T(8,128)(2,1)}, bf16[1,8,2048]{2,1,0:T(8,128)(2,1)S(1)}, u32[]{:S(2)}, u32[]{:S(2)}) %collective-permute-start.2) | collective-permute-done | bytes 32800 | tf_op jit(solution)/shard_map/ppermute | solution.py:59
  7.9 2.9 %collective-permute-done.1 = bf16[1,8,2048]{2,1,0:T(8,128)(2,1)S(1)} collective-permute-done((bf16[1,8,2048]{2,1,0:T(8,128)(2,1)}, bf16[1,8,2048]{2,1,0:T(8,128)(2,1)S(1)}, u32[]{:S(2)}, u32[]{:S(2)}) %collective-permute-start.1) | collective-permute-done | bytes 32800 | tf_op jit(solution)/shard_map/ppermute | solution.py:59
  10.8 0.8 pad_maximum_fusion.refs_0_
  11.6 2.5 %collective-permute-start.5 = (bf16[4,8,2048]{2,1,0:T(8,128)(2,1)S(1)}, bf16[4,8,2048]{2,1,0:T(8,128)(2,1)S(1)}, u32[]{:S(2)}, u32[]{:S(2)}) collective-permute-start(bf16[4,8,2048]{2,1,0:T(8,128)(2,1)S(1)} %pad_maximum_fusion.refs_0_), channel_id=1, source_target_pairs={{0,6},{1,7},{2,4},{3,5},{4,2},{5,3},{6,0},{7,1},{8,14},{9,15},{10,... | collective-permute-start | bytes 393224 | tf_op jit(solution)/shard_map/ppermute | solution.py:59
  15.1 0.7 pad_add_fusion.where
  15.8 3.1 %collective-permute-done.5.refs_3_ = bf16[4,8,2048]{2,1,0:T(8,128)(2,1)S(1)} collective-permute-done((bf16[4,8,2048]{2,1,0:T(8,128)(2,1)S(1)}, bf16[4,8,2048]{2,1,0:T(8,128)(2,1)S(1)}, u32[]{:S(2)}, u32[]{:S(2)}) %collective-permute-start.5) | collective-permute-done | bytes 131104 | tf_op jit(solution)/shard_map/ppermute | solution.py:59
  18.9 0.8 collective-permute-done.4.refs_2_
  20.4 2.1 %norm.1.own = bf16[16,8,2048]{2,1,0:T(8,128)(2,1)} custom-call(s32[2]{0:T(128)} %pad_add_fusion.where, bf16[4,8,2048]{2,1,0:T(8,128)(2,1)} %copy-done.1, bf16[4,8,2048]{2,1,0:T(8,128)(2,1)} %copy-done.9, bf16[4,8,2048]{2,1,0:T(8,128)(2,1)} %copy-done.8, bf16[4,8,2048]{2,1,0:T(8,128)(2,1)} %copy-done.7, f32[1,2048]{1,0:T(1,128)} %bitcast.59), custom_call_target="tpu_custom_call" | custom-call | tf_op jit(solution)/shard_map/norm/pallas_call | solution.py:24
  22.5 2.1 %collective-permute-done.6.other = bf16[16,8,2048]{2,1,0:T(8,128)(2,1)S(1)} collective-permute-done((bf16[16,8,2048]{2,1,0:T(8,128)(2,1)}, bf16[16,8,2048]{2,1,0:T(8,128)(2,1)S(1)}, u32[]{:S(2)}, u32[]{:S(2)}) %collective-permute-start.6) | collective-permute-done | bytes 524320 | tf_op jit(solution)/shard_map/ppermute | solution.py:59
  24.7 0.8 copy-done
  25.4 3.0 %project.1 = bf16[16,2,8,256]{3,2,1,0:T(8,128)(2,1)} custom-call(s32[2]{0:T(128)} %pad_add_fusion.where, bf16[16,8,2048]{2,1,0:T(8,128)(2,1)} %norm.1.own, bf16[16,8,2048]{2,1,0:T(8,128)(2,1)} %copy-done, bf16[64,2048]{1,0:T(8,128)(2,1)} %bitcast.45, bf16[64,2048]{1,0:T(8,128)(2,1)} %bitcast.46, bf16[64,2048]{1,0:T(8,128)(2,1)} %bitcast.47, ...), custom_call_target="tpu_custom_call" | custom-call | tf_op jit(solution)/shard_map/project/pallas_call | solution.py:24
  28.4 4.2 %all-to-all-start = ((bf16[16,2,8,256]{3,2,1,0:T(8,128)(2,1)}), bf16[16,2,8,256]{3,2,1,0:T(8,128)(2,1)S(1)}, u32[]{:S(2)}, u32[]{:S(2)}) async-start(bf16[16,2,8,256]{3,2,1,0:T(8,128)(2,1)} %project.1), calls=%async_computation | async-start | bytes 262144 | tf_op jit(solution)/shard_map/all_to_all | solution.py:291
  32.6 2.1 %rates.1 = (f32[2,8,8]{2,1,0:T(8,128)}, f32[2,8,8]{2,1,0:T(8,128)}) custom-call(s32[2]{0:T(128)} %pad_add_fusion.where, bf16[16,8,2048]{2,1,0:T(8,128)(2,1)} %norm.1.own, bf16[16,8,2048]{2,1,0:T(8,128)(2,1)} %copy-done, bf16[8,2048]{1,0:T(8,128)(2,1)} %bitcast.49, bf16[8,2048]{1,0:T(8,128)(2,1)} %bitcast.50, f32[1,8]{1,0:T(1,128)} %bitcast.63, f32[1,8]{1,0:T(1,128)} %bitcast.64), custom_call_target="tpu_custom_call" | custom-call | tf_op jit(solution)/shard_map/rates/pallas_call | solution.py:24
  34.7 5.7 %all-to-all-done = bf16[16,2,8,256]{3,2,1,0:T(8,128)(2,1)S(1)} async-done(((bf16[16,2,8,256]{3,2,1,0:T(8,128)(2,1)}), bf16[16,2,8,256]{3,2,1,0:T(8,128)(2,1)S(1)}, u32[]{:S(2)}, u32[]{:S(2)}) %all-to-all-start) | async-done | bytes 131104 | tf_op jit(solution)/shard_map/all_to_all | solution.py:291
  40.4 0.6 copy-done.2
  41.1 17.3 %state.2 = (bf16[16,1024]{1,0:T(8,128)(2,1)}, f32[16,8,128,128]{3,2,1,0:T(8,128)}) custom-call(f32[16,8]{1,0:T(8,128)} %bitcast.61, f32[16,8]{1,0:T(8,128)} %bitcast.62, bf16[256,256]{1,0:T(8,128)(2,1)} %bitcast.44, f32[1,128]{1,0:T(1,128)} %bitcast.65, f32[16,8,128,128]{3,2,1,0:T(8,128)} %state.3), custom_call_target="tpu_custom_call" | custom-call | tf_op jit(solution)/shard_map/state/pallas_call | solution.py:24
  58.4 1.6 %collective-permute-start.9 = (bf16[1,16,1024]{2,1,0:T(8,128)(2,1)}, bf16[1,16,1024]{2,1,0:T(8,128)(2,1)S(1)}, u32[]{:S(2)}, u32[]{:S(2)}) collective-permute-start(bf16[1,16,1024]{2,1,0:T(8,128)(2,1)} %bitcast.55), channel_id=1, source_target_pairs={{0,24},{1,25},{2,26},{3,27},{4,28},{5,29},{6,30},{7,31},{8,16},{9,... | collective-permute-start | bytes 98312 | tf_op jit(solution)/shard_map/ppermute | solution.py:59
  60.0 0.8 collective-permute-start.8
  60.8 2.1 %collective-permute-start.7 = (bf16[1,16,1024]{2,1,0:T(8,128)(2,1)}, bf16[1,16,1024]{2,1,0:T(8,128)(2,1)S(1)}, u32[]{:S(2)}, u32[]{:S(2)}) collective-permute-start(bf16[1,16,1024]{2,1,0:T(8,128)(2,1)} %bitcast.57), channel_id=1, source_target_pairs={{0,8},{1,9},{2,10},{3,11},{4,12},{5,13},{6,14},{7,15},{8,0},{9,1},... | collective-permute-start | bytes 98312 | tf_op jit(solution)/shard_map/ppermute | solution.py:59
  62.9 1.6 %collective-permute-done.9 = bf16[1,16,1024]{2,1,0:T(8,128)(2,1)S(1)} collective-permute-done((bf16[1,16,1024]{2,1,0:T(8,128)(2,1)}, bf16[1,16,1024]{2,1,0:T(8,128)(2,1)S(1)}, u32[]{:S(2)}, u32[]{:S(2)}) %collective-permute-start.9) | collective-permute-done | bytes 32800 | tf_op jit(solution)/shard_map/ppermute | solution.py:59
  64.5 0.8 collective-permute-done.8
  65.3 0.8 pad_maximum_fusion.1.refs_0_
  66.1 0.8 collective-permute-start.12
  67.0 1.7 %collective-permute-start.11 = (bf16[4,16,1024]{2,1,0:T(8,128)(2,1)S(1)}, bf16[4,16,1024]{2,1,0:T(8,128)(2,1)S(1)}, u32[]{:S(2)}, u32[]{:S(2)}) collective-permute-start(bf16[4,16,1024]{2,1,0:T(8,128)(2,1)S(1)} %pad_maximum_fusion.1.refs_0_), channel_id=1, source_target_pairs={{0,4},{1,5},{2,6},{3,7},{4,0},{5,1},{6,2},{7,3},{8,12},{9,13},{10,... | collective-permute-start | bytes 393224 | tf_op jit(solution)/shard_map/ppermute | solution.py:59
  68.7 1.0 collective-permute-start.10
  69.7 2.5 %collective-permute-done.12.refs_3_ = bf16[4,16,1024]{2,1,0:T(8,128)(2,1)S(1)} collective-permute-done((bf16[4,16,1024]{2,1,0:T(8,128)(2,1)S(1)}, bf16[4,16,1024]{2,1,0:T(8,128)(2,1)S(1)}, u32[]{:S(2)}, u32[]{:S(2)}) %collective-permute-start.12) | collective-permute-done | bytes 131104 | tf_op jit(solution)/shard_map/ppermute | solution.py:59
  72.2 1.2 collective-permute-done.11.refs_2_
  74.0 0.7 copy-done.15
  74.7 2.1 %mix.1 = bf16[2,16,8,128]{3,2,1,0:T(8,128)(2,1)} custom-call(s32[2]{0:T(128)} %pad_add_fusion.where, bf16[4,16,1024]{2,1,0:T(8,128)(2,1)} %copy-done.5, bf16[4,16,1024]{2,1,0:T(8,128)(2,1)} %copy-done.15, bf16[4,16,1024]{2,1,0:T(8,128)(2,1)} %copy-done.14, bf16[4,16,1024]{2,1,0:T(8,128)(2,1)} %copy-done.13, bf16[1024,128]{1,0:T(8,128)(2,1)} %refs_4_.1), custom_call_target="tpu_custom_call" | custom-call | tf_op jit(solution)/shard_map/mix/pallas_call | solution.py:24
  76.8 0.8 slice_bitcast_fusion
  77.6 1.2 collective-permute-done.13
  78.8 0.8 fusion.1
  79.5 2.0 %collective-permute-start.16 = (bf16[1,128,128]{2,1,0:T(8,128)(2,1)S(1)}, bf16[1,128,128]{2,1,0:T(8,128)(2,1)S(1)}, u32[]{:S(2)}, u32[]{:S(2)}) collective-permute-start(bf16[1,128,128]{2,1,0:T(8,128)(2,1)S(1)} %fusion.1), channel_id=1, source_target_pairs={{0,24},{1,25},{2,26},{3,27},{4,28},{5,29},{6,30},{7,31},{8,16},{9,... | collective-permute-start | bytes 98312 | tf_op jit(solution)/shard_map/ppermute | solution.py:59
  81.5 1.1 collective-permute-start.15
  82.7 1.3 collective-permute-start.14
  84.0 1.4 %collective-permute-done.16 = bf16[1,128,128]{2,1,0:T(8,128)(2,1)S(1)} collective-permute-done((bf16[1,128,128]{2,1,0:T(8,128)(2,1)S(1)}, bf16[1,128,128]{2,1,0:T(8,128)(2,1)S(1)}, u32[]{:S(2)}, u32[]{:S(2)}) %collective-permute-start.16) | collective-permute-done | bytes 32800 | tf_op jit(solution)/shard_map/ppermute | solution.py:59
  85.4 1.2 collective-permute-done.15
  87.0 0.9 collective-permute-start.19
  87.9 1.8 %collective-permute-start.18 = (bf16[4,128,128]{2,1,0:T(8,128)(2,1)S(1)}, bf16[4,128,128]{2,1,0:T(8,128)(2,1)S(1)}, u32[]{:S(2)}, u32[]{:S(2)}) collective-permute-start(bf16[4,128,128]{2,1,0:T(8,128)(2,1)S(1)} %pad_maximum_fusion.2.refs_4_), channel_id=1, source_target_pairs={{0,4},{1,5},{2,6},{3,7},{4,0},{5,1},{6,2},{7,3},{8,12},{9,13},{10,... | collective-permute-start | bytes 393224 | tf_op jit(solution)/shard_map/ppermute | solution.py:59
  89.7 0.9 collective-permute-start.17
  90.6 3.8 %collective-permute-done.19.refs_7_ = bf16[4,128,128]{2,1,0:T(8,128)(2,1)S(1)} collective-permute-done((bf16[4,128,128]{2,1,0:T(8,128)(2,1)S(1)}, bf16[4,128,128]{2,1,0:T(8,128)(2,1)S(1)}, u32[]{:S(2)}, u32[]{:S(2)}) %collective-permute-start.19) | collective-permute-done | bytes 131104 | tf_op jit(solution)/shard_map/ppermute | solution.py:59
  94.3 1.1 collective-permute-done.18.refs_6_
  96.1 2.6 %resid.1 = (bf16[128,2048]{1,0:T(8,128)(2,1)}, f32[8,2048]{1,0:T(8,128)}) custom-call(s32[2]{0:T(128)} %pad_add_fusion.where, bf16[4,8,2048]{2,1,0:T(8,128)(2,1)} %copy-done.1, bf16[4,8,2048]{2,1,0:T(8,128)(2,1)} %copy-done.9, bf16[4,8,2048]{2,1,0:T(8,128)(2,1)} %copy-done.8, bf16[4,8,2048]{2,1,0:T(8,128)(2,1)} %copy-done.7, bf16[4,128,128]{2,1,0:T(8,128)(2,1)} %copy-done.6, ...), custom_call_target="tpu_custom_call" | custom-call | tf_op jit(solution)/shard_map/resid/pallas_call | solution.py:24
  99.6 0.7 reshape.50.route
  100.9 0.8 copy-done.3
  101.7 5.9 %experts_other.1 = bf16[128,2048]{1,0:T(8,128)(2,1)} custom-call(bf16[128,2048]{1,0:T(8,128)(2,1)} %copy-done.3, f32[128,1]{1,0:T(8,128)} %reshape.50.route, bf16[1,2048]{1,0:T(2,128)(2,1)} %broadcast_in_dim.36.mix, bf16[2048,128]{1,0:T(8,128)(2,1)} %d_gate.3, bf16[2048,128]{1,0:T(8,128)(2,1)} %d_up.3, bf16[128,2048]{1,0:T(8,128)(2,1)} %d_down.3, ...), custom_call_target="tpu_custom_call" | custom-call | tf_op jit(solution)/shard_map/experts_other/pallas_call | solution.py:24
  107.7 0.7 reshape.49.route
  108.4 6.1 %experts_own.1.own = f32[128,2048]{1,0:T(8,128)} custom-call(bf16[128,2048]{1,0:T(8,128)(2,1)} %get-tuple-element.20.rows_in, f32[128,1]{1,0:T(8,128)} %reshape.49.route, bf16[1,2048]{1,0:T(2,128)(2,1)} %broadcast_in_dim.36.mix, bf16[2048,128]{1,0:T(8,128)(2,1)} %d_gate.3, bf16[2048,128]{1,0:T(8,128)(2,1)} %d_up.3, bf16[128,2048]{1,0:T(8,128)(2,1)} %d_down.3, ...), custom_call_target="tpu_custom_call" | custom-call | tf_op jit(solution)/shard_map/experts_own/pallas_call | solution.py:24
  114.5 0.8 copy-done.4
  115.3 2.2 %fold.1 = (bf16[4,8,2048]{2,1,0:T(8,128)(2,1)}, bf16[4,8,2048]{2,1,0:T(8,128)(2,1)}, bf16[4,8,2048]{2,1,0:T(8,128)(2,1)}, bf16[4,8,2048]{2,1,0:T(8,128)(2,1)}) custom-call(s32[2]{0:T(128)} %pad_add_fusion.where, f32[128,2048]{1,0:T(8,128)} %experts_own.1.own, bf16[128,2048]{1,0:T(8,128)(2,1)} %copy-done.4), custom_call_target="tpu_custom_call" | custom-call | tf_op jit(solution)/shard_map/fold/pallas_call | solution.py:24
  117.5 1.3 collective-permute-start.22
  118.9 0.7 collective-permute-start.23
  119.5 1.5 %collective-permute-start.24 = (bf16[4,8,2048]{2,1,0:T(8,128)(2,1)}, bf16[4,8,2048]{2,1,0:T(8,128)(2,1)S(1)}, u32[]{:S(2)}, u32[]{:S(2)}) collective-permute-start(bf16[4,8,2048]{2,1,0:T(8,128)(2,1)} %get-tuple-element.24), channel_id=1, source_target_pairs={{0,6},{1,7},{2,4},{3,5},{4,2},{5,3},{6,0},{7,1},{8,14},{9,15},{10,... | collective-permute-start | bytes 393224 | tf_op jit(solution)/shard_map/ppermute | solution.py:59
  121.0 3.1 %collective-permute-done.22.refs_1_ = bf16[4,8,2048]{2,1,0:T(8,128)(2,1)S(1)} collective-permute-done((bf16[4,8,2048]{2,1,0:T(8,128)(2,1)}, bf16[4,8,2048]{2,1,0:T(8,128)(2,1)S(1)}, u32[]{:S(2)}, u32[]{:S(2)}) %collective-permute-start.22) | collective-permute-done | bytes 131104 | tf_op jit(solution)/shard_map/ppermute | solution.py:59
  124.1 3.3 %collective-permute-done.23.refs_2_ = bf16[4,8,2048]{2,1,0:T(8,128)(2,1)S(1)} collective-permute-done((bf16[4,8,2048]{2,1,0:T(8,128)(2,1)}, bf16[4,8,2048]{2,1,0:T(8,128)(2,1)S(1)}, u32[]{:S(2)}, u32[]{:S(2)}) %collective-permute-start.23) | collective-permute-done | bytes 131104 | tf_op jit(solution)/shard_map/ppermute | solution.py:59
  127.4 0.6 copy-done.11
  128.1 1.8 %sum1.1 = (bf16[8,2048]{1,0:T(8,128)(2,1)}, bf16[8,2048]{1,0:T(8,128)(2,1)}, bf16[8,2048]{1,0:T(8,128)(2,1)}, bf16[8,2048]{1,0:T(8,128)(2,1)}) custom-call(bf16[4,8,2048]{2,1,0:T(8,128)(2,1)} %get-tuple-element.21.refs_0_, bf16[4,8,2048]{2,1,0:T(8,128)(2,1)} %copy-done.10, bf16[4,8,2048]{2,1,0:T(8,128)(2,1)} %copy-done.11, bf16[4,8,2048]{2,1,0:T(8,128)(2,1)} %copy-done.12), custom_call_target="tpu_custom_call" | custom-call | tf_op jit(solution)/shard_map/sum1/pallas_call | solution.py:24
  130.3 1.5 %collective-permute-start.26 = (bf16[8,2048]{1,0:T(8,128)(2,1)}, bf16[8,2048]{1,0:T(8,128)(2,1)S(1)}, u32[]{:S(2)}, u32[]{:S(2)}) collective-permute-start(bf16[8,2048]{1,0:T(8,128)(2,1)} %get-tuple-element.27), channel_id=1, source_target_pairs={{0,16},{1,17},{2,18},{3,19},{4,20},{5,21},{6,22},{7,23},{8,24},{9,... | collective-permute-start | bytes 98312 | tf_op jit(solution)/shard_map/ppermute | solution.py:59
  131.8 2.4 %collective-permute-start.27 = (bf16[8,2048]{1,0:T(8,128)(2,1)}, bf16[8,2048]{1,0:T(8,128)(2,1)S(1)}, u32[]{:S(2)}, u32[]{:S(2)}) collective-permute-start(bf16[8,2048]{1,0:T(8,128)(2,1)} %get-tuple-element.28), channel_id=1, source_target_pairs={{0,24},{1,25},{2,26},{3,27},{4,28},{5,29},{6,30},{7,31},{8,16},{9,... | collective-permute-start | bytes 98312 | tf_op jit(solution)/shard_map/ppermute | solution.py:59
  134.2 1.3 collective-permute-done.26.refs_2_
  135.5 2.2 %collective-permute-done.27.refs_3_ = bf16[8,2048]{1,0:T(8,128)(2,1)S(1)} collective-permute-done((bf16[8,2048]{1,0:T(8,128)(2,1)}, bf16[8,2048]{1,0:T(8,128)(2,1)S(1)}, u32[]{:S(2)}, u32[]{:S(2)}) %collective-permute-start.27) | collective-permute-done | bytes 32800 | tf_op jit(solution)/shard_map/ppermute | solution.py:59
  138.3 1.5 %last.1 = bf16[8,2048]{1,0:T(8,128)(2,1)} custom-call(f32[8,2048]{1,0:T(8,128)} %get-tuple-element.19.resid, bf16[8,2048]{1,0:T(8,128)(2,1)} %get-tuple-element.25.refs_0_, bf16[8,2048]{1,0:T(8,128)(2,1)} %copy-done.19, bf16[8,2048]{1,0:T(8,128)(2,1)} %copy-done.20, bf16[8,2048]{1,0:T(8,128)(2,1)} %copy-done.21), custom_call_target="tpu_custom_call" | custom-call | tf_op jit(solution)/shard_map/last/pallas_call | solution.py:24
  (67 shorter events, 6.2 us)
Async XLA Ops:
  0.6 7.2 %collective-permute-start.2 = (bf16[1,8,2048]{2,1,0:T(8,128)(2,1)}, bf16[1,8,2048]{2,1,0:T(8,128)(2,1)S(1)}, u32[]{:S(2)}, u32[]{:S(2)}) collective-permute-start(bf16[1,8,2048]{2,1,0:T(8,128)(2,1)} %bitcast.51), channel_id=1, source_target_pairs={{0,24},{1,25},{2,26},{3,27},{4,28},{5,29},{6,30},{7,31},{8,16},{9,... | collective-permute-start | bytes 98312 | tf_op jit(solution)/shard_map/ppermute | solution.py:59
  5.8 5.0 %collective-permute-start.1 = (bf16[1,8,2048]{2,1,0:T(8,128)(2,1)}, bf16[1,8,2048]{2,1,0:T(8,128)(2,1)S(1)}, u32[]{:S(2)}, u32[]{:S(2)}) collective-permute-start(bf16[1,8,2048]{2,1,0:T(8,128)(2,1)} %bitcast.52), channel_id=1, source_target_pairs={{0,16},{1,17},{2,18},{3,19},{4,20},{5,21},{6,22},{7,23},{8,24},{9,... | collective-permute-start | bytes 98312 | tf_op jit(solution)/shard_map/ppermute | solution.py:59
  5.8 5.0 %collective-permute-start = (bf16[1,8,2048]{2,1,0:T(8,128)(2,1)}, bf16[1,8,2048]{2,1,0:T(8,128)(2,1)S(1)}, u32[]{:S(2)}, u32[]{:S(2)}) collective-permute-start(bf16[1,8,2048]{2,1,0:T(8,128)(2,1)} %bitcast.53), channel_id=1, source_target_pairs={{0,8},{1,9},{2,10},{3,11},{4,12},{5,13},{6,14},{7,15},{8,0},{9,1},... | collective-permute-start | bytes 98312 | tf_op jit(solution)/shard_map/ppermute | solution.py:59
  11.6 8.1 %copy-start.1 = (bf16[4,8,2048]{2,1,0:T(8,128)(2,1)}, bf16[4,8,2048]{2,1,0:T(8,128)(2,1)S(1)}, u32[]{:S(2)}) copy-start(bf16[4,8,2048]{2,1,0:T(8,128)(2,1)S(1)} %pad_maximum_fusion.refs_0_) | copy-start | bytes 393220
  11.6 7.3 %collective-permute-start.5 = (bf16[4,8,2048]{2,1,0:T(8,128)(2,1)S(1)}, bf16[4,8,2048]{2,1,0:T(8,128)(2,1)S(1)}, u32[]{:S(2)}, u32[]{:S(2)}) collective-permute-start(bf16[4,8,2048]{2,1,0:T(8,128)(2,1)S(1)} %pad_maximum_fusion.refs_0_), channel_id=1, source_target_pairs={{0,6},{1,7},{2,4},{3,5},{4,2},{5,3},{6,0},{7,1},{8,14},{9,15},{10,... | collective-permute-start | bytes 393224 | tf_op jit(solution)/shard_map/ppermute | solution.py:59
  14.1 5.6 %collective-permute-start.4 = (bf16[4,8,2048]{2,1,0:T(8,128)(2,1)S(1)}, bf16[4,8,2048]{2,1,0:T(8,128)(2,1)S(1)}, u32[]{:S(2)}, u32[]{:S(2)}) collective-permute-start(bf16[4,8,2048]{2,1,0:T(8,128)(2,1)S(1)} %pad_maximum_fusion.refs_0_), channel_id=1, source_target_pairs={{0,4},{1,5},{2,6},{3,7},{4,0},{5,1},{6,2},{7,3},{8,12},{9,13},{10,... | collective-permute-start | bytes 393224 | tf_op jit(solution)/shard_map/ppermute | solution.py:59
  14.6 5.1 %collective-permute-start.3 = (bf16[4,8,2048]{2,1,0:T(8,128)(2,1)S(1)}, bf16[4,8,2048]{2,1,0:T(8,128)(2,1)S(1)}, u32[]{:S(2)}, u32[]{:S(2)}) collective-permute-start(bf16[4,8,2048]{2,1,0:T(8,128)(2,1)S(1)} %pad_maximum_fusion.refs_0_), channel_id=1, source_target_pairs={{0,2},{1,3},{2,0},{3,1},{4,6},{5,7},{6,4},{7,5},{8,10},{9,11},{10,... | collective-permute-start | bytes 393224 | tf_op jit(solution)/shard_map/ppermute | solution.py:59
  18.9 0.8 copy-start.7
  19.7 0.7 copy-start.8
  19.7 0.7 copy-start.9
  22.5 2.1 %collective-permute-start.6 = (bf16[16,8,2048]{2,1,0:T(8,128)(2,1)}, bf16[16,8,2048]{2,1,0:T(8,128)(2,1)S(1)}, u32[]{:S(2)}, u32[]{:S(2)}) collective-permute-start(bf16[16,8,2048]{2,1,0:T(8,128)(2,1)} %norm.1.own), channel_id=1, source_target_pairs={{0,1},{1,0},{2,3},{3,2},{4,5},{5,4},{6,7},{7,6},{8,9},{9,8},{10,11... | collective-permute-start | bytes 1572872 | tf_op jit(solution)/shard_map/ppermute | solution.py:59
  24.7 0.8 copy-start
  28.4 12.0 %all-to-all-start = ((bf16[16,2,8,256]{3,2,1,0:T(8,128)(2,1)}), bf16[16,2,8,256]{3,2,1,0:T(8,128)(2,1)S(1)}, u32[]{:S(2)}, u32[]{:S(2)}) async-start(bf16[16,2,8,256]{3,2,1,0:T(8,128)(2,1)} %project.1), calls=%async_computation | async-start | bytes 262144 | tf_op jit(solution)/shard_map/all_to_all | solution.py:291
  40.4 0.7 copy-start.2
  58.4 40.4 %copy-start.22 = (bf16[2048]{0:T(1024)(128)(2,1)S(1)}, bf16[2048]{0:T(1024)(128)(2,1)}, u32[]{:S(2)}) copy-start(bf16[2048]{0:T(1024)(128)(2,1)} %param.37) | copy-start | bytes 12292
  58.4 41.0 %copy-start.23 = (f32[256,4]{0,1:T(4,128)S(1)}, f32[256,4]{0,1:T(4,128)}, u32[]{:S(2)}) copy-start(f32[256,4]{0,1:T(4,128)} %param.45) | copy-start | bytes 12292
  58.4 41.0 %copy-start.24 = (s32[256,4]{0,1:T(4,128)S(1)}, s32[256,4]{0,1:T(4,128)}, u32[]{:S(2)}) copy-start(s32[256,4]{0,1:T(4,128)} %param.44) | copy-start | bytes 12292
  58.4 6.1 %collective-permute-start.9 = (bf16[1,16,1024]{2,1,0:T(8,128)(2,1)}, bf16[1,16,1024]{2,1,0:T(8,128)(2,1)S(1)}, u32[]{:S(2)}, u32[]{:S(2)}) collective-permute-start(bf16[1,16,1024]{2,1,0:T(8,128)(2,1)} %bitcast.55), channel_id=1, source_target_pairs={{0,24},{1,25},{2,26},{3,27},{4,28},{5,29},{6,30},{7,31},{8,16},{9,... | collective-permute-start | bytes 98312 | tf_op jit(solution)/shard_map/ppermute | solution.py:59
  60.0 5.3 %collective-permute-start.8 = (bf16[1,16,1024]{2,1,0:T(8,128)(2,1)}, bf16[1,16,1024]{2,1,0:T(8,128)(2,1)S(1)}, u32[]{:S(2)}, u32[]{:S(2)}) collective-permute-start(bf16[1,16,1024]{2,1,0:T(8,128)(2,1)} %bitcast.56), channel_id=1, source_target_pairs={{0,16},{1,17},{2,18},{3,19},{4,20},{5,21},{6,22},{7,23},{8,24},{9,... | collective-permute-start | bytes 98312 | tf_op jit(solution)/shard_map/ppermute | solution.py:59
  60.8 4.6 %collective-permute-start.7 = (bf16[1,16,1024]{2,1,0:T(8,128)(2,1)}, bf16[1,16,1024]{2,1,0:T(8,128)(2,1)S(1)}, u32[]{:S(2)}, u32[]{:S(2)}) collective-permute-start(bf16[1,16,1024]{2,1,0:T(8,128)(2,1)} %bitcast.57), channel_id=1, source_target_pairs={{0,8},{1,9},{2,10},{3,11},{4,12},{5,13},{6,14},{7,15},{8,0},{9,1},... | collective-permute-start | bytes 98312 | tf_op jit(solution)/shard_map/ppermute | solution.py:59
  66.1 7.6 %copy-start.5 = (bf16[4,16,1024]{2,1,0:T(8,128)(2,1)}, bf16[4,16,1024]{2,1,0:T(8,128)(2,1)S(1)}, u32[]{:S(2)}) copy-start(bf16[4,16,1024]{2,1,0:T(8,128)(2,1)S(1)} %pad_maximum_fusion.1.refs_0_) | copy-start | bytes 393220
  66.1 6.0 %collective-permute-start.12 = (bf16[4,16,1024]{2,1,0:T(8,128)(2,1)S(1)}, bf16[4,16,1024]{2,1,0:T(8,128)(2,1)S(1)}, u32[]{:S(2)}, u32[]{:S(2)}) collective-permute-start(bf16[4,16,1024]{2,1,0:T(8,128)(2,1)S(1)} %pad_maximum_fusion.1.refs_0_), channel_id=1, source_target_pairs={{0,6},{1,7},{2,4},{3,5},{4,2},{5,3},{6,0},{7,1},{8,14},{9,15},{10,... | collective-permute-start | bytes 393224 | tf_op jit(solution)/shard_map/ppermute | solution.py:59
  67.0 6.4 %collective-permute-start.11 = (bf16[4,16,1024]{2,1,0:T(8,128)(2,1)S(1)}, bf16[4,16,1024]{2,1,0:T(8,128)(2,1)S(1)}, u32[]{:S(2)}, u32[]{:S(2)}) collective-permute-start(bf16[4,16,1024]{2,1,0:T(8,128)(2,1)S(1)} %pad_maximum_fusion.1.refs_0_), channel_id=1, source_target_pairs={{0,4},{1,5},{2,6},{3,7},{4,0},{5,1},{6,2},{7,3},{8,12},{9,13},{10,... | collective-permute-start | bytes 393224 | tf_op jit(solution)/shard_map/ppermute | solution.py:59
  68.7 5.0 %collective-permute-start.10 = (bf16[4,16,1024]{2,1,0:T(8,128)(2,1)S(1)}, bf16[4,16,1024]{2,1,0:T(8,128)(2,1)S(1)}, u32[]{:S(2)}, u32[]{:S(2)}) collective-permute-start(bf16[4,16,1024]{2,1,0:T(8,128)(2,1)S(1)} %pad_maximum_fusion.1.refs_0_), channel_id=1, source_target_pairs={{0,2},{1,3},{2,0},{3,1},{4,6},{5,7},{6,4},{7,5},{8,10},{9,11},{10,... | collective-permute-start | bytes 393224 | tf_op jit(solution)/shard_map/ppermute | solution.py:59
  72.2 1.5 %copy-start.13 = (bf16[4,16,1024]{2,1,0:T(8,128)(2,1)}, bf16[4,16,1024]{2,1,0:T(8,128)(2,1)S(1)}, u32[]{:S(2)}) copy-start(bf16[4,16,1024]{2,1,0:T(8,128)(2,1)S(1)} %collective-permute-done.12.refs_3_) | copy-start | bytes 393220
  73.3 0.6 copy-start.14
  74.0 0.7 copy-start.15
  77.6 1.2 collective-permute-start.13
  79.5 5.9 %collective-permute-start.16 = (bf16[1,128,128]{2,1,0:T(8,128)(2,1)S(1)}, bf16[1,128,128]{2,1,0:T(8,128)(2,1)S(1)}, u32[]{:S(2)}, u32[]{:S(2)}) collective-permute-start(bf16[1,128,128]{2,1,0:T(8,128)(2,1)S(1)} %fusion.1), channel_id=1, source_target_pairs={{0,24},{1,25},{2,26},{3,27},{4,28},{5,29},{6,30},{7,31},{8,16},{9,... | collective-permute-start | bytes 98312 | tf_op jit(solution)/shard_map/ppermute | solution.py:59
  81.5 5.1 %collective-permute-start.15 = (bf16[1,128,128]{2,1,0:T(8,128)(2,1)S(1)}, bf16[1,128,128]{2,1,0:T(8,128)(2,1)S(1)}, u32[]{:S(2)}, u32[]{:S(2)}) collective-permute-start(bf16[1,128,128]{2,1,0:T(8,128)(2,1)S(1)} %fusion.1), channel_id=1, source_target_pairs={{0,16},{1,17},{2,18},{3,19},{4,20},{5,21},{6,22},{7,23},{8,24},{9,... | collective-permute-start | bytes 98312 | tf_op jit(solution)/shard_map/ppermute | solution.py:59
  82.7 4.3 %collective-permute-start.14 = (bf16[1,128,128]{2,1,0:T(8,128)(2,1)S(1)}, bf16[1,128,128]{2,1,0:T(8,128)(2,1)S(1)}, u32[]{:S(2)}, u32[]{:S(2)}) collective-permute-start(bf16[1,128,128]{2,1,0:T(8,128)(2,1)S(1)} %fusion.1), channel_id=1, source_target_pairs={{0,8},{1,9},{2,10},{3,11},{4,12},{5,13},{6,14},{7,15},{8,0},{9,1},... | collective-permute-start | bytes 98312 | tf_op jit(solution)/shard_map/ppermute | solution.py:59
  87.0 8.4 %copy-start.6 = (bf16[4,128,128]{2,1,0:T(8,128)(2,1)}, bf16[4,128,128]{2,1,0:T(8,128)(2,1)S(1)}, u32[]{:S(2)}) copy-start(bf16[4,128,128]{2,1,0:T(8,128)(2,1)S(1)} %pad_maximum_fusion.2.refs_4_) | copy-start | bytes 393220
  87.0 7.3 %collective-permute-start.19 = (bf16[4,128,128]{2,1,0:T(8,128)(2,1)S(1)}, bf16[4,128,128]{2,1,0:T(8,128)(2,1)S(1)}, u32[]{:S(2)}, u32[]{:S(2)}) collective-permute-start(bf16[4,128,128]{2,1,0:T(8,128)(2,1)S(1)} %pad_maximum_fusion.2.refs_4_), channel_id=1, source_target_pairs={{0,6},{1,7},{2,4},{3,5},{4,2},{5,3},{6,0},{7,1},{8,14},{9,15},{10,... | collective-permute-start | bytes 393224 | tf_op jit(solution)/shard_map/ppermute | solution.py:59
  87.9 7.5 %collective-permute-start.18 = (bf16[4,128,128]{2,1,0:T(8,128)(2,1)S(1)}, bf16[4,128,128]{2,1,0:T(8,128)(2,1)S(1)}, u32[]{:S(2)}, u32[]{:S(2)}) collective-permute-start(bf16[4,128,128]{2,1,0:T(8,128)(2,1)S(1)} %pad_maximum_fusion.2.refs_4_), channel_id=1, source_target_pairs={{0,4},{1,5},{2,6},{3,7},{4,0},{5,1},{6,2},{7,3},{8,12},{9,13},{10,... | collective-permute-start | bytes 393224 | tf_op jit(solution)/shard_map/ppermute | solution.py:59
  89.7 5.7 %collective-permute-start.17 = (bf16[4,128,128]{2,1,0:T(8,128)(2,1)S(1)}, bf16[4,128,128]{2,1,0:T(8,128)(2,1)S(1)}, u32[]{:S(2)}, u32[]{:S(2)}) collective-permute-start(bf16[4,128,128]{2,1,0:T(8,128)(2,1)S(1)} %pad_maximum_fusion.2.refs_4_), channel_id=1, source_target_pairs={{0,2},{1,3},{2,0},{3,1},{4,6},{5,7},{6,4},{7,5},{8,10},{9,11},{10,... | collective-permute-start | bytes 393224 | tf_op jit(solution)/shard_map/ppermute | solution.py:59
  94.3 1.1 copy-start.16
  95.4 0.6 copy-start.17
  95.4 0.7 copy-start.18
  98.8 2.1 %collective-permute-start.20 = (bf16[128,2048]{1,0:T(8,128)(2,1)}, bf16[128,2048]{1,0:T(8,128)(2,1)S(1)}, u32[]{:S(2)}, u32[]{:S(2)}) collective-permute-start(bf16[128,2048]{1,0:T(8,128)(2,1)} %get-tuple-element.20.rows_in), channel_id=1, source_target_pairs={{0,1},{1,0},{2,3},{3,2},{4,5},{5,4},{6,7},{7,6},{8,9},{9,8},{10,11... | collective-permute-start | bytes 1572872 | tf_op jit(solution)/shard_map/ppermute | solution.py:59
  100.9 0.8 copy-start.3
  107.5 6.9 %collective-permute-start.21 = (bf16[128,2048]{1,0:T(8,128)(2,1)}, bf16[128,2048]{1,0:T(8,128)(2,1)S(1)}, u32[]{:S(2)}, u32[]{:S(2)}) collective-permute-start(bf16[128,2048]{1,0:T(8,128)(2,1)} %experts_other.1), channel_id=1, source_target_pairs={{0,1},{1,0},{2,3},{3,2},{4,5},{5,4},{6,7},{7,6},{8,9},{9,8},{10,11... | collective-permute-start | bytes 1572872 | tf_op jit(solution)/shard_map/ppermute | solution.py:59
  114.5 0.8 copy-start.4
  117.5 6.5 %collective-permute-start.22 = (bf16[4,8,2048]{2,1,0:T(8,128)(2,1)}, bf16[4,8,2048]{2,1,0:T(8,128)(2,1)S(1)}, u32[]{:S(2)}, u32[]{:S(2)}) collective-permute-start(bf16[4,8,2048]{2,1,0:T(8,128)(2,1)} %get-tuple-element.22), channel_id=1, source_target_pairs={{0,2},{1,3},{2,0},{3,1},{4,6},{5,7},{6,4},{7,5},{8,10},{9,11},{10,... | collective-permute-start | bytes 393224 | tf_op jit(solution)/shard_map/ppermute | solution.py:59
  118.9 8.5 %collective-permute-start.23 = (bf16[4,8,2048]{2,1,0:T(8,128)(2,1)}, bf16[4,8,2048]{2,1,0:T(8,128)(2,1)S(1)}, u32[]{:S(2)}, u32[]{:S(2)}) collective-permute-start(bf16[4,8,2048]{2,1,0:T(8,128)(2,1)} %get-tuple-element.23), channel_id=1, source_target_pairs={{0,4},{1,5},{2,6},{3,7},{4,0},{5,1},{6,2},{7,3},{8,12},{9,13},{10,... | collective-permute-start | bytes 393224 | tf_op jit(solution)/shard_map/ppermute | solution.py:59
  119.5 7.9 %collective-permute-start.24 = (bf16[4,8,2048]{2,1,0:T(8,128)(2,1)}, bf16[4,8,2048]{2,1,0:T(8,128)(2,1)S(1)}, u32[]{:S(2)}, u32[]{:S(2)}) collective-permute-start(bf16[4,8,2048]{2,1,0:T(8,128)(2,1)} %get-tuple-element.24), channel_id=1, source_target_pairs={{0,6},{1,7},{2,4},{3,5},{4,2},{5,3},{6,0},{7,1},{8,14},{9,15},{10,... | collective-permute-start | bytes 393224 | tf_op jit(solution)/shard_map/ppermute | solution.py:59
  124.1 3.3 %copy-start.10 = (bf16[4,8,2048]{2,1,0:T(8,128)(2,1)}, bf16[4,8,2048]{2,1,0:T(8,128)(2,1)S(1)}, u32[]{:S(2)}) copy-start(bf16[4,8,2048]{2,1,0:T(8,128)(2,1)S(1)} %collective-permute-done.22.refs_1_) | copy-start | bytes 393220
  127.4 0.7 copy-start.11
  127.4 0.7 copy-start.12
  129.9 4.4 %collective-permute-start.25 = (bf16[8,2048]{1,0:T(8,128)(2,1)}, bf16[8,2048]{1,0:T(8,128)(2,1)S(1)}, u32[]{:S(2)}, u32[]{:S(2)}) collective-permute-start(bf16[8,2048]{1,0:T(8,128)(2,1)} %get-tuple-element.26), channel_id=1, source_target_pairs={{0,8},{1,9},{2,10},{3,11},{4,12},{5,13},{6,14},{7,15},{8,0},{9,1},... | collective-permute-start | bytes 98312 | tf_op jit(solution)/shard_map/ppermute | solution.py:59
  130.3 5.2 %collective-permute-start.26 = (bf16[8,2048]{1,0:T(8,128)(2,1)}, bf16[8,2048]{1,0:T(8,128)(2,1)S(1)}, u32[]{:S(2)}, u32[]{:S(2)}) collective-permute-start(bf16[8,2048]{1,0:T(8,128)(2,1)} %get-tuple-element.27), channel_id=1, source_target_pairs={{0,16},{1,17},{2,18},{3,19},{4,20},{5,21},{6,22},{7,23},{8,24},{9,... | collective-permute-start | bytes 98312 | tf_op jit(solution)/shard_map/ppermute | solution.py:59
  131.8 5.9 %collective-permute-start.27 = (bf16[8,2048]{1,0:T(8,128)(2,1)}, bf16[8,2048]{1,0:T(8,128)(2,1)S(1)}, u32[]{:S(2)}, u32[]{:S(2)}) collective-permute-start(bf16[8,2048]{1,0:T(8,128)(2,1)} %get-tuple-element.28), channel_id=1, source_target_pairs={{0,24},{1,25},{2,26},{3,27},{4,28},{5,29},{6,30},{7,31},{8,16},{9,... | collective-permute-start | bytes 98312 | tf_op jit(solution)/shard_map/ppermute | solution.py:59
  134.2 3.5 %copy-start.19 = (bf16[8,2048]{1,0:T(8,128)(2,1)}, bf16[8,2048]{1,0:T(8,128)(2,1)S(1)}, u32[]{:S(2)}) copy-start(bf16[8,2048]{1,0:T(8,128)(2,1)S(1)} %collective-permute-done.25.refs_1_) | copy-start | bytes 98308
  135.5 2.2 %copy-start.20 = (bf16[8,2048]{1,0:T(8,128)(2,1)}, bf16[8,2048]{1,0:T(8,128)(2,1)S(1)}, u32[]{:S(2)}) copy-start(bf16[8,2048]{1,0:T(8,128)(2,1)S(1)} %collective-permute-done.26.refs_2_) | copy-start | bytes 98308
  137.7 0.6 copy-start.21

commit v2 on v1

--- a/solution.py
+++ b/solution.py
@@ -15,22 +15,33 @@
 SM = pltpu.SMEM
 
 
-def call(kernel, out_shape, operands, scratch=(), smem=(0,), limit=None, grid=None, in_specs=None, out_specs=None, name=None):
-    if in_specs is None:
-        in_specs = [pl.BlockSpec(memory_space=SM if i in smem else VM) for i in range(len(operands))]
-    extra = {} if grid is None else {"grid": grid}
-    if out_specs is None:
-        out_specs = jax.tree.map(lambda _: pl.BlockSpec(memory_space=VM), out_shape)
+def padded_bytes(shape, dtype):
+    shape = (1, 1) + tuple(shape)
+    item = jnp.dtype(dtype).itemsize
+    lead = 1
+    for n in shape[:-2]:
+        lead *= n
+    return lead * -(-shape[-2] // 8) * 8 * -(-shape[-1] // 128) * 128 * item
+
+
+def call(kernel, out_shape, operands, scratch=(), smem=(0,), hbm=(), loose=(), hbm_out=(), spare=2, name=None):
+    outs, tree = jax.tree.flatten(out_shape)
+    held = [x for i, x in enumerate(operands) if i not in smem and i not in hbm and i not in loose]
+    held += [x for i, x in enumerate(outs) if i not in hbm_out]
+    held += [x for x in scratch if hasattr(x, "shape") and getattr(x, "memory_space", None) == VM]
+    limit = sum(padded_bytes(x.shape, x.dtype) for x in held) + (spare << 20)
+    space = lambda i: SM if i in smem else pltpu.HBM if i in hbm else pl.ANY if i in loose else VM
     return pl.pallas_call(
         kernel,
         out_shape=out_shape,
-        in_specs=in_specs,
-        out_specs=out_specs,
+        in_specs=[pl.BlockSpec(memory_space=space(i)) for i in range(len(operands))],
+        out_specs=jax.tree.unflatten(
+            tree, [pl.BlockSpec(memory_space=pltpu.HBM if i in hbm_out else VM) for i in range(len(outs))]
+        ),
         scratch_shapes=list(scratch),
         compiler_params=pltpu.CompilerParams(vmem_limit_bytes=limit),
         name=name,
-        **extra,
-    )(*operands)
+    )(*[pltpu.with_memory_space_constraint(x, pltpu.HBM) if i in hbm else x for i, x in enumerate(operands)])
 
 
 def digits_of(count):
@@ -71,26 +82,38 @@
     return values * lax.rsqrt(jnp.mean(values * values, axis=-1, keepdims=True) + EPS) * gain
 
 
+def load_kernel(after, wq, wk, wv, wz, gain, stacked, gain_out, rows, sems):
+    each = wq.shape[0]
+    copies = [
+        pltpu.make_async_copy(ref, rows.at[pl.ds(p * each, each), :], sems.at[p]) for p, ref in enumerate((wq, wk, wv, wz))
+    ]
+    copies.append(pltpu.make_async_copy(gain, gain_out, sems.at[4]))
+    for c in copies:
+        c.start()
+    for c in copies:
+        c.wait()
+    stacked[...] = rows[...].astype(F32).T.astype(BF16)
+
+
 def norm_kernel(masks, where, *refs):
-    pieces, gain, out = refs[: len(masks)], refs[-2], refs[-1]
+    pieces, gain, out = refs[: len(masks)], refs[-3], refs[-1]
     me = where[0]
     for ref, row in zip(pieces, masks):
         for j, mask in enumerate(row):
             out[me ^ mask] = scale_rows(ref[j].astype(F32), gain[...]).astype(BF16)
 
 
-def project_kernel(where, own, other, wq, wk, wv, wz, out, stacked):
-    par = where[1]
-    rows, each = wq.shape[0], own.shape[1]
-    for p, ref in enumerate((wq, wk, wv, wz)):
-        stacked[p * rows : (p + 1) * rows, :] = ref[...]
-    for side, ref in ((par, own), (1 - par, other)):
-        x = ref[...].reshape(-1, ref.shape[2])
-        y = lax.dot_general(x, stacked[...], (((1,), (1,)), ((), ())), preferred_element_type=F32)
-        out[:, side] = y.reshape(ref.shape[0], each, -1).astype(BF16)
-
-
-def rates_kernel(where, own, other, wb, wd, rate, bias, beta, retain):
+def project_kernel(other, where, x_ref, stacked, *refs):
+    out = refs[-1]
+    side = 1 - where[1] if other else where[1]
+    x = x_ref[...].reshape(-1, x_ref.shape[2])
+    y = jnp.dot(x, stacked[...], preferred_element_type=F32)
+    out[:, side] = y.reshape(out.shape[0], out.shape[2], -1).astype(BF16)
+    if other:
+        out[:, 1 - side] = refs[0][:, 1 - side]
+
+
+def rates_kernel(where, own, other, wb, wd, rate, bias, ids, chance, beta, retain, route, route_other, column):
     me, par = where[0], where[1]
     each = own.shape[1]
     for side, ref in ((par, own), (1 - par, other)):
@@ -101,82 +124,123 @@
         soft = jnp.maximum(d, 0.0) + jnp.log1p(jnp.exp(-jnp.abs(d)))
         beta[side] = 1.0 / (1.0 + jnp.exp(-b))
         retain[side] = jnp.exp(-rate[...] * soft)
+    picked = jnp.sum(jnp.where(ids[...] == me, chance[...], 0.0), axis=0, keepdims=True)
+    picked = jnp.broadcast_to(picked, (8, picked.shape[1])).T[:, :1]
+    column[...] = picked.reshape(column.shape)
+    route[...] = column[:, par].reshape(route.shape)
+    route_other[...] = column[:, 1 - par].reshape(route.shape)
 
 
 def silu(x):
     return x / (1.0 + jnp.exp(-x))
 
 
-def state_kernel(heads, beta, retain, cols, gain, state, gated, new_state, rows, qt, kt, reads):
-    step = pl.program_id(0)
-    seqs = pl.num_programs(0)
-    size = state.shape[3]
-
-    @pl.when(step == 0)
-    def _():
-        table = cols[...]
-        width = table.shape[1]
-        count = table.shape[0] // gated.shape[0]
-        piece = width // (4 * heads)
-        lane = lax.broadcasted_iota(jnp.int32, (table.shape[0], size), 1)
-        src = lax.broadcasted_iota(jnp.int32, (table.shape[0], size), 0)
-        keep = (lane // piece) == (src // gated.shape[0])
-        pick_lane = lax.broadcasted_iota(jnp.int32, (width, size), 1) % piece
-        pick_row = lax.broadcasted_iota(jnp.int32, (width, size), 0)
-        for p in range(4):
-            for h in range(heads):
-                pick = jnp.where(pick_row == pick_lane + (p * heads + h) * piece, 1.0, 0.0).astype(BF16)
-                spread = jnp.dot(table, pick, preferred_element_type=F32)
-                spread = jnp.where(keep, spread, 0.0).reshape(count, gated.shape[0], size)
-                rows[p, pl.ds(h, gated.shape[0], stride=heads), :] = jnp.sum(spread, axis=0)
-        q = silu(rows[0])
-        q = q * lax.rsqrt(jnp.sum(q * q, axis=-1, keepdims=True) + EPS) * size ** (-0.5)
-        qt[...] = q.T
-        k = silu(rows[1])
-        k = k * lax.rsqrt(jnp.sum(k * k, axis=-1, keepdims=True) + EPS)
-        kt[...] = k.T
-        rows[2] = silu(rows[2])
-        rows[3] = silu(rows[3])
-
+def regroup(blocks, piece):
+    lane = lax.broadcasted_iota(jnp.int32, blocks[0].shape, 1) // piece
+    step = 1
+    while step < len(blocks):
+        low = (lane & step) == 0
+        blocks = list(blocks)
+        for i in range(len(blocks)):
+            if i & step:
+                continue
+            a, b = blocks[i], blocks[i | step]
+            lanes = a.shape[1]
+            blocks[i] = jnp.where(low, a, pltpu.roll(b, step * piece, 1))
+            blocks[i | step] = jnp.where(low, pltpu.roll(a, lanes - step * piece, 1), b)
+        step *= 2
+    return blocks
+
+
+def state_kernel(
+    heads, cols, beta, retain, gain, state, gated, new_state, rows, qt, kt, reads, old, new, wide, sem_in, sem_out
+):
+    seqs, size = state.shape[0], state.shape[3]
+    fetch = lambda i: pltpu.make_async_copy(state.at[i], old.at[i], sem_in.at[i])
+    store = lambda i: pltpu.make_async_copy(new.at[i], new_state.at[i], sem_out.at[i])
+    for i in range(seqs):
+        fetch(i).start()
+    count, width = cols.shape[0], cols.shape[2]
+    piece = width // (4 * heads)
+    for first in range(0, width, size):
+        blocks = []
+        for e in range(count):
+            block = cols[e, :, first : min(first + size, width)].astype(F32)
+            if block.shape[1] < size:
+                block = jnp.concatenate([block, jnp.zeros((seqs, size - block.shape[1]), F32)], axis=1)
+            blocks.append(block)
+        for i, block in enumerate(regroup(blocks, piece)):
+            n = first // piece + i
+            if n < 4 * heads:
+                rows[n // heads, pl.ds(n % heads, seqs, stride=heads), :] = block
+    for h in range(heads):
+        rows[4, pl.ds(h, seqs, stride=heads), :] = jnp.broadcast_to(beta[:, h : h + 1], (seqs, size))
+        rows[5, pl.ds(h, seqs, stride=heads), :] = jnp.broadcast_to(retain[:, h : h + 1], (seqs, size))
+    q = silu(rows[0])
+    q = q * lax.rsqrt(jnp.sum(q * q, axis=-1, keepdims=True) + EPS) * size ** (-0.5)
+    qt[...] = q.T
+    k = silu(rows[1])
+    k = k * lax.rsqrt(jnp.sum(k * k, axis=-1, keepdims=True) + EPS)
+    kt[...] = k.T
+    rows[6] = jnp.broadcast_to(jnp.sum(q * k, axis=-1, keepdims=True), k.shape)
+    rows[2] = silu(rows[2])
+    rows[3] = silu(rows[3])
     lanes = qt.shape[1]
-    back = lax.rem(lanes - step * heads, lanes)
-    q_cols = pltpu.roll(qt[...], back, 1)
-    k_cols = pltpu.roll(kt[...], back, 1)
-    first = pl.multiple_of(step * heads, heads)
-    values = rows[2, pl.ds(first, heads), :]
-    gates = rows[3, pl.ds(first, heads), :]
-    found = []
+
+    def one(step, carry):
+        fetch(step).wait()
+        back = lax.rem(lanes - step * heads, lanes)
+        q_cols = pltpu.roll(qt[...], back, 1)
+        k_cols = pltpu.roll(kt[...], back, 1)
+        at = pl.ds(pl.multiple_of(step * heads, heads), heads)
+        by_key, by_query = [], []
+        for h in range(heads):
+            key_sum = query_sum = None
+            for i in range(0, size, 8):
+                part = old[step, h, i : i + 8, :]
+                k_wide = jnp.broadcast_to(k_cols[i : i + 8, h : h + 1], (8, size))
+                q_wide = jnp.broadcast_to(q_cols[i : i + 8, h : h + 1], (8, size))
+                wide[h, i : i + 8, :] = k_wide
+                key_sum = part * k_wide if key_sum is None else key_sum + part * k_wide
+                query_sum = part * q_wide if query_sum is None else query_sum + part * q_wide
+            by_key.append(jnp.sum(key_sum, axis=0, keepdims=True))
+            by_query.append(jnp.sum(query_sum, axis=0, keepdims=True))
+        keep = rows[5, at, :]
+        change = rows[4, at, :] * (rows[2, at, :] - keep * jnp.concatenate(by_key, axis=0))
+        read = keep * jnp.concatenate(by_query, axis=0) + rows[6, at, :] * change
+        for h in range(heads):
+            keep_h = jnp.broadcast_to(keep[h : h + 1, :], (8, size))
+            change_h = jnp.broadcast_to(change[h : h + 1, :], (8, size))
+            for i in range(0, size, 8):
+                new[step, h, i : i + 8, :] = keep_h * old[step, h, i : i + 8, :] + wide[h, i : i + 8, :] * change_h
+        store(step).start()
+        reads[at, :] = scale_rows(read, gain[...]) * rows[3, at, :]
+        return carry
+
+    lax.fori_loop(0, seqs, one, 0)
     for h in range(heads):
-        keep_rate = retain[step, h]
-        write_rate = beta[step, h]
-        old = state[0, h]
-        k_wide = jnp.broadcast_to(k_cols[:, h : h + 1], (size, size))
-        q_wide = jnp.broadcast_to(q_cols[:, h : h + 1], (size, size))
-        recalled = jnp.sum(old * k_wide, axis=0, keepdims=True)
-        change = write_rate * (values[h : h + 1, :] - keep_rate * recalled)
-        new = keep_rate * old + k_wide * change
-        new_state[0, h] = new
-        found.append(jnp.sum(new * q_wide, axis=0, keepdims=True))
-    read = jnp.concatenate(found, axis=0)
-    reads[pl.ds(first, heads), :] = scale_rows(read, gain[...]) * gates
-
-    @pl.when(step == seqs - 1)
-    def _():
-        for h in range(heads):
-            gated[:, h * size : (h + 1) * size] = reads[pl.ds(h, gated.shape[0], stride=heads), :].astype(BF16)
+        gated[:, h * size : (h + 1) * size] = reads[pl.ds(h, seqs, stride=heads), :].astype(BF16)
+    for i in range(seqs):
+        store(i).wait()
 
 
 def mix_kernel(masks, where, *refs):
-    pieces, weight, out = refs[: len(masks)], refs[-2], refs[-1]
+    pieces, weight, out, out_other, both = refs[: len(masks)], *refs[-4:]
     me, par = where[0], where[1]
-    each = out.shape[2]
+    each = out.shape[1]
     for ref, row in zip(pieces, masks):
         x = ref[...].reshape(-1, ref.shape[2])
         y = jnp.dot(x, weight[...], preferred_element_type=F32)
         y = y.reshape(len(row), 2, each, -1).astype(BF16)
         for j, mask in enumerate(row):
             for side in range(2):
-                out[side ^ par, me ^ mask] = y[j, side]
+                both[side, me ^ mask] = y[j, side]
+    out[...] = both[par]
+    out_other[...] = both[1 - par]
+
+
+def pair_kernel(own, other, out):
+    out[...] = (own[...].astype(F32) + other[...].astype(F32)).reshape(out.shape).astype(out.dtype)
 
 
 def resid_kernel(masks, where, *refs):
@@ -270,71 +334,101 @@
     half = ep_count * each
     sds = jax.ShapeDtypeStruct
 
+    flat = [w.transpose(1, 2, 0).reshape(-1, width) for w in (w_query, w_key, w_value, w_zgate)]
+    columns = 4 * flat[0].shape[0]
     tok_pieces = gather_xor(tokens, digits)
+    stacked, gain_near = call(
+        load_kernel,
+        (sds((width, columns), BF16), sds((1, width), F32)),
+        [tok_pieces[0], *flat, mix_gain[None]],
+        scratch=[VM((columns, width), BF16), pltpu.SemaphoreType.DMA((5,))],
+        smem=(),
+        hbm=range(1, 6),
+        loose=(0,),
+        spare=6,
+        name="load",
+    )
     normed = call(
         functools.partial(norm_kernel, masks),
         sds((ep_count, each, width), BF16),
-        [where, *tok_pieces, mix_gain[None]],
+        [where, *tok_pieces, gain_near, stacked],
+        loose=(len(masks) + 2,),
         name="norm",
     )
     normed_other = exchange(normed, 0, 1)
-
-    flat = [w.transpose(1, 2, 0).reshape(-1, width) for w in (w_query, w_key, w_value, w_zgate)]
-    columns = 4 * flat[0].shape[0]
+    shape = sds((ep_count, 2, each, columns), BF16)
     projected = call(
-        project_kernel,
-        sds((ep_count, 2, each, columns), BF16),
-        [where, normed, normed_other, *flat],
-        scratch=[VM((columns, width), BF16)],
-        name="project",
+        functools.partial(project_kernel, False), shape, [where, normed, stacked], spare=3, name="project_own"
+    )
+    projected = call(
+        functools.partial(project_kernel, True),
+        shape,
+        [where, normed_other, stacked, projected],
+        spare=3,
+        name="project_other",
     )
     by_seq = lax.all_to_all(projected, "ep", split_axis=0, concat_axis=0, tiled=True)
-    beta, retain = call(
+    beta, retain, route, route_other = call(
         rates_kernel,
-        (sds((2, each, heads), F32), sds((2, each, heads), F32)),
-        [where, normed, normed_other, w_beta.T, w_decay.T, decay_rate[None], decay_bias[None]],
+        (
+            sds((2, each, heads), F32),
+            sds((2, each, heads), F32),
+            sds((half, 1), F32),
+            sds((half, 1), F32),
+        ),
+        [
+            where,
+            normed,
+            normed_other,
+            w_beta.T,
+            w_decay.T,
+            decay_rate[None],
+            decay_bias[None],
+            expert_ids.T,
+            route_weight.T,
+        ],
+        scratch=[VM((ep_count, 2, each, 1), F32)],
         name="rates",
     )
 
-    whole = lambda shape: pl.BlockSpec(shape, lambda i: (0,) * len(shape))
-    blocked = pl.BlockSpec((1, heads, size, size), lambda i: (i, 0, 0, 0))
     gated, new_state = call(
         functools.partial(state_kernel, heads),
         (sds((seqs, heads * size), BF16), sds(state.shape, F32)),
         [
+            by_seq.reshape(ep_count, seqs, columns),
             beta.reshape(seqs, heads),
             retain.reshape(seqs, heads),
-            by_seq.reshape(ep_count * seqs, columns),
             head_gain[None],
             state,
         ],
+        smem=(),
+        hbm=(4,),
+        hbm_out=(1,),
         scratch=[
-            VM((4, seqs * heads, size), F32),
+            VM((7, seqs * heads, size), F32),
             VM((size, seqs * heads), F32),
             VM((size, seqs * heads), F32),
             VM((seqs * heads, size), F32),
+            VM(state.shape, F32),
+            VM(state.shape, F32),
+            VM((heads, size, size), F32),
+            pltpu.SemaphoreType.DMA((seqs,)),
+            pltpu.SemaphoreType.DMA((seqs,)),
         ],
-        grid=(seqs,),
-        in_specs=[
-            pl.BlockSpec(memory_space=SM),
-            pl.BlockSpec(memory_space=SM),
-            whole((ep_count * seqs, columns)),
-            whole((1, size)),
-            blocked,
-        ],
-        out_specs=(whole((seqs, heads * size)), blocked),
         name="state",
     )
 
     gated_pieces = gather_xor(gated, digits)
     out_cols = w_out.shape[1]
-    mixed = call(
+    mixed, mixed_other = call(
         functools.partial(mix_kernel, masks),
-        sds((2, ep_count, each, out_cols), BF16),
+        (sds((ep_count, each, out_cols), BF16), sds((ep_count, each, out_cols), BF16)),
         [where, *gated_pieces, w_out],
+        scratch=[VM((2, ep_count, each, out_cols), BF16)],
         name="mix",
     )
-    mixed = (mixed[0].astype(F32) + exchange(mixed[1], 0, 1).astype(F32)).astype(BF16).reshape(half, out_cols)
+    mixed_other = exchange(mixed_other, 0, 1)
+    mixed = call(pair_kernel, sds((half, out_cols), BF16), [mixed, mixed_other], smem=(), name="pair")
     mixed_pieces = gather_xor(mixed, digits)
     if out_cols % 128:
         order = jnp.argsort(me ^ jnp.array([m for row in masks for m in row], jnp.int32))
@@ -349,11 +443,8 @@
     )
     moe_other = exchange(moe_in, 0, 1)
 
-    chosen = jnp.sum(jnp.where(expert_ids == me, route_weight, 0.0), axis=1).reshape(ep_count, 2, each)
-    route = lax.dynamic_index_in_dim(chosen, par, 1, False).reshape(half, 1)
-    route_other = lax.dynamic_index_in_dim(chosen, 1 - par, 1, False).reshape(half, 1)
     weights = [dense_mix[None], dense_gate, dense_up, dense_down, expert_gate[0], expert_up[0], expert_down[0]]
-    run = lambda x, r, dt, name: call(expert_kernel, sds((half, width), dt), [x, r, *weights], smem=(), name=name)
+    run = lambda x, r, dt, name: call(expert_kernel, sds((half, width), dt), [x, r, *weights], smem=(), spare=6, name=name)
     part_own = run(moe_in, route, F32, "experts_own")
     part_other = run(moe_other, route_other, BF16, "experts_other")
 

time: 141 us -> 105 us (0.74)
  Pallas kernels: 46.7 us -> 23.6 us
  local copies, waits for them, and re-layouts: 9.71 us -> 0.1 us
  other arithmetic: 3.02 us -> 0.89 us
    pallas_call x11 -> x14, Pallas kernels: 46.7 us -> 23.6 us  [call(): pl.pallas_call(kernel, out_shape=out_shape, in_specs=[pl.BlockSpec(memory...]
    unnamed x50 -> x32, local copies, waits for them, and re-layouts: 6.77 us -> 0.09 us
    ppermute x28, waiting for transfers between devices: 36.4 us -> 34.7 us  [exchange(): return lax.ppermute(value, AXES, pairs)]
    reshape x3 -> x0, local copies, waits for them, and re-layouts: 1.52 us -> none  [the longest x1 0.72 us: body(): route = lax.dynamic_index_in_dim(chosen, par, 1, False).reshape(half, 1)]
  transfers between devices with their start and end apart: 29 -> 29, of which waited for: 22 -> 23; matrix products, arithmetic and copies ran while one was open for 2% -> 0% of each run, Pallas kernels for 6% -> 5%
where the time goes in v2:
time: 105 us
  waiting for transfers between devices  41.6 us (40%)
  starting transfers between devices  38 us (36%)
  Pallas kernels  23.6 us (22%)
    ppermute x28, waiting for transfers between devices, exchange(): return lax.ppermute(value, AXES, pairs)  34.7 us
    ppermute x28, starting transfers between devices, exchange(): return lax.ppermute(value, AXES, pairs)  33.8 us
    pallas_call x14, Pallas kernels, call(): pl.pallas_call(kernel, out_shape=out_shape, in_specs=[pl.BlockSpec(memory...  23.6 us
    all_to_all x1, waiting for transfers between devices, body(): lax.all_to_all(projected, 'ep', split_axis=0, concat_axis=0, tiled=True)  6.95 us
    all_to_all x1, starting transfers between devices, body(): lax.all_to_all(projected, 'ep', split_axis=0, concat_axis=0, tiled=True)  4.23 us
  transfers between devices with their start and end apart: 29, of which 23 were waited for; matrix products, arithmetic and copies ran while one was open for 0% of the time, Pallas kernels for 5%

profile of v2, /device:TPU:0, one launch (start us, length us, event | category | flops | bytes accessed | tf_op | source)
XLA Modules:
  0.0 105.2 jit_solution(12252534034461120811)
XLA Ops:
  0.6 5.1 %collective-permute-start.2 = (bf16[1,8,2048]{2,1,0:T(8,128)(2,1)}, bf16[1,8,2048]{2,1,0:T(8,128)(2,1)S(1)}, u32[]{:S(2)}, u32[]{:S(2)}) collective-permute-start(bf16[1,8,2048]{2,1,0:T(8,128)(2,1)} %bitcast.61), channel_id=1, source_target_pairs={{0,24},{1,25},{2,26},{3,27},{4,28},{5,29},{6,30},{7,31},{8,16},{9,... | collective-permute-start | bytes 98312 | tf_op jit(solution)/shard_map/ppermute | solution.py:70
  5.8 0.6 collective-permute-start
  6.4 1.5 %collective-permute-done.2 = bf16[1,8,2048]{2,1,0:T(8,128)(2,1)S(1)} collective-permute-done((bf16[1,8,2048]{2,1,0:T(8,128)(2,1)}, bf16[1,8,2048]{2,1,0:T(8,128)(2,1)S(1)}, u32[]{:S(2)}, u32[]{:S(2)}) %collective-permute-start.2) | collective-permute-done | bytes 32800 | tf_op jit(solution)/shard_map/ppermute | solution.py:70
  7.9 2.9 %collective-permute-done.1 = bf16[1,8,2048]{2,1,0:T(8,128)(2,1)S(1)} collective-permute-done((bf16[1,8,2048]{2,1,0:T(8,128)(2,1)}, bf16[1,8,2048]{2,1,0:T(8,128)(2,1)S(1)}, u32[]{:S(2)}, u32[]{:S(2)}) %collective-permute-start.1) | collective-permute-done | bytes 32800 | tf_op jit(solution)/shard_map/ppermute | solution.py:70
  10.8 0.8 pad_maximum_fusion.after.refs_0_
  11.6 2.5 %collective-permute-start.5 = (bf16[4,8,2048]{2,1,0:T(8,128)(2,1)S(1)}, bf16[4,8,2048]{2,1,0:T(8,128)(2,1)S(1)}, u32[]{:S(2)}, u32[]{:S(2)}) collective-permute-start(bf16[4,8,2048]{2,1,0:T(8,128)(2,1)S(1)} %pad_maximum_fusion.after.refs_0_), channel_id=1, source_target_pairs={{0,6},{1,7},{2,4},{3,5},{4,2},{5,3},{6,0},{7,1},{8,14},{9,15},{10,... | collective-permute-start | bytes 393224 | tf_op jit(solution)/shard_map/ppermute | solution.py:70
  14.1 0.5 collective-permute-start.4
  14.6 0.5 collective-permute-start.3
  15.1 0.1 pad_add_fusion.where
  15.2 1.6 %load.1 = (bf16[2048,256]{1,0:T(8,128)(2,1)S(1)}, f32[1,2048]{1,0:T(1,128)S(1)}) custom-call(bf16[4,8,2048]{2,1,0:T(8,128)(2,1)S(1)} %pad_maximum_fusion.after.refs_0_, bf16[64,2048]{1,0:T(8,128)(2,1)} %bitcast.57, bf16[64,2048]{1,0:T(8,128)(2,1)} %bitcast.58, bf16[64,2048]{1,0:T(8,128)(2,1)} %bitcast.59, bf16[64,2048]{1,0:T(8,128)(2,1)} %bitcast.60, ...), custom_call_target="tpu_custom_call" | custom-call | tf_op jit(solution)/shard_map/load/pallas_call | solution.py:34
  16.8 2.1 %collective-permute-done.5.refs_3_ = bf16[4,8,2048]{2,1,0:T(8,128)(2,1)S(1)} collective-permute-done((bf16[4,8,2048]{2,1,0:T(8,128)(2,1)S(1)}, bf16[4,8,2048]{2,1,0:T(8,128)(2,1)S(1)}, u32[]{:S(2)}, u32[]{:S(2)}) %collective-permute-start.5) | collective-permute-done | bytes 131104 | tf_op jit(solution)/shard_map/ppermute | solution.py:70
  18.9 0.8 collective-permute-done.4.refs_2_
  19.7 0.8 norm.1.x_ref.own
  20.5 0.1 collective-permute-start.6
  20.6 0.8 project_own.1.refs_0_
  21.5 1.0 collective-permute-done.6.x_ref.other
  22.5 1.5 %project_other.1 = bf16[16,2,8,256]{3,2,1,0:T(8,128)(2,1)} custom-call(s32[2]{0:T(128)S(1)} %pad_add_fusion.where, bf16[16,8,2048]{2,1,0:T(8,128)(2,1)S(1)} %collective-permute-done.6.x_ref.other, bf16[2048,256]{1,0:T(8,128)(2,1)S(1)} %get-tuple-element.23.refs_5_.stacked, bf16[16,2,8,256]{3,2,1,0:T(8,128)(2,1)S(1)} %project_own.1.refs_0_), custom_call_target="tpu_custom_call" | custom-call | tf_op jit(solution)/shard_map/project_other/pallas_call | solution.py:34
  24.0 4.2 %all-to-all-start = ((bf16[16,2,8,256]{3,2,1,0:T(8,128)(2,1)}), bf16[16,2,8,256]{3,2,1,0:T(8,128)(2,1)S(1)}, u32[]{:S(2)}, u32[]{:S(2)}) async-start(bf16[16,2,8,256]{3,2,1,0:T(8,128)(2,1)} %project_other.1), calls=%async_computation | async-start | bytes 262144 | tf_op jit(solution)/shard_map/all_to_all | solution.py:370
  28.3 0.8 rates.1
  29.1 7.0 %all-to-all-done = bf16[16,2,8,256]{3,2,1,0:T(8,128)(2,1)S(1)} async-done(((bf16[16,2,8,256]{3,2,1,0:T(8,128)(2,1)}), bf16[16,2,8,256]{3,2,1,0:T(8,128)(2,1)S(1)}, u32[]{:S(2)}, u32[]{:S(2)}) %all-to-all-start) | async-done | bytes 131104 | tf_op jit(solution)/shard_map/all_to_all | solution.py:370
  36.1 11.7 %state.2 = (bf16[16,1024]{1,0:T(8,128)(2,1)S(1)}, f32[16,8,128,128]{3,2,1,0:T(8,128)}) custom-call(bf16[16,16,256]{2,1,0:T(8,128)(2,1)S(1)} %bitcast.38, f32[16,8]{1,0:T(8,128)S(1)} %bitcast.50, f32[16,8]{1,0:T(8,128)S(1)} %bitcast.51, f32[1,128]{1,0:T(1,128)S(1)} %bitcast.56, f32[16,8,128,128]{3,2,1,0:T(8,128)} %state.3), custom_call_target="tpu_custom_call" | custom-call | tf_op jit(solution)/shard_map/state/pallas_call | solution.py:34
  47.8 1.6 %collective-permute-start.9 = (bf16[1,16,1024]{2,1,0:T(8,128)(2,1)S(1)}, bf16[1,16,1024]{2,1,0:T(8,128)(2,1)S(1)}, u32[]{:S(2)}, u32[]{:S(2)}) collective-permute-start(bf16[1,16,1024]{2,1,0:T(8,128)(2,1)S(1)} %bitcast.45), channel_id=1, source_target_pairs={{0,24},{1,25},{2,26},{3,27},{4,28},{5,29},{6,30},{7,31},{8,16},{9,... | collective-permute-start | bytes 98312 | tf_op jit(solution)/shard_map/ppermute | solution.py:70
  49.5 0.8 collective-permute-start.8
  50.2 2.1 %collective-permute-start.7 = (bf16[1,16,1024]{2,1,0:T(8,128)(2,1)S(1)}, bf16[1,16,1024]{2,1,0:T(8,128)(2,1)S(1)}, u32[]{:S(2)}, u32[]{:S(2)}) collective-permute-start(bf16[1,16,1024]{2,1,0:T(8,128)(2,1)S(1)} %bitcast.47), channel_id=1, source_target_pairs={{0,8},{1,9},{2,10},{3,11},{4,12},{5,13},{6,14},{7,15},{8,0},{9,1},... | collective-permute-start | bytes 98312 | tf_op jit(solution)/shard_map/ppermute | solution.py:70
  52.3 1.4 %collective-permute-done.9 = bf16[1,16,1024]{2,1,0:T(8,128)(2,1)S(1)} collective-permute-done((bf16[1,16,1024]{2,1,0:T(8,128)(2,1)S(1)}, bf16[1,16,1024]{2,1,0:T(8,128)(2,1)S(1)}, u32[]{:S(2)}, u32[]{:S(2)}) %collective-permute-start.9) | collective-permute-done | bytes 32800 | tf_op jit(solution)/shard_map/ppermute | solution.py:70
  53.7 0.8 collective-permute-done.8
  54.6 0.9 collective-permute-start.12
  55.4 1.7 %collective-permute-start.11 = (bf16[4,16,1024]{2,1,0:T(8,128)(2,1)S(1)}, bf16[4,16,1024]{2,1,0:T(8,128)(2,1)S(1)}, u32[]{:S(2)}, u32[]{:S(2)}) collective-permute-start(bf16[4,16,1024]{2,1,0:T(8,128)(2,1)S(1)} %pad_maximum_fusion.1.refs_0_), channel_id=1, source_target_pairs={{0,4},{1,5},{2,6},{3,7},{4,0},{5,1},{6,2},{7,3},{8,12},{9,13},{10,... | collective-permute-start | bytes 393224 | tf_op jit(solution)/shard_map/ppermute | solution.py:70
  57.1 1.0 collective-permute-start.10
  58.1 2.5 %collective-permute-done.12.refs_3_ = bf16[4,16,1024]{2,1,0:T(8,128)(2,1)S(1)} collective-permute-done((bf16[4,16,1024]{2,1,0:T(8,128)(2,1)S(1)}, bf16[4,16,1024]{2,1,0:T(8,128)(2,1)S(1)}, u32[]{:S(2)}, u32[]{:S(2)}) %collective-permute-start.12) | collective-permute-done | bytes 131104 | tf_op jit(solution)/shard_map/ppermute | solution.py:70
  60.6 1.2 %collective-permute-done.11.refs_2_ = bf16[4,16,1024]{2,1,0:T(8,128)(2,1)S(1)} collective-permute-done((bf16[4,16,1024]{2,1,0:T(8,128)(2,1)S(1)}, bf16[4,16,1024]{2,1,0:T(8,128)(2,1)S(1)}, u32[]{:S(2)}, u32[]{:S(2)}) %collective-permute-start.11) | collective-permute-done | bytes 131104 | tf_op jit(solution)/shard_map/ppermute | solution.py:70
  61.8 0.3 collective-permute-done.10.refs_1_
  62.1 0.8 mix.1
  63.0 0.1 collective-permute-start.13
  63.0 1.2 %collective-permute-done.13.other = bf16[16,8,128]{2,1,0:T(8,128)(2,1)S(1)} collective-permute-done((bf16[16,8,128]{2,1,0:T(8,128)(2,1)S(1)}, bf16[16,8,128]{2,1,0:T(8,128)(2,1)S(1)}, u32[]{:S(2)}, u32[]{:S(2)}) %collective-permute-start.13) | collective-permute-done | bytes 32800 | tf_op jit(solution)/shard_map/ppermute | solution.py:70
  64.2 2.1 %collective-permute-start.16 = (bf16[1,128,128]{2,1,0:T(8,128)(2,1)S(1)}, bf16[1,128,128]{2,1,0:T(8,128)(2,1)S(1)}, u32[]{:S(2)}, u32[]{:S(2)}) collective-permute-start(bf16[1,128,128]{2,1,0:T(8,128)(2,1)S(1)} %bitcast.39), channel_id=1, source_target_pairs={{0,24},{1,25},{2,26},{3,27},{4,28},{5,29},{6,30},{7,31},{8,16},{9,... | collective-permute-start | bytes 98312 | tf_op jit(solution)/shard_map/ppermute | solution.py:70
  66.4 1.1 %collective-permute-start.15 = (bf16[1,128,128]{2,1,0:T(8,128)(2,1)S(1)}, bf16[1,128,128]{2,1,0:T(8,128)(2,1)S(1)}, u32[]{:S(2)}, u32[]{:S(2)}) collective-permute-start(bf16[1,128,128]{2,1,0:T(8,128)(2,1)S(1)} %bitcast.40), channel_id=1, source_target_pairs={{0,16},{1,17},{2,18},{3,19},{4,20},{5,21},{6,22},{7,23},{8,24},{9,... | collective-permute-start | bytes 98312 | tf_op jit(solution)/shard_map/ppermute | solution.py:70
  67.5 1.2 %collective-permute-start.14 = (bf16[1,128,128]{2,1,0:T(8,128)(2,1)S(1)}, bf16[1,128,128]{2,1,0:T(8,128)(2,1)S(1)}, u32[]{:S(2)}, u32[]{:S(2)}) collective-permute-start(bf16[1,128,128]{2,1,0:T(8,128)(2,1)S(1)} %bitcast.41), channel_id=1, source_target_pairs={{0,8},{1,9},{2,10},{3,11},{4,12},{5,13},{6,14},{7,15},{8,0},{9,1},... | collective-permute-start | bytes 98312 | tf_op jit(solution)/shard_map/ppermute | solution.py:70
  68.7 1.4 %collective-permute-done.16 = bf16[1,128,128]{2,1,0:T(8,128)(2,1)S(1)} collective-permute-done((bf16[1,128,128]{2,1,0:T(8,128)(2,1)S(1)}, bf16[1,128,128]{2,1,0:T(8,128)(2,1)S(1)}, u32[]{:S(2)}, u32[]{:S(2)}) %collective-permute-start.16) | collective-permute-done | bytes 32800 | tf_op jit(solution)/shard_map/ppermute | solution.py:70
  70.1 1.3 %collective-permute-done.15 = bf16[1,128,128]{2,1,0:T(8,128)(2,1)S(1)} collective-permute-done((bf16[1,128,128]{2,1,0:T(8,128)(2,1)S(1)}, bf16[1,128,128]{2,1,0:T(8,128)(2,1)S(1)}, u32[]{:S(2)}, u32[]{:S(2)}) %collective-permute-start.15) | collective-permute-done | bytes 32800 | tf_op jit(solution)/shard_map/ppermute | solution.py:70
  71.3 0.4 collective-permute-done.14
  71.7 1.3 %collective-permute-start.19 = (bf16[4,128,128]{2,1,0:T(8,128)(2,1)S(1)}, bf16[4,128,128]{2,1,0:T(8,128)(2,1)S(1)}, u32[]{:S(2)}, u32[]{:S(2)}) collective-permute-start(bf16[4,128,128]{2,1,0:T(8,128)(2,1)S(1)} %pad_maximum_fusion.2.refs_4_), channel_id=1, source_target_pairs={{0,6},{1,7},{2,4},{3,5},{4,2},{5,3},{6,0},{7,1},{8,14},{9,15},{10,... | collective-permute-start | bytes 393224 | tf_op jit(solution)/shard_map/ppermute | solution.py:70
  73.0 1.2 %collective-permute-start.18 = (bf16[4,128,128]{2,1,0:T(8,128)(2,1)S(1)}, bf16[4,128,128]{2,1,0:T(8,128)(2,1)S(1)}, u32[]{:S(2)}, u32[]{:S(2)}) collective-permute-start(bf16[4,128,128]{2,1,0:T(8,128)(2,1)S(1)} %pad_maximum_fusion.2.refs_4_), channel_id=1, source_target_pairs={{0,4},{1,5},{2,6},{3,7},{4,0},{5,1},{6,2},{7,3},{8,12},{9,13},{10,... | collective-permute-start | bytes 393224 | tf_op jit(solution)/shard_map/ppermute | solution.py:70
  74.2 1.1 collective-permute-start.17
  75.2 3.7 %collective-permute-done.19.refs_7_ = bf16[4,128,128]{2,1,0:T(8,128)(2,1)S(1)} collective-permute-done((bf16[4,128,128]{2,1,0:T(8,128)(2,1)S(1)}, bf16[4,128,128]{2,1,0:T(8,128)(2,1)S(1)}, u32[]{:S(2)}, u32[]{:S(2)}) %collective-permute-start.19) | collective-permute-done | bytes 131104 | tf_op jit(solution)/shard_map/ppermute | solution.py:70
  79.0 1.4 %collective-permute-done.18.refs_6_ = bf16[4,128,128]{2,1,0:T(8,128)(2,1)S(1)} collective-permute-done((bf16[4,128,128]{2,1,0:T(8,128)(2,1)S(1)}, bf16[4,128,128]{2,1,0:T(8,128)(2,1)S(1)}, u32[]{:S(2)}, u32[]{:S(2)}) %collective-permute-start.18) | collective-permute-done | bytes 131104 | tf_op jit(solution)/shard_map/ppermute | solution.py:70
  80.4 1.1 %resid.1 = (bf16[128,2048]{1,0:T(8,128)(2,1)S(1)}, f32[8,2048]{1,0:T(8,128)S(1)}) custom-call(s32[2]{0:T(128)S(1)} %pad_add_fusion.where, bf16[4,8,2048]{2,1,0:T(8,128)(2,1)S(1)} %pad_maximum_fusion.after.refs_0_, bf16[4,8,2048]{2,1,0:T(8,128)(2,1)S(1)} %collective-permute-done.3.refs_1_, bf16[4,8,2048]{2,1,0:T(8,128)(2,1)S(1)} %collective-permute-done.4.refs_2_, ...), custom_call_target="tpu_custom_call" | custom-call | tf_op jit(solution)/shard_map/resid/pallas_call | solution.py:34
  81.6 1.9 %collective-permute-done.20.rows_in = bf16[128,2048]{1,0:T(8,128)(2,1)S(1)} collective-permute-done((bf16[128,2048]{1,0:T(8,128)(2,1)S(1)}, bf16[128,2048]{1,0:T(8,128)(2,1)S(1)}, u32[]{:S(2)}, u32[]{:S(2)}) %collective-permute-start.20) | collective-permute-done | bytes 524320 | tf_op jit(solution)/shard_map/ppermute | solution.py:70
  83.5 1.6 %experts_other.1 = bf16[128,2048]{1,0:T(8,128)(2,1)S(1)} custom-call(bf16[128,2048]{1,0:T(8,128)(2,1)S(1)} %collective-permute-done.20.rows_in, f32[128,1]{1,0:T(8,128)S(1)} %get-tuple-element.32.route, bf16[1,2048]{1,0:T(2,128)(2,1)S(1)} %broadcast_in_dim.35.mix, bf16[2048,128]{1,0:T(8,128)(2,1)S(1)} %copy-done.3, bf16[2048,128]{1,0:T(8,128)(2,1)S(1)} %copy-done.4, ...), custom_call_target="tpu_custom_call" | custom-call | tf_op jit(solution)/shard_map/experts_other/pallas_call | solution.py:34
  85.1 0.2 collective-permute-start.21
  85.3 1.6 %experts_own.1.own = f32[128,2048]{1,0:T(8,128)S(1)} custom-call(bf16[128,2048]{1,0:T(8,128)(2,1)S(1)} %get-tuple-element.30.rows_in, f32[128,1]{1,0:T(8,128)S(1)} %get-tuple-element.31.route, bf16[1,2048]{1,0:T(2,128)(2,1)S(1)} %broadcast_in_dim.35.mix, bf16[2048,128]{1,0:T(8,128)(2,1)S(1)} %copy-done.3, bf16[2048,128]{1,0:T(8,128)(2,1)S(1)} %copy-done.4, ...), custom_call_target="tpu_custom_call" | custom-call | tf_op jit(solution)/shard_map/experts_own/pallas_call | solution.py:34
  86.9 0.2 collective-permute-done.21.other
  87.1 0.6 fold.1
  87.7 0.8 collective-permute-start.22
  88.6 1.1 %collective-permute-start.23 = (bf16[4,8,2048]{2,1,0:T(8,128)(2,1)S(1)}, bf16[4,8,2048]{2,1,0:T(8,128)(2,1)S(1)}, u32[]{:S(2)}, u32[]{:S(2)}) collective-permute-start(bf16[4,8,2048]{2,1,0:T(8,128)(2,1)S(1)} %get-tuple-element.35), channel_id=1, source_target_pairs={{0,4},{1,5},{2,6},{3,7},{4,0},{5,1},{6,2},{7,3},{8,12},{9,13},{10,... | collective-permute-start | bytes 393224 | tf_op jit(solution)/shard_map/ppermute | solution.py:70
  89.6 1.7 %collective-permute-start.24 = (bf16[4,8,2048]{2,1,0:T(8,128)(2,1)S(1)}, bf16[4,8,2048]{2,1,0:T(8,128)(2,1)S(1)}, u32[]{:S(2)}, u32[]{:S(2)}) collective-permute-start(bf16[4,8,2048]{2,1,0:T(8,128)(2,1)S(1)} %get-tuple-element.36), channel_id=1, source_target_pairs={{0,6},{1,7},{2,4},{3,5},{4,2},{5,3},{6,0},{7,1},{8,14},{9,15},{10,... | collective-permute-start | bytes 393224 | tf_op jit(solution)/shard_map/ppermute | solution.py:70
  91.3 2.9 %collective-permute-done.22.refs_1_ = bf16[4,8,2048]{2,1,0:T(8,128)(2,1)S(1)} collective-permute-done((bf16[4,8,2048]{2,1,0:T(8,128)(2,1)S(1)}, bf16[4,8,2048]{2,1,0:T(8,128)(2,1)S(1)}, u32[]{:S(2)}, u32[]{:S(2)}) %collective-permute-start.22) | collective-permute-done | bytes 131104 | tf_op jit(solution)/shard_map/ppermute | solution.py:70
  94.1 2.6 %collective-permute-done.23.refs_2_ = bf16[4,8,2048]{2,1,0:T(8,128)(2,1)S(1)} collective-permute-done((bf16[4,8,2048]{2,1,0:T(8,128)(2,1)S(1)}, bf16[4,8,2048]{2,1,0:T(8,128)(2,1)S(1)}, u32[]{:S(2)}, u32[]{:S(2)}) %collective-permute-start.23) | collective-permute-done | bytes 131104 | tf_op jit(solution)/shard_map/ppermute | solution.py:70
  96.8 0.6 collective-permute-start.25
  97.4 1.4 %collective-permute-start.26 = (bf16[8,2048]{1,0:T(8,128)(2,1)S(1)}, bf16[8,2048]{1,0:T(8,128)(2,1)S(1)}, u32[]{:S(2)}, u32[]{:S(2)}) collective-permute-start(bf16[8,2048]{1,0:T(8,128)(2,1)S(1)} %get-tuple-element.39), channel_id=1, source_target_pairs={{0,16},{1,17},{2,18},{3,19},{4,20},{5,21},{6,22},{7,23},{8,24},{9,... | collective-permute-start | bytes 98312 | tf_op jit(solution)/shard_map/ppermute | solution.py:70
  98.8 2.4 %collective-permute-start.27 = (bf16[8,2048]{1,0:T(8,128)(2,1)S(1)}, bf16[8,2048]{1,0:T(8,128)(2,1)S(1)}, u32[]{:S(2)}, u32[]{:S(2)}) collective-permute-start(bf16[8,2048]{1,0:T(8,128)(2,1)S(1)} %get-tuple-element.40), channel_id=1, source_target_pairs={{0,24},{1,25},{2,26},{3,27},{4,28},{5,29},{6,30},{7,31},{8,16},{9,... | collective-permute-start | bytes 98312 | tf_op jit(solution)/shard_map/ppermute | solution.py:70
  101.2 1.0 collective-permute-done.26.refs_2_
  102.2 2.3 %collective-permute-done.27.refs_3_ = bf16[8,2048]{1,0:T(8,128)(2,1)S(1)} collective-permute-done((bf16[8,2048]{1,0:T(8,128)(2,1)S(1)}, bf16[8,2048]{1,0:T(8,128)(2,1)S(1)}, u32[]{:S(2)}, u32[]{:S(2)}) %collective-permute-start.27) | collective-permute-done | bytes 32800 | tf_op jit(solution)/shard_map/ppermute | solution.py:70
  104.6 0.6 last.1
  (45 shorter events, 0.3 us)
Async XLA Ops:
  0.6 7.2 %collective-permute-start.2 = (bf16[1,8,2048]{2,1,0:T(8,128)(2,1)}, bf16[1,8,2048]{2,1,0:T(8,128)(2,1)S(1)}, u32[]{:S(2)}, u32[]{:S(2)}) collective-permute-start(bf16[1,8,2048]{2,1,0:T(8,128)(2,1)} %bitcast.61), channel_id=1, source_target_pairs={{0,24},{1,25},{2,26},{3,27},{4,28},{5,29},{6,30},{7,31},{8,16},{9,... | collective-permute-start | bytes 98312 | tf_op jit(solution)/shard_map/ppermute | solution.py:70
  5.8 5.0 %collective-permute-start.1 = (bf16[1,8,2048]{2,1,0:T(8,128)(2,1)}, bf16[1,8,2048]{2,1,0:T(8,128)(2,1)S(1)}, u32[]{:S(2)}, u32[]{:S(2)}) collective-permute-start(bf16[1,8,2048]{2,1,0:T(8,128)(2,1)} %bitcast.62), channel_id=1, source_target_pairs={{0,16},{1,17},{2,18},{3,19},{4,20},{5,21},{6,22},{7,23},{8,24},{9,... | collective-permute-start | bytes 98312 | tf_op jit(solution)/shard_map/ppermute | solution.py:70
  5.8 5.0 %collective-permute-start = (bf16[1,8,2048]{2,1,0:T(8,128)(2,1)}, bf16[1,8,2048]{2,1,0:T(8,128)(2,1)S(1)}, u32[]{:S(2)}, u32[]{:S(2)}) collective-permute-start(bf16[1,8,2048]{2,1,0:T(8,128)(2,1)} %bitcast.63), channel_id=1, source_target_pairs={{0,8},{1,9},{2,10},{3,11},{4,12},{5,13},{6,14},{7,15},{8,0},{9,1},... | collective-permute-start | bytes 98312 | tf_op jit(solution)/shard_map/ppermute | solution.py:70
  11.6 7.3 %collective-permute-start.5 = (bf16[4,8,2048]{2,1,0:T(8,128)(2,1)S(1)}, bf16[4,8,2048]{2,1,0:T(8,128)(2,1)S(1)}, u32[]{:S(2)}, u32[]{:S(2)}) collective-permute-start(bf16[4,8,2048]{2,1,0:T(8,128)(2,1)S(1)} %pad_maximum_fusion.after.refs_0_), channel_id=1, source_target_pairs={{0,6},{1,7},{2,4},{3,5},{4,2},{5,3},{6,0},{7,1},{8,14},{9,15},{10,... | collective-permute-start | bytes 393224 | tf_op jit(solution)/shard_map/ppermute | solution.py:70
  14.1 5.6 %collective-permute-start.4 = (bf16[4,8,2048]{2,1,0:T(8,128)(2,1)S(1)}, bf16[4,8,2048]{2,1,0:T(8,128)(2,1)S(1)}, u32[]{:S(2)}, u32[]{:S(2)}) collective-permute-start(bf16[4,8,2048]{2,1,0:T(8,128)(2,1)S(1)} %pad_maximum_fusion.after.refs_0_), channel_id=1, source_target_pairs={{0,4},{1,5},{2,6},{3,7},{4,0},{5,1},{6,2},{7,3},{8,12},{9,13},{10,... | collective-permute-start | bytes 393224 | tf_op jit(solution)/shard_map/ppermute | solution.py:70
  14.6 5.1 %collective-permute-start.3 = (bf16[4,8,2048]{2,1,0:T(8,128)(2,1)S(1)}, bf16[4,8,2048]{2,1,0:T(8,128)(2,1)S(1)}, u32[]{:S(2)}, u32[]{:S(2)}) collective-permute-start(bf16[4,8,2048]{2,1,0:T(8,128)(2,1)S(1)} %pad_maximum_fusion.after.refs_0_), channel_id=1, source_target_pairs={{0,2},{1,3},{2,0},{3,1},{4,6},{5,7},{6,4},{7,5},{8,10},{9,11},{10,... | collective-permute-start | bytes 393224 | tf_op jit(solution)/shard_map/ppermute | solution.py:70
  20.5 7.8 %copy-start.7 = (bf16[2048,8]{0,1:T(8,128)(2,1)S(1)}, bf16[2048,8]{0,1:T(8,128)(2,1)}, u32[]{:S(2)}) copy-start(bf16[2048,8]{0,1:T(8,128)(2,1)} %param.29) | copy-start | bytes 98308
  20.5 7.8 %copy-start.8 = (bf16[2048,8]{0,1:T(8,128)(2,1)S(1)}, bf16[2048,8]{0,1:T(8,128)(2,1)}, u32[]{:S(2)}) copy-start(bf16[2048,8]{0,1:T(8,128)(2,1)} %param.30) | copy-start | bytes 98308
  20.5 7.8 %copy-start.10 = (s32[256,4]{0,1:T(4,128)S(1)}, s32[256,4]{0,1:T(4,128)}, u32[]{:S(2)}) copy-start(s32[256,4]{0,1:T(4,128)} %param.44) | copy-start | bytes 12292
  20.5 7.8 %copy-start.11 = (f32[256,4]{0,1:T(4,128)S(1)}, f32[256,4]{0,1:T(4,128)}, u32[]{:S(2)}) copy-start(f32[256,4]{0,1:T(4,128)} %param.45) | copy-start | bytes 12292
  20.5 7.8 %copy-start.12 = (f32[8]{0:T(128)S(1)}, f32[8]{0:T(128)}, u32[]{:S(2)}) copy-start(f32[8]{0:T(128)} %param.31) | copy-start | bytes 100
  20.5 7.8 %copy-start.13 = (f32[8]{0:T(128)S(1)}, f32[8]{0:T(128)}, u32[]{:S(2)}) copy-start(f32[8]{0:T(128)} %param.32) | copy-start | bytes 100
  20.5 15.5 %copy-start.14 = (f32[128]{0:T(128)S(1)}, f32[128]{0:T(128)}, u32[]{:S(2)}) copy-start(f32[128]{0:T(128)} %param.33) | copy-start | bytes 1540
  20.5 2.0 %collective-permute-start.6 = (bf16[16,8,2048]{2,1,0:T(8,128)(2,1)S(1)}, bf16[16,8,2048]{2,1,0:T(8,128)(2,1)S(1)}, u32[]{:S(2)}, u32[]{:S(2)}) collective-permute-start(bf16[16,8,2048]{2,1,0:T(8,128)(2,1)S(1)} %norm.1.x_ref.own), channel_id=1, source_target_pairs={{0,1},{1,0},{2,3},{3,2},{4,5},{5,4},{6,7},{7,6},{8,9},{9,8},{10,11... | collective-permute-start | bytes 1572872 | tf_op jit(solution)/shard_map/ppermute | solution.py:70
  24.0 12.0 %all-to-all-start = ((bf16[16,2,8,256]{3,2,1,0:T(8,128)(2,1)}), bf16[16,2,8,256]{3,2,1,0:T(8,128)(2,1)S(1)}, u32[]{:S(2)}, u32[]{:S(2)}) async-start(bf16[16,2,8,256]{3,2,1,0:T(8,128)(2,1)} %project_other.1), calls=%async_computation | async-start | bytes 262144 | tf_op jit(solution)/shard_map/all_to_all | solution.py:370
  36.1 26.0 %copy-start.6 = (bf16[1024,128]{1,0:T(8,128)(2,1)S(1)}, bf16[1024,128]{1,0:T(8,128)(2,1)}, u32[]{:S(2)}) copy-start(bf16[1024,128]{1,0:T(8,128)(2,1)} %refs_4_.1) | copy-start | bytes 786436
  36.1 44.3 %copy-start.9 = (f32[2048]{0:T(1024)S(1)}, f32[2048]{0:T(1024)}, u32[]{:S(2)}) copy-start(f32[2048]{0:T(1024)} %param.36) | copy-start | bytes 24580
  36.1 47.4 %copy-start.1 = (bf16[1,2048,512]{2,1,0:T(8,128)(2,1)S(1)}, bf16[1,2048,512]{2,1,0:T(8,128)(2,1)}, u32[]{:S(2)}) copy-start(bf16[1,2048,512]{2,1,0:T(8,128)(2,1)} %param.42) | copy-start | bytes 6291460
  36.1 47.4 %copy-start.2 = (bf16[1,512,2048]{2,1,0:T(8,128)(2,1)S(1)}, bf16[1,512,2048]{2,1,0:T(8,128)(2,1)}, u32[]{:S(2)}) copy-start(bf16[1,512,2048]{2,1,0:T(8,128)(2,1)} %param.43) | copy-start | bytes 6291460
  36.1 47.4 %copy-start.3 = (bf16[2048,128]{1,0:T(8,128)(2,1)S(1)}, bf16[2048,128]{1,0:T(8,128)(2,1)}, u32[]{:S(2)}) copy-start(bf16[2048,128]{1,0:T(8,128)(2,1)} %d_gate.3) | copy-start | bytes 1572868
  36.1 47.3 %copy-start.4 = (bf16[2048,128]{1,0:T(8,128)(2,1)S(1)}, bf16[2048,128]{1,0:T(8,128)(2,1)}, u32[]{:S(2)}) copy-start(bf16[2048,128]{1,0:T(8,128)(2,1)} %d_up.3) | copy-start | bytes 1572868
  36.1 47.3 %copy-start.5 = (bf16[128,2048]{1,0:T(8,128)(2,1)S(1)}, bf16[128,2048]{1,0:T(8,128)(2,1)}, u32[]{:S(2)}) copy-start(bf16[128,2048]{1,0:T(8,128)(2,1)} %d_down.3) | copy-start | bytes 1572868
  47.8 33.7 %copy-start.15 = (bf16[2048]{0:T(1024)(128)(2,1)S(1)}, bf16[2048]{0:T(1024)(128)(2,1)}, u32[]{:S(2)}) copy-start(bf16[2048]{0:T(1024)(128)(2,1)} %param.37) | copy-start | bytes 12292
  47.8 35.6 %copy-start = (bf16[1,2048,512]{2,1,0:T(8,128)(2,1)S(1)}, bf16[1,2048,512]{2,1,0:T(8,128)(2,1)}, u32[]{:S(2)}) copy-start(bf16[1,2048,512]{2,1,0:T(8,128)(2,1)} %param.41) | copy-start | bytes 6291460
  47.8 5.9 %collective-permute-start.9 = (bf16[1,16,1024]{2,1,0:T(8,128)(2,1)S(1)}, bf16[1,16,1024]{2,1,0:T(8,128)(2,1)S(1)}, u32[]{:S(2)}, u32[]{:S(2)}) collective-permute-start(bf16[1,16,1024]{2,1,0:T(8,128)(2,1)S(1)} %bitcast.45), channel_id=1, source_target_pairs={{0,24},{1,25},{2,26},{3,27},{4,28},{5,29},{6,30},{7,31},{8,16},{9,... | collective-permute-start | bytes 98312 | tf_op jit(solution)/shard_map/ppermute | solution.py:70
  49.5 5.1 %collective-permute-start.8 = (bf16[1,16,1024]{2,1,0:T(8,128)(2,1)S(1)}, bf16[1,16,1024]{2,1,0:T(8,128)(2,1)S(1)}, u32[]{:S(2)}, u32[]{:S(2)}) collective-permute-start(bf16[1,16,1024]{2,1,0:T(8,128)(2,1)S(1)} %bitcast.46), channel_id=1, source_target_pairs={{0,16},{1,17},{2,18},{3,19},{4,20},{5,21},{6,22},{7,23},{8,24},{9,... | collective-permute-start | bytes 98312 | tf_op jit(solution)/shard_map/ppermute | solution.py:70
  50.2 4.3 %collective-permute-start.7 = (bf16[1,16,1024]{2,1,0:T(8,128)(2,1)S(1)}, bf16[1,16,1024]{2,1,0:T(8,128)(2,1)S(1)}, u32[]{:S(2)}, u32[]{:S(2)}) collective-permute-start(bf16[1,16,1024]{2,1,0:T(8,128)(2,1)S(1)} %bitcast.47), channel_id=1, source_target_pairs={{0,8},{1,9},{2,10},{3,11},{4,12},{5,13},{6,14},{7,15},{8,0},{9,1},... | collective-permute-start | bytes 98312 | tf_op jit(solution)/shard_map/ppermute | solution.py:70
  54.6 6.0 %collective-permute-start.12 = (bf16[4,16,1024]{2,1,0:T(8,128)(2,1)S(1)}, bf16[4,16,1024]{2,1,0:T(8,128)(2,1)S(1)}, u32[]{:S(2)}, u32[]{:S(2)}) collective-permute-start(bf16[4,16,1024]{2,1,0:T(8,128)(2,1)S(1)} %pad_maximum_fusion.1.refs_0_), channel_id=1, source_target_pairs={{0,6},{1,7},{2,4},{3,5},{4,2},{5,3},{6,0},{7,1},{8,14},{9,15},{10,... | collective-permute-start | bytes 393224 | tf_op jit(solution)/shard_map/ppermute | solution.py:70
  55.4 6.4 %collective-permute-start.11 = (bf16[4,16,1024]{2,1,0:T(8,128)(2,1)S(1)}, bf16[4,16,1024]{2,1,0:T(8,128)(2,1)S(1)}, u32[]{:S(2)}, u32[]{:S(2)}) collective-permute-start(bf16[4,16,1024]{2,1,0:T(8,128)(2,1)S(1)} %pad_maximum_fusion.1.refs_0_), channel_id=1, source_target_pairs={{0,4},{1,5},{2,6},{3,7},{4,0},{5,1},{6,2},{7,3},{8,12},{9,13},{10,... | collective-permute-start | bytes 393224 | tf_op jit(solution)/shard_map/ppermute | solution.py:70
  57.1 5.0 %collective-permute-start.10 = (bf16[4,16,1024]{2,1,0:T(8,128)(2,1)S(1)}, bf16[4,16,1024]{2,1,0:T(8,128)(2,1)S(1)}, u32[]{:S(2)}, u32[]{:S(2)}) collective-permute-start(bf16[4,16,1024]{2,1,0:T(8,128)(2,1)S(1)} %pad_maximum_fusion.1.refs_0_), channel_id=1, source_target_pairs={{0,2},{1,3},{2,0},{3,1},{4,6},{5,7},{6,4},{7,5},{8,10},{9,11},{10,... | collective-permute-start | bytes 393224 | tf_op jit(solution)/shard_map/ppermute | solution.py:70
  63.0 1.3 %collective-permute-start.13 = (bf16[16,8,128]{2,1,0:T(8,128)(2,1)S(1)}, bf16[16,8,128]{2,1,0:T(8,128)(2,1)S(1)}, u32[]{:S(2)}, u32[]{:S(2)}) collective-permute-start(bf16[16,8,128]{2,1,0:T(8,128)(2,1)S(1)} %get-tuple-element.28), channel_id=1, source_target_pairs={{0,1},{1,0},{2,3},{3,2},{4,5},{5,4},{6,7},{7,6},{8,9},{9,8},{10,11... | collective-permute-start | bytes 98312 | tf_op jit(solution)/shard_map/ppermute | solution.py:70
  64.2 5.8 %collective-permute-start.16 = (bf16[1,128,128]{2,1,0:T(8,128)(2,1)S(1)}, bf16[1,128,128]{2,1,0:T(8,128)(2,1)S(1)}, u32[]{:S(2)}, u32[]{:S(2)}) collective-permute-start(bf16[1,128,128]{2,1,0:T(8,128)(2,1)S(1)} %bitcast.39), channel_id=1, source_target_pairs={{0,24},{1,25},{2,26},{3,27},{4,28},{5,29},{6,30},{7,31},{8,16},{9,... | collective-permute-start | bytes 98312 | tf_op jit(solution)/shard_map/ppermute | solution.py:70
  66.4 5.0 %collective-permute-start.15 = (bf16[1,128,128]{2,1,0:T(8,128)(2,1)S(1)}, bf16[1,128,128]{2,1,0:T(8,128)(2,1)S(1)}, u32[]{:S(2)}, u32[]{:S(2)}) collective-permute-start(bf16[1,128,128]{2,1,0:T(8,128)(2,1)S(1)} %bitcast.40), channel_id=1, source_target_pairs={{0,16},{1,17},{2,18},{3,19},{4,20},{5,21},{6,22},{7,23},{8,24},{9,... | collective-permute-start | bytes 98312 | tf_op jit(solution)/shard_map/ppermute | solution.py:70
  67.5 4.2 %collective-permute-start.14 = (bf16[1,128,128]{2,1,0:T(8,128)(2,1)S(1)}, bf16[1,128,128]{2,1,0:T(8,128)(2,1)S(1)}, u32[]{:S(2)}, u32[]{:S(2)}) collective-permute-start(bf16[1,128,128]{2,1,0:T(8,128)(2,1)S(1)} %bitcast.41), channel_id=1, source_target_pairs={{0,8},{1,9},{2,10},{3,11},{4,12},{5,13},{6,14},{7,15},{8,0},{9,1},... | collective-permute-start | bytes 98312 | tf_op jit(solution)/shard_map/ppermute | solution.py:70
  71.7 7.3 %collective-permute-start.19 = (bf16[4,128,128]{2,1,0:T(8,128)(2,1)S(1)}, bf16[4,128,128]{2,1,0:T(8,128)(2,1)S(1)}, u32[]{:S(2)}, u32[]{:S(2)}) collective-permute-start(bf16[4,128,128]{2,1,0:T(8,128)(2,1)S(1)} %pad_maximum_fusion.2.refs_4_), channel_id=1, source_target_pairs={{0,6},{1,7},{2,4},{3,5},{4,2},{5,3},{6,0},{7,1},{8,14},{9,15},{10,... | collective-permute-start | bytes 393224 | tf_op jit(solution)/shard_map/ppermute | solution.py:70
  73.0 7.4 %collective-permute-start.18 = (bf16[4,128,128]{2,1,0:T(8,128)(2,1)S(1)}, bf16[4,128,128]{2,1,0:T(8,128)(2,1)S(1)}, u32[]{:S(2)}, u32[]{:S(2)}) collective-permute-start(bf16[4,128,128]{2,1,0:T(8,128)(2,1)S(1)} %pad_maximum_fusion.2.refs_4_), channel_id=1, source_target_pairs={{0,4},{1,5},{2,6},{3,7},{4,0},{5,1},{6,2},{7,3},{8,12},{9,13},{10,... | collective-permute-start | bytes 393224 | tf_op jit(solution)/shard_map/ppermute | solution.py:70
  74.2 6.2 %collective-permute-start.17 = (bf16[4,128,128]{2,1,0:T(8,128)(2,1)S(1)}, bf16[4,128,128]{2,1,0:T(8,128)(2,1)S(1)}, u32[]{:S(2)}, u32[]{:S(2)}) collective-permute-start(bf16[4,128,128]{2,1,0:T(8,128)(2,1)S(1)} %pad_maximum_fusion.2.refs_4_), channel_id=1, source_target_pairs={{0,2},{1,3},{2,0},{3,1},{4,6},{5,7},{6,4},{7,5},{8,10},{9,11},{10,... | collective-permute-start | bytes 393224 | tf_op jit(solution)/shard_map/ppermute | solution.py:70
  81.5 2.0 %collective-permute-start.20 = (bf16[128,2048]{1,0:T(8,128)(2,1)S(1)}, bf16[128,2048]{1,0:T(8,128)(2,1)S(1)}, u32[]{:S(2)}, u32[]{:S(2)}) collective-permute-start(bf16[128,2048]{1,0:T(8,128)(2,1)S(1)} %get-tuple-element.30.rows_in), channel_id=1, source_target_pairs={{0,1},{1,0},{2,3},{3,2},{4,5},{5,4},{6,7},{7,6},{8,9},{9,8},{10,11... | collective-permute-start | bytes 1572872 | tf_op jit(solution)/shard_map/ppermute | solution.py:70
  85.1 2.0 %collective-permute-start.21 = (bf16[128,2048]{1,0:T(8,128)(2,1)S(1)}, bf16[128,2048]{1,0:T(8,128)(2,1)S(1)}, u32[]{:S(2)}, u32[]{:S(2)}) collective-permute-start(bf16[128,2048]{1,0:T(8,128)(2,1)S(1)} %experts_other.1), channel_id=1, source_target_pairs={{0,1},{1,0},{2,3},{3,2},{4,5},{5,4},{6,7},{7,6},{8,9},{9,8},{10,11... | collective-permute-start | bytes 1572872 | tf_op jit(solution)/shard_map/ppermute | solution.py:70
  87.7 6.4 %collective-permute-start.22 = (bf16[4,8,2048]{2,1,0:T(8,128)(2,1)S(1)}, bf16[4,8,2048]{2,1,0:T(8,128)(2,1)S(1)}, u32[]{:S(2)}, u32[]{:S(2)}) collective-permute-start(bf16[4,8,2048]{2,1,0:T(8,128)(2,1)S(1)} %get-tuple-element.34), channel_id=1, source_target_pairs={{0,2},{1,3},{2,0},{3,1},{4,6},{5,7},{6,4},{7,5},{8,10},{9,11},{10,... | collective-permute-start | bytes 393224 | tf_op jit(solution)/shard_map/ppermute | solution.py:70
  88.6 8.2 %collective-permute-start.23 = (bf16[4,8,2048]{2,1,0:T(8,128)(2,1)S(1)}, bf16[4,8,2048]{2,1,0:T(8,128)(2,1)S(1)}, u32[]{:S(2)}, u32[]{:S(2)}) collective-permute-start(bf16[4,8,2048]{2,1,0:T(8,128)(2,1)S(1)} %get-tuple-element.35), channel_id=1, source_target_pairs={{0,4},{1,5},{2,6},{3,7},{4,0},{5,1},{6,2},{7,3},{8,12},{9,13},{10,... | collective-permute-start | bytes 393224 | tf_op jit(solution)/shard_map/ppermute | solution.py:70
  89.6 7.1 %collective-permute-start.24 = (bf16[4,8,2048]{2,1,0:T(8,128)(2,1)S(1)}, bf16[4,8,2048]{2,1,0:T(8,128)(2,1)S(1)}, u32[]{:S(2)}, u32[]{:S(2)}) collective-permute-start(bf16[4,8,2048]{2,1,0:T(8,128)(2,1)S(1)} %get-tuple-element.36), channel_id=1, source_target_pairs={{0,6},{1,7},{2,4},{3,5},{4,2},{5,3},{6,0},{7,1},{8,14},{9,15},{10,... | collective-permute-start | bytes 393224 | tf_op jit(solution)/shard_map/ppermute | solution.py:70
  96.8 4.5 %collective-permute-start.25 = (bf16[8,2048]{1,0:T(8,128)(2,1)S(1)}, bf16[8,2048]{1,0:T(8,128)(2,1)S(1)}, u32[]{:S(2)}, u32[]{:S(2)}) collective-permute-start(bf16[8,2048]{1,0:T(8,128)(2,1)S(1)} %get-tuple-element.38), channel_id=1, source_target_pairs={{0,8},{1,9},{2,10},{3,11},{4,12},{5,13},{6,14},{7,15},{8,0},{9,1},... | collective-permute-start | bytes 98312 | tf_op jit(solution)/shard_map/ppermute | solution.py:70
  97.4 4.8 %collective-permute-start.26 = (bf16[8,2048]{1,0:T(8,128)(2,1)S(1)}, bf16[8,2048]{1,0:T(8,128)(2,1)S(1)}, u32[]{:S(2)}, u32[]{:S(2)}) collective-permute-start(bf16[8,2048]{1,0:T(8,128)(2,1)S(1)} %get-tuple-element.39), channel_id=1, source_target_pairs={{0,16},{1,17},{2,18},{3,19},{4,20},{5,21},{6,22},{7,23},{8,24},{9,... | collective-permute-start | bytes 98312 | tf_op jit(solution)/shard_map/ppermute | solution.py:70
  98.8 5.7 %collective-permute-start.27 = (bf16[8,2048]{1,0:T(8,128)(2,1)S(1)}, bf16[8,2048]{1,0:T(8,128)(2,1)S(1)}, u32[]{:S(2)}, u32[]{:S(2)}) collective-permute-start(bf16[8,2048]{1,0:T(8,128)(2,1)S(1)} %get-tuple-element.40), channel_id=1, source_target_pairs={{0,24},{1,25},{2,26},{3,27},{4,28},{5,29},{6,30},{7,31},{8,16},{9,... | collective-permute-start | bytes 98312 | tf_op jit(solution)/shard_map/ppermute | solution.py:70

commit v3 on v2

--- a/solution.py
+++ b/solution.py
@@ -6,6 +6,7 @@
 from jax.experimental import pallas as pl
 from jax.experimental.pallas import tpu as pltpu
 from jax.sharding import PartitionSpec as P
+
 
 EPS = 1e-06
 AXES = ("ep", "tp")
@@ -24,7 +25,7 @@
     return lead * -(-shape[-2] // 8) * 8 * -(-shape[-1] // 128) * 128 * item
 
 
-def call(kernel, out_shape, operands, scratch=(), smem=(0,), hbm=(), loose=(), hbm_out=(), spare=2, name=None):
+def call(kernel, out_shape, operands, scratch=(), smem=(0,), hbm=(), loose=(), hbm_out=(), spare=2):
     outs, tree = jax.tree.flatten(out_shape)
     held = [x for i, x in enumerate(operands) if i not in smem and i not in hbm and i not in loose]
     held += [x for i, x in enumerate(outs) if i not in hbm_out]
@@ -40,7 +41,6 @@
         ),
         scratch_shapes=list(scratch),
         compiler_params=pltpu.CompilerParams(vmem_limit_bytes=limit),
-        name=name,
     )(*[pltpu.with_memory_space_constraint(x, pltpu.HBM) if i in hbm else x for i, x in enumerate(operands)])
 
 
@@ -70,19 +70,59 @@
     return lax.ppermute(value, AXES, pairs)
 
 
+def exchange_all(parts, shift, radix):
+    got = [parts[0]]
+    for d in range(1, radix):
+        got.append(exchange(parts[d], d << shift))
+    return got
+
+
 def gather_xor(piece, digits):
     cur = piece[None]
     for shift, radix in digits[:-1]:
-        cur = jnp.concatenate([cur] + [exchange(cur, d << shift) for d in range(1, radix)], axis=0)
+        cur = jnp.concatenate(exchange_all([cur] * radix, shift, radix), axis=0)
     shift, radix = digits[-1]
-    return [cur] + [exchange(cur, d << shift) for d in range(1, radix)]
+    return exchange_all([cur] * radix, shift, radix)
+
+
+def scatter_masks(order):
+    rest, done = [0], [0]
+    for shift, radix in order[1:]:
+        rest = [m | (d << shift) for m in rest for d in range(radix)]
+    for shift, radix in order[:-1]:
+        done = [(d << shift) | m for d in range(radix) for m in done]
+    (first, first_radix), (last, last_radix) = order[0], order[-1]
+    sent = [[(d << first) | m for m in rest] for d in range(first_radix)]
+    return sent, [[(d << last) | m for m in done] for d in range(last_radix)]
+
+
+def scatter_xor(parts, order):
+    block = parts[0].shape[1:]
+    for level, (shift, radix) in enumerate(order):
+        got = exchange_all(parts, shift, radix)
+        if level + 1 == len(order):
+            return got
+        nxt, rest = order[level + 1][1], 1
+        for _, r in order[level + 2 :]:
+            rest *= r
+        got = [g.reshape(-1, nxt, rest, *block) for g in got]
+        cut = jax.ShapeDtypeStruct((radix, got[0].shape[0], rest, *block), got[0].dtype)
+        parts = call(cut_kernel, (cut,) * nxt, got, smem=())
+        parts = [p.reshape(-1, *block) for p in parts]
+
+
+def cut_kernel(*refs):
+    radix = refs[-1].shape[0]
+    for j, out in enumerate(refs[radix:]):
+        for d in range(radix):
+            out[d] = refs[d][:, j]
 
 
 def scale_rows(values, gain):
     return values * lax.rsqrt(jnp.mean(values * values, axis=-1, keepdims=True) + EPS) * gain
 
 
-def load_kernel(after, wq, wk, wv, wz, gain, stacked, gain_out, rows, sems):
+def load_kernel(after, wq, wk, wv, wz, gain, state, stacked, gain_out, near, short, rows, sems, state_sems):
     each = wq.shape[0]
     copies = [
         pltpu.make_async_copy(ref, rows.at[pl.ds(p * each, each), :], sems.at[p]) for p, ref in enumerate((wq, wk, wv, wz))
@@ -90,9 +130,20 @@
     copies.append(pltpu.make_async_copy(gain, gain_out, sems.at[4]))
     for c in copies:
         c.start()
+    seqs = state.shape[0]
+    fetch = lambda i: pltpu.make_async_copy(state.at[i], near.at[i], state_sems.at[i])
+    for i in range(seqs):
+        fetch(i).start()
     for c in copies:
         c.wait()
     stacked[...] = rows[...].astype(F32).T.astype(BF16)
+
+    def one(i, carry):
+        fetch(i).wait()
+        short[i] = near[i].astype(BF16)
+        return carry
+
+    lax.fori_loop(0, seqs, one, 0)
 
 
 def norm_kernel(masks, where, *refs):
@@ -103,19 +154,26 @@
             out[me ^ mask] = scale_rows(ref[j].astype(F32), gain[...]).astype(BF16)
 
 
-def project_kernel(other, where, x_ref, stacked, *refs):
-    out = refs[-1]
-    side = 1 - where[1] if other else where[1]
+def project_own_kernel(x_ref, stacked, out):
     x = x_ref[...].reshape(-1, x_ref.shape[2])
     y = jnp.dot(x, stacked[...], preferred_element_type=F32)
-    out[:, side] = y.reshape(out.shape[0], out.shape[2], -1).astype(BF16)
-    if other:
-        out[:, 1 - side] = refs[0][:, 1 - side]
-
-
-def rates_kernel(where, own, other, wb, wd, rate, bias, ids, chance, beta, retain, route, route_other, column):
+    out[...] = y.reshape(out.shape).astype(BF16)
+
+
+def project_kernel(sent, where, x_ref, own, stacked, *refs):
+    outs, other = refs[:-1], refs[-1]
     me, par = where[0], where[1]
-    each = own.shape[1]
+    project_own_kernel(x_ref, stacked, other)
+    for out, row in zip(outs, sent):
+        for j, mask in enumerate(row):
+            out[j, par] = own[me ^ mask]
+            out[j, 1 - par] = other[me ^ mask]
+
+
+def rates_kernel(
+    where, own, other, wb, wd, rate, bias, ids, chance, beta, retain, route, route_other, column
+):
+    me, par = where[0], where[1]
     for side, ref in ((par, own), (1 - par, other)):
         x = ref[me]
         b = lax.dot_general(x, wb[...], (((1,), (1,)), ((), ())), preferred_element_type=F32)
@@ -152,14 +210,14 @@
     return blocks
 
 
-def state_kernel(
-    heads, cols, beta, retain, gain, state, gated, new_state, rows, qt, kt, reads, old, new, wide, sem_in, sem_out
-):
-    seqs, size = state.shape[0], state.shape[3]
-    fetch = lambda i: pltpu.make_async_copy(state.at[i], old.at[i], sem_in.at[i])
-    store = lambda i: pltpu.make_async_copy(new.at[i], new_state.at[i], sem_out.at[i])
-    for i in range(seqs):
-        fetch(i).start()
+def state_kernel(heads, came, where, *refs):
+    pieces, (beta, retain, gain, near, short, gated, new_state) = refs[: len(came)], refs[len(came) : len(came) + 7]
+    cols, rows, both, reads, lefts, new, sems = refs[len(came) + 7 :]
+    for ref, row in zip(pieces, came):
+        for j, mask in enumerate(row):
+            cols[where[0] ^ mask] = ref[j].reshape(cols.shape[1:])
+    seqs, size = near.shape[0], near.shape[2]
+    store = lambda i: pltpu.make_async_copy(new.at[i], new_state.at[i], sems.at[i])
     count, width = cols.shape[0], cols.shape[2]
     piece = width // (4 * heads)
     for first in range(0, width, size):
@@ -178,50 +236,73 @@
         rows[5, pl.ds(h, seqs, stride=heads), :] = jnp.broadcast_to(retain[:, h : h + 1], (seqs, size))
     q = silu(rows[0])
     q = q * lax.rsqrt(jnp.sum(q * q, axis=-1, keepdims=True) + EPS) * size ** (-0.5)
-    qt[...] = q.T
     k = silu(rows[1])
     k = k * lax.rsqrt(jnp.sum(k * k, axis=-1, keepdims=True) + EPS)
-    kt[...] = k.T
-    rows[6] = jnp.broadcast_to(jnp.sum(q * k, axis=-1, keepdims=True), k.shape)
-    rows[2] = silu(rows[2])
-    rows[3] = silu(rows[3])
-    lanes = qt.shape[1]
-
-    def one(step, carry):
-        fetch(step).wait()
-        back = lax.rem(lanes - step * heads, lanes)
-        q_cols = pltpu.roll(qt[...], back, 1)
-        k_cols = pltpu.roll(kt[...], back, 1)
-        at = pl.ds(pl.multiple_of(step * heads, heads), heads)
-        by_key, by_query = [], []
+    dots = jnp.sum(q * k, axis=-1, keepdims=True)
+    owner = lax.broadcasted_iota(jnp.int32, (seqs, heads, size), 1)
+    k3, q3 = k.reshape(seqs, heads, size), q.reshape(seqs, heads, size)
+    for h in range(heads):
+        at = slice(h * size, (h + 1) * size)
+        both[:, :heads, at] = jnp.where(owner == h, k3, 0.0).astype(BF16)
+        both[:, heads:, at] = jnp.where(owner == h, q3, 0.0).astype(BF16)
+    for i in range(seqs):
+        found = jnp.dot(both[i], short[i], preferred_element_type=F32)
+        reads[0, i * heads : (i + 1) * heads, :] = found[:heads]
+        reads[1, i * heads : (i + 1) * heads, :] = found[heads:]
+    keep = rows[5]
+    change = rows[4] * (silu(rows[2]) - keep * reads[0])
+    reads[0] = change
+    read = keep * reads[1] + dots * change
+    reads[1] = scale_rows(read, gain[...]) * silu(rows[3])
+    for h in range(heads):
+        gated[:, h * size : (h + 1) * size] = reads[1, pl.ds(h, seqs, stride=heads), :].astype(BF16)
+    high = k.astype(BF16).astype(F32)
+    low = (k - high).astype(BF16).astype(F32)
+    lefts[:, :heads] = high.reshape(seqs, heads, size)
+    lefts[:, heads : 2 * heads] = high.reshape(seqs, heads, size)
+    lefts[:, 2 * heads : 3 * heads] = low.reshape(seqs, heads, size)
+    lefts[:, 3 * heads :] = jnp.zeros((seqs, lefts.shape[1] - 3 * heads, size), F32)
+    head_row = lax.broadcasted_iota(jnp.int32, (lefts.shape[1], size), 0) % heads
+
+    def one(i, carry):
+        at = pl.ds(pl.multiple_of(i * heads, heads), heads)
+        step = reads[0, at, :]
+        top = step.astype(BF16).astype(F32)
+        rest = step - top
+        right = jnp.concatenate([top, rest, top, jnp.zeros_like(top)], axis=0)
+        right = jnp.concatenate([jnp.where(head_row == h, right, 0.0).astype(BF16) for h in range(heads)], axis=1)
+        added = jnp.dot(lefts[i].T.astype(BF16), right, preferred_element_type=F32)
+        rate = rows[5, at, :]
         for h in range(heads):
-            key_sum = query_sum = None
-            for i in range(0, size, 8):
-                part = old[step, h, i : i + 8, :]
-                k_wide = jnp.broadcast_to(k_cols[i : i + 8, h : h + 1], (8, size))
-                q_wide = jnp.broadcast_to(q_cols[i : i + 8, h : h + 1], (8, size))
-                wide[h, i : i + 8, :] = k_wide
-                key_sum = part * k_wide if key_sum is None else key_sum + part * k_wide
-                query_sum = part * q_wide if query_sum is None else query_sum + part * q_wide
-            by_key.append(jnp.sum(key_sum, axis=0, keepdims=True))
-            by_query.append(jnp.sum(query_sum, axis=0, keepdims=True))
-        keep = rows[5, at, :]
-        change = rows[4, at, :] * (rows[2, at, :] - keep * jnp.concatenate(by_key, axis=0))
-        read = keep * jnp.concatenate(by_query, axis=0) + rows[6, at, :] * change
-        for h in range(heads):
-            keep_h = jnp.broadcast_to(keep[h : h + 1, :], (8, size))
-            change_h = jnp.broadcast_to(change[h : h + 1, :], (8, size))
-            for i in range(0, size, 8):
-                new[step, h, i : i + 8, :] = keep_h * old[step, h, i : i + 8, :] + wide[h, i : i + 8, :] * change_h
-        store(step).start()
-        reads[at, :] = scale_rows(read, gain[...]) * rows[3, at, :]
+            old = near[i, h * size : (h + 1) * size, :]
+            new[i, h] = rate[h : h + 1, :] * old + added[:, h * size : (h + 1) * size]
+        store(i).start()
         return carry
 
-    lax.fori_loop(0, seqs, one, 0)
-    for h in range(heads):
-        gated[:, h * size : (h + 1) * size] = reads[pl.ds(h, seqs, stride=heads), :].astype(BF16)
+    lax.fori_loop(0, seqs, one, 0, unroll=2)
     for i in range(seqs):
         store(i).wait()
+
+
+def run_state(came, where, pieces, beta, retain, gain, near, short, shape):
+    seqs, heads, size = shape[:3]
+    count, columns = sum(map(len, came)), pieces[0].shape[-1]
+    sds = jax.ShapeDtypeStruct
+    return call(
+        functools.partial(state_kernel, heads, came),
+        (sds((seqs, heads * size), BF16), sds(shape, F32)),
+        [where, *pieces, beta, retain, gain, near, short],
+        hbm_out=(1,),
+        scratch=[
+            VM((count, seqs, columns), BF16),
+            VM((6, seqs * heads, size), F32),
+            VM((seqs, 2 * heads, heads * size), BF16),
+            VM((2, seqs * heads, size), F32),
+            VM((seqs, 4 * heads, size), F32),
+            VM(shape, F32),
+            pltpu.SemaphoreType.DMA((seqs,)),
+        ],
+    )
 
 
 def mix_kernel(masks, where, *refs):
@@ -337,37 +418,39 @@
     flat = [w.transpose(1, 2, 0).reshape(-1, width) for w in (w_query, w_key, w_value, w_zgate)]
     columns = 4 * flat[0].shape[0]
     tok_pieces = gather_xor(tokens, digits)
-    stacked, gain_near = call(
+    stacked, gain_near, near, short = call(
         load_kernel,
-        (sds((width, columns), BF16), sds((1, width), F32)),
-        [tok_pieces[0], *flat, mix_gain[None]],
-        scratch=[VM((columns, width), BF16), pltpu.SemaphoreType.DMA((5,))],
+        (
+            sds((width, columns), BF16),
+            sds((1, width), F32),
+            sds((seqs, heads * size, size), F32),
+            sds((seqs, heads * size, size), BF16),
+        ),
+        [tok_pieces[0], *flat, mix_gain[None], state.reshape(seqs, heads * size, size)],
+        scratch=[VM((columns, width), BF16), pltpu.SemaphoreType.DMA((5,)), pltpu.SemaphoreType.DMA((seqs,))],
         smem=(),
-        hbm=range(1, 6),
+        hbm=range(1, 7),
         loose=(0,),
         spare=6,
-        name="load",
     )
     normed = call(
         functools.partial(norm_kernel, masks),
         sds((ep_count, each, width), BF16),
         [where, *tok_pieces, gain_near, stacked],
         loose=(len(masks) + 2,),
-        name="norm",
     )
     normed_other = exchange(normed, 0, 1)
-    shape = sds((ep_count, 2, each, columns), BF16)
+    order = digits[::-1]
+    sent, came = scatter_masks(order)
+    projected = call(project_own_kernel, sds((ep_count, each, columns), BF16), [normed, stacked], smem=(), spare=3)
     projected = call(
-        functools.partial(project_kernel, False), shape, [where, normed, stacked], spare=3, name="project_own"
-    )
-    projected = call(
-        functools.partial(project_kernel, True),
-        shape,
-        [where, normed_other, stacked, projected],
+        functools.partial(project_kernel, sent),
+        tuple(sds((len(row), 2, each, columns), BF16) for row in sent),
+        [where, normed_other, projected, stacked],
+        scratch=[VM((ep_count, each, columns), BF16)],
         spare=3,
-        name="project_other",
-    )
-    by_seq = lax.all_to_all(projected, "ep", split_axis=0, concat_axis=0, tiled=True)
+    )
+    by_seq = scatter_xor(projected, order)
     beta, retain, route, route_other = call(
         rates_kernel,
         (
@@ -388,34 +471,17 @@
             route_weight.T,
         ],
         scratch=[VM((ep_count, 2, each, 1), F32)],
-        name="rates",
-    )
-
-    gated, new_state = call(
-        functools.partial(state_kernel, heads),
-        (sds((seqs, heads * size), BF16), sds(state.shape, F32)),
-        [
-            by_seq.reshape(ep_count, seqs, columns),
-            beta.reshape(seqs, heads),
-            retain.reshape(seqs, heads),
-            head_gain[None],
-            state,
-        ],
-        smem=(),
-        hbm=(4,),
-        hbm_out=(1,),
-        scratch=[
-            VM((7, seqs * heads, size), F32),
-            VM((size, seqs * heads), F32),
-            VM((size, seqs * heads), F32),
-            VM((seqs * heads, size), F32),
-            VM(state.shape, F32),
-            VM(state.shape, F32),
-            VM((heads, size, size), F32),
-            pltpu.SemaphoreType.DMA((seqs,)),
-            pltpu.SemaphoreType.DMA((seqs,)),
-        ],
-        name="state",
+    )
+    gated, new_state = run_state(
+        came,
+        where,
+        by_seq,
+        beta.reshape(seqs, heads),
+        retain.reshape(seqs, heads),
+        head_gain[None],
+        near,
+        short,
+        state.shape,
     )
 
     gated_pieces = gather_xor(gated, digits)
@@ -425,10 +491,9 @@
         (sds((ep_count, each, out_cols), BF16), sds((ep_count, each, out_cols), BF16)),
         [where, *gated_pieces, w_out],
         scratch=[VM((2, ep_count, each, out_cols), BF16)],
-        name="mix",
     )
     mixed_other = exchange(mixed_other, 0, 1)
-    mixed = call(pair_kernel, sds((half, out_cols), BF16), [mixed, mixed_other], smem=(), name="pair")
+    mixed = call(pair_kernel, sds((half, out_cols), BF16), [mixed, mixed_other], smem=())
     mixed_pieces = gather_xor(mixed, digits)
     if out_cols % 128:
         order = jnp.argsort(me ^ jnp.array([m for row in masks for m in row], jnp.int32))
@@ -439,25 +504,23 @@
         (sds((half, width), BF16), sds((each, width), F32)),
         [where, *tok_pieces, *mixed_pieces, moe_gain[None]],
         scratch=[VM((half, width), F32)],
-        name="resid",
     )
     moe_other = exchange(moe_in, 0, 1)
 
     weights = [dense_mix[None], dense_gate, dense_up, dense_down, expert_gate[0], expert_up[0], expert_down[0]]
-    run = lambda x, r, dt, name: call(expert_kernel, sds((half, width), dt), [x, r, *weights], smem=(), spare=6, name=name)
-    part_own = run(moe_in, route, F32, "experts_own")
-    part_other = run(moe_other, route_other, BF16, "experts_other")
+    run = lambda x, r, dt: call(expert_kernel, sds((half, width), dt), [x, r, *weights], smem=(), spare=6)
+    part_own = run(moe_in, route, F32)
+    part_other = run(moe_other, route_other, BF16)
 
     prev = len(masks[0])
     parts = call(
         functools.partial(fold_kernel, masks),
         tuple(sds((prev, each, width), BF16) for _ in masks),
         [where, part_own, exchange(part_other, 0, 1)],
-        name="fold",
     )
     for level in range(len(digits) - 1, 0, -1):
         shift, radix = digits[level]
-        got = [parts[0]] + [exchange(parts[d], d << shift) for d in range(1, radix)]
+        got = exchange_all(parts, shift, radix)
         nxt = digits[level - 1][1]
         got = [g.reshape(nxt, -1, width) for g in got]
         parts = call(
@@ -465,11 +528,10 @@
             tuple(sds(got[0].shape[1:], BF16) for _ in range(nxt)),
             got,
             smem=(),
-            name=f"sum{level}",
         )
     shift, radix = digits[0]
-    got = [parts[0]] + [exchange(parts[d], d << shift) for d in range(1, radix)]
-    layer_out = call(last_kernel, sds((each, width), BF16), [resid, *got], smem=(), name="last")
+    got = exchange_all(parts, shift, radix)
+    layer_out = call(last_kernel, sds((each, width), BF16), [resid, *got], smem=())
     return (layer_out, new_state)
 
 

time: 105 us -> 107 us (1.019)
  Pallas kernels: 23.6 us -> 19.1 us
  starting transfers between devices: 38 us -> 41.7 us
  waiting for transfers between devices: 41.6 us -> 43.6 us
    ppermute x28 -> x34, waiting for transfers between devices: 34.7 us -> 43.6 us  [exchange(): return lax.ppermute(value, AXES, pairs)]
    ppermute x28 -> x34, starting transfers between devices: 33.8 us -> 41.7 us  [exchange(): return lax.ppermute(value, AXES, pairs)]
    all_to_all x1 -> x0, waiting for transfers between devices: 6.95 us -> none  [body(): lax.all_to_all(projected, 'ep', split_axis=0, concat_axis=0, tiled=True)]
    pallas_call x14 -> x15, Pallas kernels: 23.6 us -> 19.1 us  [call(): pl.pallas_call(kernel, out_shape=out_shape, in_specs=[pl.BlockSpec(memory...]
    all_to_all x1 -> x0, starting transfers between devices: 4.23 us -> none  [body(): lax.all_to_all(projected, 'ep', split_axis=0, concat_axis=0, tiled=True)]
  transfers between devices with their start and end apart: 29 -> 34, of which waited for: 23 -> 24; matrix products, arithmetic and copies ran while one was open for 0% -> 0% of each run, Pallas kernels for 5% -> 7%
where the time goes in v3:
time: 107 us; the launch traced here: 106 us
  waiting for transfers between devices  43.6 us (41%)
  starting transfers between devices  41.7 us (39%)
  Pallas kernels  19.1 us (18%)
    ppermute x34, waiting for transfers between devices, exchange(): return lax.ppermute(value, AXES, pairs)  43.6 us
    ppermute x34, starting transfers between devices, exchange(): return lax.ppermute(value, AXES, pairs)  41.7 us
    pallas_call x15, Pallas kernels, call(): pl.pallas_call(kernel, out_shape=out_shape, in_specs=[pl.BlockSpec(memory...  19.1 us
  transfers between devices with their start and end apart: 34, of which 24 were waited for; matrix products, arithmetic and copies ran while one was open for 0% of the time, Pallas kernels for 7%

profile of v3, /device:TPU:0, one launch (start us, length us, event | category | flops | bytes accessed | tf_op | source)
XLA Modules:
  0.0 106.4 jit_solution(1639077318007899375)
XLA Ops:
  0.6 3.1 %collective-permute-start = (bf16[1,8,2048]{2,1,0:T(8,128)(2,1)}, bf16[1,8,2048]{2,1,0:T(8,128)(2,1)S(1)}, u32[]{:S(2)}, u32[]{:S(2)}) collective-permute-start(bf16[1,8,2048]{2,1,0:T(8,128)(2,1)} %bitcast.77), channel_id=1, source_target_pairs={{0,8},{1,9},{2,10},{3,11},{4,12},{5,13},{6,14},{7,15},{8,0},{9,1},... | collective-permute-start | bytes 98312 | tf_op jit(solution)/shard_map/ppermute | solution.py:70
  3.7 2.6 %collective-permute-start.1 = (bf16[1,8,2048]{2,1,0:T(8,128)(2,1)}, bf16[1,8,2048]{2,1,0:T(8,128)(2,1)S(1)}, u32[]{:S(2)}, u32[]{:S(2)}) collective-permute-start(bf16[1,8,2048]{2,1,0:T(8,128)(2,1)} %bitcast.78), channel_id=1, source_target_pairs={{0,16},{1,17},{2,18},{3,19},{4,20},{5,21},{6,22},{7,23},{8,24},{9,... | collective-permute-start | bytes 98312 | tf_op jit(solution)/shard_map/ppermute | solution.py:70
  6.3 3.0 %collective-permute-done.1 = bf16[1,8,2048]{2,1,0:T(8,128)(2,1)S(1)} collective-permute-done((bf16[1,8,2048]{2,1,0:T(8,128)(2,1)}, bf16[1,8,2048]{2,1,0:T(8,128)(2,1)S(1)}, u32[]{:S(2)}, u32[]{:S(2)}) %collective-permute-start.1) | collective-permute-done | bytes 32800 | tf_op jit(solution)/shard_map/ppermute | solution.py:70
  9.4 2.9 %collective-permute-done.2 = bf16[1,8,2048]{2,1,0:T(8,128)(2,1)S(1)} collective-permute-done((bf16[1,8,2048]{2,1,0:T(8,128)(2,1)}, bf16[1,8,2048]{2,1,0:T(8,128)(2,1)S(1)}, u32[]{:S(2)}, u32[]{:S(2)}) %collective-permute-start.2) | collective-permute-done | bytes 32800 | tf_op jit(solution)/shard_map/ppermute | solution.py:70
  12.3 0.8 pad_maximum_fusion.after.refs_0_
  13.0 1.6 %collective-permute-start.3 = (bf16[4,8,2048]{2,1,0:T(8,128)(2,1)S(1)}, bf16[4,8,2048]{2,1,0:T(8,128)(2,1)S(1)}, u32[]{:S(2)}, u32[]{:S(2)}) collective-permute-start(bf16[4,8,2048]{2,1,0:T(8,128)(2,1)S(1)} %pad_maximum_fusion.after.refs_0_), channel_id=1, source_target_pairs={{0,2},{1,3},{2,0},{3,1},{4,6},{5,7},{6,4},{7,5},{8,10},{9,11},{10,... | collective-permute-start | bytes 393224 | tf_op jit(solution)/shard_map/ppermute | solution.py:70
  14.6 1.5 %collective-permute-start.4 = (bf16[4,8,2048]{2,1,0:T(8,128)(2,1)S(1)}, bf16[4,8,2048]{2,1,0:T(8,128)(2,1)S(1)}, u32[]{:S(2)}, u32[]{:S(2)}) collective-permute-start(bf16[4,8,2048]{2,1,0:T(8,128)(2,1)S(1)} %pad_maximum_fusion.after.refs_0_), channel_id=1, source_target_pairs={{0,4},{1,5},{2,6},{3,7},{4,0},{5,1},{6,2},{7,3},{8,12},{9,13},{10,... | collective-permute-start | bytes 393224 | tf_op jit(solution)/shard_map/ppermute | solution.py:70
  16.1 0.5 collective-permute-start.5
  16.7 4.3 %shard_map.230 = (bf16[2048,256]{1,0:T(8,128)(2,1)S(1)}, f32[1,2048]{1,0:T(1,128)S(1)}, f32[16,1024,128]{2,1,0:T(8,128)S(1)}, bf16[16,1024,128]{2,1,0:T(8,128)(2,1)S(1)}) custom-call(bf16[4,8,2048]{2,1,0:T(8,128)(2,1)S(1)} %pad_maximum_fusion.after.refs_0_, bf16[64,2048]{1,0:T(8,128)(2,1)} %bitcast.73, bf16[64,2048]{1,0:T(8,128)(2,1)} %bitcast.74, ...), custom_call_target="tpu_custom_call" | custom-call | tf_op jit(solution)/shard_map/pallas_call | solution.py:35
  21.1 0.9 collective-permute-done.5.refs_3_
  22.0 0.8 shard_map.231.x_ref.own
  22.8 0.3 shard_map.232.own
  23.1 1.6 %collective-permute-done.6.x_ref.other = bf16[16,8,2048]{2,1,0:T(8,128)(2,1)S(1)} collective-permute-done((bf16[16,8,2048]{2,1,0:T(8,128)(2,1)S(1)}, bf16[16,8,2048]{2,1,0:T(8,128)(2,1)S(1)}, u32[]{:S(2)}, u32[]{:S(2)}) %collective-permute-start.6) | collective-permute-done | bytes 524320 | tf_op jit(solution)/shard_map/ppermute | solution.py:70
  24.7 0.9 shard_map.233
  25.6 0.7 collective-permute-start.7
  26.3 1.5 %collective-permute-start.8 = (bf16[4,2,8,256]{3,2,1,0:T(8,128)(2,1)S(1)}, bf16[4,2,8,256]{3,2,1,0:T(8,128)(2,1)S(1)}, u32[]{:S(2)}, u32[]{:S(2)}) collective-permute-start(bf16[4,2,8,256]{3,2,1,0:T(8,128)(2,1)S(1)} %get-tuple-element.36), channel_id=1, source_target_pairs={{0,4},{1,5},{2,6},{3,7},{4,0},{5,1},{6,2},{7,3},{8,12},{9,13},{10,... | collective-permute-start | bytes 98312 | tf_op jit(solution)/shard_map/ppermute | solution.py:70
  27.8 1.3 %collective-permute-start.9 = (bf16[4,2,8,256]{3,2,1,0:T(8,128)(2,1)S(1)}, bf16[4,2,8,256]{3,2,1,0:T(8,128)(2,1)S(1)}, u32[]{:S(2)}, u32[]{:S(2)}) collective-permute-start(bf16[4,2,8,256]{3,2,1,0:T(8,128)(2,1)S(1)} %get-tuple-element.37), channel_id=1, source_target_pairs={{0,6},{1,7},{2,4},{3,5},{4,2},{5,3},{6,0},{7,1},{8,14},{9,15},{10,... | collective-permute-start | bytes 98312 | tf_op jit(solution)/shard_map/ppermute | solution.py:70
  29.1 0.4 collective-permute-done.7
  29.6 0.6 collective-permute-done.8
  30.2 2.4 %collective-permute-done.9 = bf16[4,2,8,256]{3,2,1,0:T(8,128)(2,1)S(1)} collective-permute-done((bf16[4,2,8,256]{3,2,1,0:T(8,128)(2,1)S(1)}, bf16[4,2,8,256]{3,2,1,0:T(8,128)(2,1)S(1)}, u32[]{:S(2)}, u32[]{:S(2)}) %collective-permute-start.9) | collective-permute-done | bytes 32800 | tf_op jit(solution)/shard_map/ppermute | solution.py:70
  32.7 0.9 collective-permute-start.11
  33.6 3.5 %collective-permute-start.12 = (bf16[4,2,8,256]{3,2,1,0:T(8,128)(2,1)S(1)}, bf16[4,2,8,256]{3,2,1,0:T(8,128)(2,1)S(1)}, u32[]{:S(2)}, u32[]{:S(2)}) collective-permute-start(bf16[4,2,8,256]{3,2,1,0:T(8,128)(2,1)S(1)} %bitcast.69), channel_id=1, source_target_pairs={{0,24},{1,25},{2,26},{3,27},{4,28},{5,29},{6,30},{7,31},{8,16},{9,... | collective-permute-start | bytes 98312 | tf_op jit(solution)/shard_map/ppermute | solution.py:70
  37.1 0.8 shard_map.235
  37.9 1.4 %collective-permute-done.12.refs_3_ = bf16[4,2,8,256]{3,2,1,0:T(8,128)(2,1)S(1)} collective-permute-done((bf16[4,2,8,256]{3,2,1,0:T(8,128)(2,1)S(1)}, bf16[4,2,8,256]{3,2,1,0:T(8,128)(2,1)S(1)}, u32[]{:S(2)}, u32[]{:S(2)}) %collective-permute-start.12) | collective-permute-done | bytes 32800 | tf_op jit(solution)/shard_map/ppermute | solution.py:70
  39.4 5.6 %shard_map.236 = (bf16[16,1024]{1,0:T(8,128)(2,1)S(1)}, f32[16,8,128,128]{3,2,1,0:T(8,128)}) custom-call(s32[2]{0:T(128)S(1)} %pad_add_fusion.where, bf16[4,2,8,256]{3,2,1,0:T(8,128)(2,1)S(1)} %bitcast.50, bf16[4,2,8,256]{3,2,1,0:T(8,128)(2,1)S(1)} %collective-permute-done.10.refs_1_, bf16[4,2,8,256]{3,2,1,0:T(8,128)(2,1)S(1)} %collective-permute-done.11.refs_2_, ...), custom_call_target="tpu_custom_call" | custom-call | tf_op jit(solution)/shard_map/pallas_call | solution.py:35
  45.1 0.3 collective-permute-start.13
  45.4 3.8 %collective-permute-start.14 = (bf16[1,16,1024]{2,1,0:T(8,128)(2,1)S(1)}, bf16[1,16,1024]{2,1,0:T(8,128)(2,1)S(1)}, u32[]{:S(2)}, u32[]{:S(2)}) collective-permute-start(bf16[1,16,1024]{2,1,0:T(8,128)(2,1)S(1)} %bitcast.58), channel_id=1, source_target_pairs={{0,16},{1,17},{2,18},{3,19},{4,20},{5,21},{6,22},{7,23},{8,24},{9,... | collective-permute-start | bytes 98312 | tf_op jit(solution)/shard_map/ppermute | solution.py:70
  49.2 0.3 collective-permute-start.15
  49.5 1.6 %collective-permute-done.14 = bf16[1,16,1024]{2,1,0:T(8,128)(2,1)S(1)} collective-permute-done((bf16[1,16,1024]{2,1,0:T(8,128)(2,1)S(1)}, bf16[1,16,1024]{2,1,0:T(8,128)(2,1)S(1)}, u32[]{:S(2)}, u32[]{:S(2)}) %collective-permute-start.14) | collective-permute-done | bytes 32800 | tf_op jit(solution)/shard_map/ppermute | solution.py:70
  51.1 3.8 %collective-permute-done.15 = bf16[1,16,1024]{2,1,0:T(8,128)(2,1)S(1)} collective-permute-done((bf16[1,16,1024]{2,1,0:T(8,128)(2,1)S(1)}, bf16[1,16,1024]{2,1,0:T(8,128)(2,1)S(1)}, u32[]{:S(2)}, u32[]{:S(2)}) %collective-permute-start.15) | collective-permute-done | bytes 32800 | tf_op jit(solution)/shard_map/ppermute | solution.py:70
  54.9 0.7 collective-permute-start.16
  55.6 1.2 %collective-permute-start.17 = (bf16[4,16,1024]{2,1,0:T(8,128)(2,1)S(1)}, bf16[4,16,1024]{2,1,0:T(8,128)(2,1)S(1)}, u32[]{:S(2)}, u32[]{:S(2)}) collective-permute-start(bf16[4,16,1024]{2,1,0:T(8,128)(2,1)S(1)} %pad_maximum_fusion.1.refs_0_), channel_id=1, source_target_pairs={{0,4},{1,5},{2,6},{3,7},{4,0},{5,1},{6,2},{7,3},{8,12},{9,13},{10,... | collective-permute-start | bytes 393224 | tf_op jit(solution)/shard_map/ppermute | solution.py:70
  56.9 1.6 %collective-permute-start.18 = (bf16[4,16,1024]{2,1,0:T(8,128)(2,1)S(1)}, bf16[4,16,1024]{2,1,0:T(8,128)(2,1)S(1)}, u32[]{:S(2)}, u32[]{:S(2)}) collective-permute-start(bf16[4,16,1024]{2,1,0:T(8,128)(2,1)S(1)} %pad_maximum_fusion.1.refs_0_), channel_id=1, source_target_pairs={{0,6},{1,7},{2,4},{3,5},{4,2},{5,3},{6,0},{7,1},{8,14},{9,15},{10,... | collective-permute-start | bytes 393224 | tf_op jit(solution)/shard_map/ppermute | solution.py:70
  58.5 1.5 %collective-permute-done.16.refs_1_ = bf16[4,16,1024]{2,1,0:T(8,128)(2,1)S(1)} collective-permute-done((bf16[4,16,1024]{2,1,0:T(8,128)(2,1)S(1)}, bf16[4,16,1024]{2,1,0:T(8,128)(2,1)S(1)}, u32[]{:S(2)}, u32[]{:S(2)}) %collective-permute-start.16) | collective-permute-done | bytes 131104 | tf_op jit(solution)/shard_map/ppermute | solution.py:70
  60.0 0.7 collective-permute-done.17.refs_2_
  60.6 2.1 %collective-permute-done.18.refs_3_ = bf16[4,16,1024]{2,1,0:T(8,128)(2,1)S(1)} collective-permute-done((bf16[4,16,1024]{2,1,0:T(8,128)(2,1)S(1)}, bf16[4,16,1024]{2,1,0:T(8,128)(2,1)S(1)}, u32[]{:S(2)}, u32[]{:S(2)}) %collective-permute-start.18) | collective-permute-done | bytes 131104 | tf_op jit(solution)/shard_map/ppermute | solution.py:70
  62.7 0.8 shard_map.237
  63.7 1.2 %collective-permute-done.19.other = bf16[16,8,128]{2,1,0:T(8,128)(2,1)S(1)} collective-permute-done((bf16[16,8,128]{2,1,0:T(8,128)(2,1)S(1)}, bf16[16,8,128]{2,1,0:T(8,128)(2,1)S(1)}, u32[]{:S(2)}, u32[]{:S(2)}) %collective-permute-start.19) | collective-permute-done | bytes 32800 | tf_op jit(solution)/shard_map/ppermute | solution.py:70
  65.0 0.9 collective-permute-start.21
  65.9 3.5 %collective-permute-start.22 = (bf16[1,128,128]{2,1,0:T(8,128)(2,1)S(1)}, bf16[1,128,128]{2,1,0:T(8,128)(2,1)S(1)}, u32[]{:S(2)}, u32[]{:S(2)}) collective-permute-start(bf16[1,128,128]{2,1,0:T(8,128)(2,1)S(1)} %bitcast.48), channel_id=1, source_target_pairs={{0,24},{1,25},{2,26},{3,27},{4,28},{5,29},{6,30},{7,31},{8,16},{9,... | collective-permute-start | bytes 98312 | tf_op jit(solution)/shard_map/ppermute | solution.py:70
  69.3 0.5 collective-permute-done.21
  69.8 1.7 %collective-permute-done.22 = bf16[1,128,128]{2,1,0:T(8,128)(2,1)S(1)} collective-permute-done((bf16[1,128,128]{2,1,0:T(8,128)(2,1)S(1)}, bf16[1,128,128]{2,1,0:T(8,128)(2,1)S(1)}, u32[]{:S(2)}, u32[]{:S(2)}) %collective-permute-start.22) | collective-permute-done | bytes 32800 | tf_op jit(solution)/shard_map/ppermute | solution.py:70
  71.6 0.7 collective-permute-start.23
  72.3 1.5 %collective-permute-start.24 = (bf16[4,128,128]{2,1,0:T(8,128)(2,1)S(1)}, bf16[4,128,128]{2,1,0:T(8,128)(2,1)S(1)}, u32[]{:S(2)}, u32[]{:S(2)}) collective-permute-start(bf16[4,128,128]{2,1,0:T(8,128)(2,1)S(1)} %pad_maximum_fusion.2.refs_4_), channel_id=1, source_target_pairs={{0,4},{1,5},{2,6},{3,7},{4,0},{5,1},{6,2},{7,3},{8,12},{9,13},{10,... | collective-permute-start | bytes 393224 | tf_op jit(solution)/shard_map/ppermute | solution.py:70
  73.8 1.3 %collective-permute-start.25 = (bf16[4,128,128]{2,1,0:T(8,128)(2,1)S(1)}, bf16[4,128,128]{2,1,0:T(8,128)(2,1)S(1)}, u32[]{:S(2)}, u32[]{:S(2)}) collective-permute-start(bf16[4,128,128]{2,1,0:T(8,128)(2,1)S(1)} %pad_maximum_fusion.2.refs_4_), channel_id=1, source_target_pairs={{0,6},{1,7},{2,4},{3,5},{4,2},{5,3},{6,0},{7,1},{8,14},{9,15},{10,... | collective-permute-start | bytes 393224 | tf_op jit(solution)/shard_map/ppermute | solution.py:70
  75.2 2.3 %collective-permute-done.23.refs_5_ = bf16[4,128,128]{2,1,0:T(8,128)(2,1)S(1)} collective-permute-done((bf16[4,128,128]{2,1,0:T(8,128)(2,1)S(1)}, bf16[4,128,128]{2,1,0:T(8,128)(2,1)S(1)}, u32[]{:S(2)}, u32[]{:S(2)}) %collective-permute-start.23) | collective-permute-done | bytes 131104 | tf_op jit(solution)/shard_map/ppermute | solution.py:70
  77.4 2.5 %collective-permute-done.24.refs_6_ = bf16[4,128,128]{2,1,0:T(8,128)(2,1)S(1)} collective-permute-done((bf16[4,128,128]{2,1,0:T(8,128)(2,1)S(1)}, bf16[4,128,128]{2,1,0:T(8,128)(2,1)S(1)}, u32[]{:S(2)}, u32[]{:S(2)}) %collective-permute-start.24) | collective-permute-done | bytes 131104 | tf_op jit(solution)/shard_map/ppermute | solution.py:70
  79.9 1.1 shard_map.239
  81.1 1.9 %collective-permute-done.26.rows_in = bf16[128,2048]{1,0:T(8,128)(2,1)S(1)} collective-permute-done((bf16[128,2048]{1,0:T(8,128)(2,1)S(1)}, bf16[128,2048]{1,0:T(8,128)(2,1)S(1)}, u32[]{:S(2)}, u32[]{:S(2)}) %collective-permute-start.26) | collective-permute-done | bytes 524320 | tf_op jit(solution)/shard_map/ppermute | solution.py:70
  83.0 1.6 %shard_map.241 = bf16[128,2048]{1,0:T(8,128)(2,1)S(1)} custom-call(bf16[128,2048]{1,0:T(8,128)(2,1)S(1)} %collective-permute-done.26.rows_in, f32[128,1]{1,0:T(8,128)S(1)} %get-tuple-element.52.route, bf16[1,2048]{1,0:T(2,128)(2,1)S(1)} %broadcast_in_dim.35.mix, bf16[2048,128]{1,0:T(8,128)(2,1)S(1)} %copy-done.3, bf16[2048,128]{1,0:T(8,128)(2,1)S(1)} %copy-done.4, ...), custom_call_target="tpu_custom_call" | custom-call | tf_op jit(solution)/shard_map/pallas_call | solution.py:35
  84.6 0.2 collective-permute-start.27
  84.8 1.6 %shard_map.240.own = f32[128,2048]{1,0:T(8,128)S(1)} custom-call(bf16[128,2048]{1,0:T(8,128)(2,1)S(1)} %get-tuple-element.50.rows_in, f32[128,1]{1,0:T(8,128)S(1)} %get-tuple-element.51.route, bf16[1,2048]{1,0:T(2,128)(2,1)S(1)} %broadcast_in_dim.35.mix, bf16[2048,128]{1,0:T(8,128)(2,1)S(1)} %copy-done.3, bf16[2048,128]{1,0:T(8,128)(2,1)S(1)} %copy-done.4, ...), custom_call_target="tpu_custom_call" | custom-call | tf_op jit(solution)/shard_map/pallas_call | solution.py:35
  86.6 0.6 shard_map.242
  87.2 0.8 collective-permute-start.28
  88.0 1.4 %collective-permute-start.29 = (bf16[4,8,2048]{2,1,0:T(8,128)(2,1)S(1)}, bf16[4,8,2048]{2,1,0:T(8,128)(2,1)S(1)}, u32[]{:S(2)}, u32[]{:S(2)}) collective-permute-start(bf16[4,8,2048]{2,1,0:T(8,128)(2,1)S(1)} %get-tuple-element.55), channel_id=1, source_target_pairs={{0,4},{1,5},{2,6},{3,7},{4,0},{5,1},{6,2},{7,3},{8,12},{9,13},{10,... | collective-permute-start | bytes 393224 | tf_op jit(solution)/shard_map/ppermute | solution.py:70
  89.5 1.3 %collective-permute-start.30 = (bf16[4,8,2048]{2,1,0:T(8,128)(2,1)S(1)}, bf16[4,8,2048]{2,1,0:T(8,128)(2,1)S(1)}, u32[]{:S(2)}, u32[]{:S(2)}) collective-permute-start(bf16[4,8,2048]{2,1,0:T(8,128)(2,1)S(1)} %get-tuple-element.56), channel_id=1, source_target_pairs={{0,6},{1,7},{2,4},{3,5},{4,2},{5,3},{6,0},{7,1},{8,14},{9,15},{10,... | collective-permute-start | bytes 393224 | tf_op jit(solution)/shard_map/ppermute | solution.py:70
  90.8 2.9 %collective-permute-done.28.refs_1_ = bf16[4,8,2048]{2,1,0:T(8,128)(2,1)S(1)} collective-permute-done((bf16[4,8,2048]{2,1,0:T(8,128)(2,1)S(1)}, bf16[4,8,2048]{2,1,0:T(8,128)(2,1)S(1)}, u32[]{:S(2)}, u32[]{:S(2)}) %collective-permute-start.28) | collective-permute-done | bytes 131104 | tf_op jit(solution)/shard_map/ppermute | solution.py:70
  93.7 2.5 %collective-permute-done.29.refs_2_ = bf16[4,8,2048]{2,1,0:T(8,128)(2,1)S(1)} collective-permute-done((bf16[4,8,2048]{2,1,0:T(8,128)(2,1)S(1)}, bf16[4,8,2048]{2,1,0:T(8,128)(2,1)S(1)}, u32[]{:S(2)}, u32[]{:S(2)}) %collective-permute-start.29) | collective-permute-done | bytes 131104 | tf_op jit(solution)/shard_map/ppermute | solution.py:70
  96.3 0.3 collective-permute-start.31
  96.5 3.5 %collective-permute-start.32 = (bf16[8,2048]{1,0:T(8,128)(2,1)S(1)}, bf16[8,2048]{1,0:T(8,128)(2,1)S(1)}, u32[]{:S(2)}, u32[]{:S(2)}) collective-permute-start(bf16[8,2048]{1,0:T(8,128)(2,1)S(1)} %get-tuple-element.59), channel_id=1, source_target_pairs={{0,16},{1,17},{2,18},{3,19},{4,20},{5,21},{6,22},{7,23},{8,24},{9,... | collective-permute-start | bytes 98312 | tf_op jit(solution)/shard_map/ppermute | solution.py:70
  100.0 0.7 collective-permute-start.33
  100.7 1.2 %collective-permute-done.32.refs_2_ = bf16[8,2048]{1,0:T(8,128)(2,1)S(1)} collective-permute-done((bf16[8,2048]{1,0:T(8,128)(2,1)S(1)}, bf16[8,2048]{1,0:T(8,128)(2,1)S(1)}, u32[]{:S(2)}, u32[]{:S(2)}) %collective-permute-start.32) | collective-permute-done | bytes 32800 | tf_op jit(solution)/shard_map/ppermute | solution.py:70
  101.9 3.8 %collective-permute-done.33.refs_3_ = bf16[8,2048]{1,0:T(8,128)(2,1)S(1)} collective-permute-done((bf16[8,2048]{1,0:T(8,128)(2,1)S(1)}, bf16[8,2048]{1,0:T(8,128)(2,1)S(1)}, u32[]{:S(2)}, u32[]{:S(2)}) %collective-permute-start.33) | collective-permute-done | bytes 32800 | tf_op jit(solution)/shard_map/ppermute | solution.py:70
  105.8 0.6 shard_map.244
  (56 shorter events, 0.9 us)
Async XLA Ops:
  0.6 5.7 %collective-permute-start = (bf16[1,8,2048]{2,1,0:T(8,128)(2,1)}, bf16[1,8,2048]{2,1,0:T(8,128)(2,1)S(1)}, u32[]{:S(2)}, u32[]{:S(2)}) collective-permute-start(bf16[1,8,2048]{2,1,0:T(8,128)(2,1)} %bitcast.77), channel_id=1, source_target_pairs={{0,8},{1,9},{2,10},{3,11},{4,12},{5,13},{6,14},{7,15},{8,0},{9,1},... | collective-permute-start | bytes 98312 | tf_op jit(solution)/shard_map/ppermute | solution.py:70
  3.7 5.6 %collective-permute-start.1 = (bf16[1,8,2048]{2,1,0:T(8,128)(2,1)}, bf16[1,8,2048]{2,1,0:T(8,128)(2,1)S(1)}, u32[]{:S(2)}, u32[]{:S(2)}) collective-permute-start(bf16[1,8,2048]{2,1,0:T(8,128)(2,1)} %bitcast.78), channel_id=1, source_target_pairs={{0,16},{1,17},{2,18},{3,19},{4,20},{5,21},{6,22},{7,23},{8,24},{9,... | collective-permute-start | bytes 98312 | tf_op jit(solution)/shard_map/ppermute | solution.py:70
  6.3 5.9 %collective-permute-start.2 = (bf16[1,8,2048]{2,1,0:T(8,128)(2,1)}, bf16[1,8,2048]{2,1,0:T(8,128)(2,1)S(1)}, u32[]{:S(2)}, u32[]{:S(2)}) collective-permute-start(bf16[1,8,2048]{2,1,0:T(8,128)(2,1)} %bitcast.79), channel_id=1, source_target_pairs={{0,24},{1,25},{2,26},{3,27},{4,28},{5,29},{6,30},{7,31},{8,16},{9,... | collective-permute-start | bytes 98312 | tf_op jit(solution)/shard_map/ppermute | solution.py:70
  13.0 8.1 %collective-permute-start.3 = (bf16[4,8,2048]{2,1,0:T(8,128)(2,1)S(1)}, bf16[4,8,2048]{2,1,0:T(8,128)(2,1)S(1)}, u32[]{:S(2)}, u32[]{:S(2)}) collective-permute-start(bf16[4,8,2048]{2,1,0:T(8,128)(2,1)S(1)} %pad_maximum_fusion.after.refs_0_), channel_id=1, source_target_pairs={{0,2},{1,3},{2,0},{3,1},{4,6},{5,7},{6,4},{7,5},{8,10},{9,11},{10,... | collective-permute-start | bytes 393224 | tf_op jit(solution)/shard_map/ppermute | solution.py:70
  14.6 6.5 %collective-permute-start.4 = (bf16[4,8,2048]{2,1,0:T(8,128)(2,1)S(1)}, bf16[4,8,2048]{2,1,0:T(8,128)(2,1)S(1)}, u32[]{:S(2)}, u32[]{:S(2)}) collective-permute-start(bf16[4,8,2048]{2,1,0:T(8,128)(2,1)S(1)} %pad_maximum_fusion.after.refs_0_), channel_id=1, source_target_pairs={{0,4},{1,5},{2,6},{3,7},{4,0},{5,1},{6,2},{7,3},{8,12},{9,13},{10,... | collective-permute-start | bytes 393224 | tf_op jit(solution)/shard_map/ppermute | solution.py:70
  16.1 5.9 %collective-permute-start.5 = (bf16[4,8,2048]{2,1,0:T(8,128)(2,1)S(1)}, bf16[4,8,2048]{2,1,0:T(8,128)(2,1)S(1)}, u32[]{:S(2)}, u32[]{:S(2)}) collective-permute-start(bf16[4,8,2048]{2,1,0:T(8,128)(2,1)S(1)} %pad_maximum_fusion.after.refs_0_), channel_id=1, source_target_pairs={{0,6},{1,7},{2,4},{3,5},{4,2},{5,3},{6,0},{7,1},{8,14},{9,15},{10,... | collective-permute-start | bytes 393224 | tf_op jit(solution)/shard_map/ppermute | solution.py:70
  21.0 16.1 %copy-start.7 = (bf16[2048,8]{0,1:T(8,128)(2,1)S(1)}, bf16[2048,8]{0,1:T(8,128)(2,1)}, u32[]{:S(2)}) copy-start(bf16[2048,8]{0,1:T(8,128)(2,1)} %param.29) | copy-start | bytes 98308
  21.0 16.1 %copy-start.8 = (bf16[2048,8]{0,1:T(8,128)(2,1)S(1)}, bf16[2048,8]{0,1:T(8,128)(2,1)}, u32[]{:S(2)}) copy-start(bf16[2048,8]{0,1:T(8,128)(2,1)} %param.30) | copy-start | bytes 98308
  21.0 16.1 %copy-start.10 = (s32[256,4]{0,1:T(4,128)S(1)}, s32[256,4]{0,1:T(4,128)}, u32[]{:S(2)}) copy-start(s32[256,4]{0,1:T(4,128)} %param.44) | copy-start | bytes 12292
  21.0 16.1 %copy-start.11 = (f32[256,4]{0,1:T(4,128)S(1)}, f32[256,4]{0,1:T(4,128)}, u32[]{:S(2)}) copy-start(f32[256,4]{0,1:T(4,128)} %param.45) | copy-start | bytes 12292
  21.1 16.0 %copy-start.12 = (f32[8]{0:T(128)S(1)}, f32[8]{0:T(128)}, u32[]{:S(2)}) copy-start(f32[8]{0:T(128)} %param.31) | copy-start | bytes 100
  21.1 16.0 %copy-start.13 = (f32[8]{0:T(128)S(1)}, f32[8]{0:T(128)}, u32[]{:S(2)}) copy-start(f32[8]{0:T(128)} %param.32) | copy-start | bytes 100
  21.1 18.3 %copy-start.14 = (f32[128]{0:T(128)S(1)}, f32[128]{0:T(128)}, u32[]{:S(2)}) copy-start(f32[128]{0:T(128)} %param.33) | copy-start | bytes 1540
  22.7 2.0 %collective-permute-start.6 = (bf16[16,8,2048]{2,1,0:T(8,128)(2,1)S(1)}, bf16[16,8,2048]{2,1,0:T(8,128)(2,1)S(1)}, u32[]{:S(2)}, u32[]{:S(2)}) collective-permute-start(bf16[16,8,2048]{2,1,0:T(8,128)(2,1)S(1)} %shard_map.231.x_ref.own), channel_id=1, source_target_pairs={{0,1},{1,0},{2,3},{3,2},{4,5},{5,4},{6,7},{7,6},{8,9},{9,8},{10,11... | collective-permute-start | bytes 1572872 | tf_op jit(solution)/shard_map/ppermute | solution.py:70
  25.6 4.0 %collective-permute-start.7 = (bf16[4,2,8,256]{3,2,1,0:T(8,128)(2,1)S(1)}, bf16[4,2,8,256]{3,2,1,0:T(8,128)(2,1)S(1)}, u32[]{:S(2)}, u32[]{:S(2)}) collective-permute-start(bf16[4,2,8,256]{3,2,1,0:T(8,128)(2,1)S(1)} %get-tuple-element.35), channel_id=1, source_target_pairs={{0,2},{1,3},{2,0},{3,1},{4,6},{5,7},{6,4},{7,5},{8,10},{9,11},{10,... | collective-permute-start | bytes 98312 | tf_op jit(solution)/shard_map/ppermute | solution.py:70
  26.3 3.9 %collective-permute-start.8 = (bf16[4,2,8,256]{3,2,1,0:T(8,128)(2,1)S(1)}, bf16[4,2,8,256]{3,2,1,0:T(8,128)(2,1)S(1)}, u32[]{:S(2)}, u32[]{:S(2)}) collective-permute-start(bf16[4,2,8,256]{3,2,1,0:T(8,128)(2,1)S(1)} %get-tuple-element.36), channel_id=1, source_target_pairs={{0,4},{1,5},{2,6},{3,7},{4,0},{5,1},{6,2},{7,3},{8,12},{9,13},{10,... | collective-permute-start | bytes 98312 | tf_op jit(solution)/shard_map/ppermute | solution.py:70
  27.8 4.8 %collective-permute-start.9 = (bf16[4,2,8,256]{3,2,1,0:T(8,128)(2,1)S(1)}, bf16[4,2,8,256]{3,2,1,0:T(8,128)(2,1)S(1)}, u32[]{:S(2)}, u32[]{:S(2)}) collective-permute-start(bf16[4,2,8,256]{3,2,1,0:T(8,128)(2,1)S(1)} %get-tuple-element.37), channel_id=1, source_target_pairs={{0,6},{1,7},{2,4},{3,5},{4,2},{5,3},{6,0},{7,1},{8,14},{9,15},{10,... | collective-permute-start | bytes 98312 | tf_op jit(solution)/shard_map/ppermute | solution.py:70
  32.6 5.3 %collective-permute-start.10 = (bf16[4,2,8,256]{3,2,1,0:T(8,128)(2,1)S(1)}, bf16[4,2,8,256]{3,2,1,0:T(8,128)(2,1)S(1)}, u32[]{:S(2)}, u32[]{:S(2)}) collective-permute-start(bf16[4,2,8,256]{3,2,1,0:T(8,128)(2,1)S(1)} %bitcast.71), channel_id=1, source_target_pairs={{0,8},{1,9},{2,10},{3,11},{4,12},{5,13},{6,14},{7,15},{8,0},{9,1},... | collective-permute-start | bytes 98312 | tf_op jit(solution)/shard_map/ppermute | solution.py:70
  32.7 5.2 %collective-permute-start.11 = (bf16[4,2,8,256]{3,2,1,0:T(8,128)(2,1)S(1)}, bf16[4,2,8,256]{3,2,1,0:T(8,128)(2,1)S(1)}, u32[]{:S(2)}, u32[]{:S(2)}) collective-permute-start(bf16[4,2,8,256]{3,2,1,0:T(8,128)(2,1)S(1)} %bitcast.70), channel_id=1, source_target_pairs={{0,16},{1,17},{2,18},{3,19},{4,20},{5,21},{6,22},{7,23},{8,24},{9,... | collective-permute-start | bytes 98312 | tf_op jit(solution)/shard_map/ppermute | solution.py:70
  33.6 5.7 %collective-permute-start.12 = (bf16[4,2,8,256]{3,2,1,0:T(8,128)(2,1)S(1)}, bf16[4,2,8,256]{3,2,1,0:T(8,128)(2,1)S(1)}, u32[]{:S(2)}, u32[]{:S(2)}) collective-permute-start(bf16[4,2,8,256]{3,2,1,0:T(8,128)(2,1)S(1)} %bitcast.69), channel_id=1, source_target_pairs={{0,24},{1,25},{2,26},{3,27},{4,28},{5,29},{6,30},{7,31},{8,16},{9,... | collective-permute-start | bytes 98312 | tf_op jit(solution)/shard_map/ppermute | solution.py:70
  39.3 23.4 %copy-start.6 = (bf16[1024,128]{1,0:T(8,128)(2,1)S(1)}, bf16[1024,128]{1,0:T(8,128)(2,1)}, u32[]{:S(2)}) copy-start(bf16[1024,128]{1,0:T(8,128)(2,1)} %refs_4_.1) | copy-start | bytes 786436
  39.3 40.6 %copy-start.9 = (f32[2048]{0:T(1024)S(1)}, f32[2048]{0:T(1024)}, u32[]{:S(2)}) copy-start(f32[2048]{0:T(1024)} %param.36) | copy-start | bytes 24580
  39.3 41.7 %copy-start.15 = (bf16[2048]{0:T(1024)(128)(2,1)S(1)}, bf16[2048]{0:T(1024)(128)(2,1)}, u32[]{:S(2)}) copy-start(bf16[2048]{0:T(1024)(128)(2,1)} %param.37) | copy-start | bytes 12292
  39.3 43.6 %copy-start = (bf16[1,2048,512]{2,1,0:T(8,128)(2,1)S(1)}, bf16[1,2048,512]{2,1,0:T(8,128)(2,1)}, u32[]{:S(2)}) copy-start(bf16[1,2048,512]{2,1,0:T(8,128)(2,1)} %param.41) | copy-start | bytes 6291460
  39.4 43.6 %copy-start.1 = (bf16[1,2048,512]{2,1,0:T(8,128)(2,1)S(1)}, bf16[1,2048,512]{2,1,0:T(8,128)(2,1)}, u32[]{:S(2)}) copy-start(bf16[1,2048,512]{2,1,0:T(8,128)(2,1)} %param.42) | copy-start | bytes 6291460
  39.4 43.6 %copy-start.2 = (bf16[1,512,2048]{2,1,0:T(8,128)(2,1)S(1)}, bf16[1,512,2048]{2,1,0:T(8,128)(2,1)}, u32[]{:S(2)}) copy-start(bf16[1,512,2048]{2,1,0:T(8,128)(2,1)} %param.43) | copy-start | bytes 6291460
  39.4 43.6 %copy-start.3 = (bf16[2048,128]{1,0:T(8,128)(2,1)S(1)}, bf16[2048,128]{1,0:T(8,128)(2,1)}, u32[]{:S(2)}) copy-start(bf16[2048,128]{1,0:T(8,128)(2,1)} %d_gate.3) | copy-start | bytes 1572868
  39.4 43.6 %copy-start.4 = (bf16[2048,128]{1,0:T(8,128)(2,1)S(1)}, bf16[2048,128]{1,0:T(8,128)(2,1)}, u32[]{:S(2)}) copy-start(bf16[2048,128]{1,0:T(8,128)(2,1)} %d_up.3) | copy-start | bytes 1572868
  39.4 43.6 %copy-start.5 = (bf16[128,2048]{1,0:T(8,128)(2,1)S(1)}, bf16[128,2048]{1,0:T(8,128)(2,1)}, u32[]{:S(2)}) copy-start(bf16[128,2048]{1,0:T(8,128)(2,1)} %d_down.3) | copy-start | bytes 1572868
  45.1 4.5 %collective-permute-start.13 = (bf16[1,16,1024]{2,1,0:T(8,128)(2,1)S(1)}, bf16[1,16,1024]{2,1,0:T(8,128)(2,1)S(1)}, u32[]{:S(2)}, u32[]{:S(2)}) collective-permute-start(bf16[1,16,1024]{2,1,0:T(8,128)(2,1)S(1)} %bitcast.57), channel_id=1, source_target_pairs={{0,8},{1,9},{2,10},{3,11},{4,12},{5,13},{6,14},{7,15},{8,0},{9,1},... | collective-permute-start | bytes 98312 | tf_op jit(solution)/shard_map/ppermute | solution.py:70
  45.4 5.7 %collective-permute-start.14 = (bf16[1,16,1024]{2,1,0:T(8,128)(2,1)S(1)}, bf16[1,16,1024]{2,1,0:T(8,128)(2,1)S(1)}, u32[]{:S(2)}, u32[]{:S(2)}) collective-permute-start(bf16[1,16,1024]{2,1,0:T(8,128)(2,1)S(1)} %bitcast.58), channel_id=1, source_target_pairs={{0,16},{1,17},{2,18},{3,19},{4,20},{5,21},{6,22},{7,23},{8,24},{9,... | collective-permute-start | bytes 98312 | tf_op jit(solution)/shard_map/ppermute | solution.py:70
  49.2 5.7 %collective-permute-start.15 = (bf16[1,16,1024]{2,1,0:T(8,128)(2,1)S(1)}, bf16[1,16,1024]{2,1,0:T(8,128)(2,1)S(1)}, u32[]{:S(2)}, u32[]{:S(2)}) collective-permute-start(bf16[1,16,1024]{2,1,0:T(8,128)(2,1)S(1)} %bitcast.59), channel_id=1, source_target_pairs={{0,24},{1,25},{2,26},{3,27},{4,28},{5,29},{6,30},{7,31},{8,16},{9,... | collective-permute-start | bytes 98312 | tf_op jit(solution)/shard_map/ppermute | solution.py:70
  54.9 5.0 %collective-permute-start.16 = (bf16[4,16,1024]{2,1,0:T(8,128)(2,1)S(1)}, bf16[4,16,1024]{2,1,0:T(8,128)(2,1)S(1)}, u32[]{:S(2)}, u32[]{:S(2)}) collective-permute-start(bf16[4,16,1024]{2,1,0:T(8,128)(2,1)S(1)} %pad_maximum_fusion.1.refs_0_), channel_id=1, source_target_pairs={{0,2},{1,3},{2,0},{3,1},{4,6},{5,7},{6,4},{7,5},{8,10},{9,11},{10,... | collective-permute-start | bytes 393224 | tf_op jit(solution)/shard_map/ppermute | solution.py:70
  55.6 5.0 %collective-permute-start.17 = (bf16[4,16,1024]{2,1,0:T(8,128)(2,1)S(1)}, bf16[4,16,1024]{2,1,0:T(8,128)(2,1)S(1)}, u32[]{:S(2)}, u32[]{:S(2)}) collective-permute-start(bf16[4,16,1024]{2,1,0:T(8,128)(2,1)S(1)} %pad_maximum_fusion.1.refs_0_), channel_id=1, source_target_pairs={{0,4},{1,5},{2,6},{3,7},{4,0},{5,1},{6,2},{7,3},{8,12},{9,13},{10,... | collective-permute-start | bytes 393224 | tf_op jit(solution)/shard_map/ppermute | solution.py:70
  56.9 5.9 %collective-permute-start.18 = (bf16[4,16,1024]{2,1,0:T(8,128)(2,1)S(1)}, bf16[4,16,1024]{2,1,0:T(8,128)(2,1)S(1)}, u32[]{:S(2)}, u32[]{:S(2)}) collective-permute-start(bf16[4,16,1024]{2,1,0:T(8,128)(2,1)S(1)} %pad_maximum_fusion.1.refs_0_), channel_id=1, source_target_pairs={{0,6},{1,7},{2,4},{3,5},{4,2},{5,3},{6,0},{7,1},{8,14},{9,15},{10,... | collective-permute-start | bytes 393224 | tf_op jit(solution)/shard_map/ppermute | solution.py:70
  63.6 1.3 %collective-permute-start.19 = (bf16[16,8,128]{2,1,0:T(8,128)(2,1)S(1)}, bf16[16,8,128]{2,1,0:T(8,128)(2,1)S(1)}, u32[]{:S(2)}, u32[]{:S(2)}) collective-permute-start(bf16[16,8,128]{2,1,0:T(8,128)(2,1)S(1)} %get-tuple-element.48), channel_id=1, source_target_pairs={{0,1},{1,0},{2,3},{3,2},{4,5},{5,4},{6,7},{7,6},{8,9},{9,8},{10,11... | collective-permute-start | bytes 98312 | tf_op jit(solution)/shard_map/ppermute | solution.py:70
  64.9 4.5 %collective-permute-start.20 = (bf16[1,128,128]{2,1,0:T(8,128)(2,1)S(1)}, bf16[1,128,128]{2,1,0:T(8,128)(2,1)S(1)}, u32[]{:S(2)}, u32[]{:S(2)}) collective-permute-start(bf16[1,128,128]{2,1,0:T(8,128)(2,1)S(1)} %bitcast.46), channel_id=1, source_target_pairs={{0,8},{1,9},{2,10},{3,11},{4,12},{5,13},{6,14},{7,15},{8,0},{9,1},... | collective-permute-start | bytes 98312 | tf_op jit(solution)/shard_map/ppermute | solution.py:70
  65.0 4.9 %collective-permute-start.21 = (bf16[1,128,128]{2,1,0:T(8,128)(2,1)S(1)}, bf16[1,128,128]{2,1,0:T(8,128)(2,1)S(1)}, u32[]{:S(2)}, u32[]{:S(2)}) collective-permute-start(bf16[1,128,128]{2,1,0:T(8,128)(2,1)S(1)} %bitcast.47), channel_id=1, source_target_pairs={{0,16},{1,17},{2,18},{3,19},{4,20},{5,21},{6,22},{7,23},{8,24},{9,... | collective-permute-start | bytes 98312 | tf_op jit(solution)/shard_map/ppermute | solution.py:70
  65.9 5.7 %collective-permute-start.22 = (bf16[1,128,128]{2,1,0:T(8,128)(2,1)S(1)}, bf16[1,128,128]{2,1,0:T(8,128)(2,1)S(1)}, u32[]{:S(2)}, u32[]{:S(2)}) collective-permute-start(bf16[1,128,128]{2,1,0:T(8,128)(2,1)S(1)} %bitcast.48), channel_id=1, source_target_pairs={{0,24},{1,25},{2,26},{3,27},{4,28},{5,29},{6,30},{7,31},{8,16},{9,... | collective-permute-start | bytes 98312 | tf_op jit(solution)/shard_map/ppermute | solution.py:70
  71.6 5.8 %collective-permute-start.23 = (bf16[4,128,128]{2,1,0:T(8,128)(2,1)S(1)}, bf16[4,128,128]{2,1,0:T(8,128)(2,1)S(1)}, u32[]{:S(2)}, u32[]{:S(2)}) collective-permute-start(bf16[4,128,128]{2,1,0:T(8,128)(2,1)S(1)} %pad_maximum_fusion.2.refs_4_), channel_id=1, source_target_pairs={{0,2},{1,3},{2,0},{3,1},{4,6},{5,7},{6,4},{7,5},{8,10},{9,11},{10,... | collective-permute-start | bytes 393224 | tf_op jit(solution)/shard_map/ppermute | solution.py:70
  72.3 7.6 %collective-permute-start.24 = (bf16[4,128,128]{2,1,0:T(8,128)(2,1)S(1)}, bf16[4,128,128]{2,1,0:T(8,128)(2,1)S(1)}, u32[]{:S(2)}, u32[]{:S(2)}) collective-permute-start(bf16[4,128,128]{2,1,0:T(8,128)(2,1)S(1)} %pad_maximum_fusion.2.refs_4_), channel_id=1, source_target_pairs={{0,4},{1,5},{2,6},{3,7},{4,0},{5,1},{6,2},{7,3},{8,12},{9,13},{10,... | collective-permute-start | bytes 393224 | tf_op jit(solution)/shard_map/ppermute | solution.py:70
  73.8 6.1 %collective-permute-start.25 = (bf16[4,128,128]{2,1,0:T(8,128)(2,1)S(1)}, bf16[4,128,128]{2,1,0:T(8,128)(2,1)S(1)}, u32[]{:S(2)}, u32[]{:S(2)}) collective-permute-start(bf16[4,128,128]{2,1,0:T(8,128)(2,1)S(1)} %pad_maximum_fusion.2.refs_4_), channel_id=1, source_target_pairs={{0,6},{1,7},{2,4},{3,5},{4,2},{5,3},{6,0},{7,1},{8,14},{9,15},{10,... | collective-permute-start | bytes 393224 | tf_op jit(solution)/shard_map/ppermute | solution.py:70
  81.0 2.0 %collective-permute-start.26 = (bf16[128,2048]{1,0:T(8,128)(2,1)S(1)}, bf16[128,2048]{1,0:T(8,128)(2,1)S(1)}, u32[]{:S(2)}, u32[]{:S(2)}) collective-permute-start(bf16[128,2048]{1,0:T(8,128)(2,1)S(1)} %get-tuple-element.50.rows_in), channel_id=1, source_target_pairs={{0,1},{1,0},{2,3},{3,2},{4,5},{5,4},{6,7},{7,6},{8,9},{9,8},{10,11... | collective-permute-start | bytes 1572872 | tf_op jit(solution)/shard_map/ppermute | solution.py:70
  84.6 2.0 %collective-permute-start.27 = (bf16[128,2048]{1,0:T(8,128)(2,1)S(1)}, bf16[128,2048]{1,0:T(8,128)(2,1)S(1)}, u32[]{:S(2)}, u32[]{:S(2)}) collective-permute-start(bf16[128,2048]{1,0:T(8,128)(2,1)S(1)} %shard_map.241), channel_id=1, source_target_pairs={{0,1},{1,0},{2,3},{3,2},{4,5},{5,4},{6,7},{7,6},{8,9},{9,8},{10,11... | collective-permute-start | bytes 1572872 | tf_op jit(solution)/shard_map/ppermute | solution.py:70
  87.2 6.4 %collective-permute-start.28 = (bf16[4,8,2048]{2,1,0:T(8,128)(2,1)S(1)}, bf16[4,8,2048]{2,1,0:T(8,128)(2,1)S(1)}, u32[]{:S(2)}, u32[]{:S(2)}) collective-permute-start(bf16[4,8,2048]{2,1,0:T(8,128)(2,1)S(1)} %get-tuple-element.54), channel_id=1, source_target_pairs={{0,2},{1,3},{2,0},{3,1},{4,6},{5,7},{6,4},{7,5},{8,10},{9,11},{10,... | collective-permute-start | bytes 393224 | tf_op jit(solution)/shard_map/ppermute | solution.py:70
  88.0 8.2 %collective-permute-start.29 = (bf16[4,8,2048]{2,1,0:T(8,128)(2,1)S(1)}, bf16[4,8,2048]{2,1,0:T(8,128)(2,1)S(1)}, u32[]{:S(2)}, u32[]{:S(2)}) collective-permute-start(bf16[4,8,2048]{2,1,0:T(8,128)(2,1)S(1)} %get-tuple-element.55), channel_id=1, source_target_pairs={{0,4},{1,5},{2,6},{3,7},{4,0},{5,1},{6,2},{7,3},{8,12},{9,13},{10,... | collective-permute-start | bytes 393224 | tf_op jit(solution)/shard_map/ppermute | solution.py:70
  89.5 6.7 %collective-permute-start.30 = (bf16[4,8,2048]{2,1,0:T(8,128)(2,1)S(1)}, bf16[4,8,2048]{2,1,0:T(8,128)(2,1)S(1)}, u32[]{:S(2)}, u32[]{:S(2)}) collective-permute-start(bf16[4,8,2048]{2,1,0:T(8,128)(2,1)S(1)} %get-tuple-element.56), channel_id=1, source_target_pairs={{0,6},{1,7},{2,4},{3,5},{4,2},{5,3},{6,0},{7,1},{8,14},{9,15},{10,... | collective-permute-start | bytes 393224 | tf_op jit(solution)/shard_map/ppermute | solution.py:70
  96.3 4.5 %collective-permute-start.31 = (bf16[8,2048]{1,0:T(8,128)(2,1)S(1)}, bf16[8,2048]{1,0:T(8,128)(2,1)S(1)}, u32[]{:S(2)}, u32[]{:S(2)}) collective-permute-start(bf16[8,2048]{1,0:T(8,128)(2,1)S(1)} %get-tuple-element.58), channel_id=1, source_target_pairs={{0,8},{1,9},{2,10},{3,11},{4,12},{5,13},{6,14},{7,15},{8,0},{9,1},... | collective-permute-start | bytes 98312 | tf_op jit(solution)/shard_map/ppermute | solution.py:70
  96.5 5.4 %collective-permute-start.32 = (bf16[8,2048]{1,0:T(8,128)(2,1)S(1)}, bf16[8,2048]{1,0:T(8,128)(2,1)S(1)}, u32[]{:S(2)}, u32[]{:S(2)}) collective-permute-start(bf16[8,2048]{1,0:T(8,128)(2,1)S(1)} %get-tuple-element.59), channel_id=1, source_target_pairs={{0,16},{1,17},{2,18},{3,19},{4,20},{5,21},{6,22},{7,23},{8,24},{9,... | collective-permute-start | bytes 98312 | tf_op jit(solution)/shard_map/ppermute | solution.py:70
  100.0 5.7 %collective-permute-start.33 = (bf16[8,2048]{1,0:T(8,128)(2,1)S(1)}, bf16[8,2048]{1,0:T(8,128)(2,1)S(1)}, u32[]{:S(2)}, u32[]{:S(2)}) collective-permute-start(bf16[8,2048]{1,0:T(8,128)(2,1)S(1)} %get-tuple-element.60), channel_id=1, source_target_pairs={{0,24},{1,25},{2,26},{3,27},{4,28},{5,29},{6,30},{7,31},{8,16},{9,... | collective-permute-start | bytes 98312 | tf_op jit(solution)/shard_map/ppermute | solution.py:70

commit v4 on v3

--- a/solution.py
+++ b/solution.py
@@ -77,10 +77,13 @@
     return got
 
 
-def gather_xor(piece, digits):
+def gather_xor(piece, digits, near=None):
     cur = piece[None]
     for shift, radix in digits[:-1]:
-        cur = jnp.concatenate(exchange_all([cur] * radix, shift, radix), axis=0)
+        got = exchange_all([cur] * radix, shift, radix)
+        if near is not None:
+            got[0], near = near[None], None
+        cur = jnp.concatenate(got, axis=0)
     shift, radix = digits[-1]
     return exchange_all([cur] * radix, shift, radix)
 
@@ -171,9 +174,13 @@
 
 
 def rates_kernel(
-    where, own, other, wb, wd, rate, bias, ids, chance, beta, retain, route, route_other, column
+    masks, where, own, other, wb, wd, rate, bias, ids, chance, *refs
 ):
+    pieces, (beta, retain, route, route_other, ordered, column) = refs[: len(masks)], refs[len(masks) :]
     me, par = where[0], where[1]
+    for ref, row in zip(pieces, masks):
+        for j, mask in enumerate(row):
+            ordered[me ^ mask] = ref[j]
     for side, ref in ((par, own), (1 - par, other)):
         x = ref[me]
         b = lax.dot_general(x, wb[...], (((1,), (1,)), ((), ())), preferred_element_type=F32)
@@ -211,13 +218,15 @@
 
 
 def state_kernel(heads, came, where, *refs):
-    pieces, (beta, retain, gain, near, short, gated, new_state) = refs[: len(came)], refs[len(came) : len(came) + 7]
-    cols, rows, both, reads, lefts, new, sems = refs[len(came) + 7 :]
+    pieces, (beta, retain, gain, short, gated, k_out, keep_out, change_out) = (
+        refs[: len(came)],
+        refs[len(came) : len(came) + 8],
+    )
+    cols, rows, both, reads = refs[len(came) + 8 :]
     for ref, row in zip(pieces, came):
         for j, mask in enumerate(row):
             cols[where[0] ^ mask] = ref[j].reshape(cols.shape[1:])
-    seqs, size = near.shape[0], near.shape[2]
-    store = lambda i: pltpu.make_async_copy(new.at[i], new_state.at[i], sems.at[i])
+    seqs, size = short.shape[0], short.shape[2]
     count, width = cols.shape[0], cols.shape[2]
     piece = width // (4 * heads)
     for first in range(0, width, size):
@@ -251,11 +260,17 @@
         reads[1, i * heads : (i + 1) * heads, :] = found[heads:]
     keep = rows[5]
     change = rows[4] * (silu(rows[2]) - keep * reads[0])
-    reads[0] = change
+    k_out[...], keep_out[...], change_out[...] = k, keep, change
     read = keep * reads[1] + dots * change
     reads[1] = scale_rows(read, gain[...]) * silu(rows[3])
     for h in range(heads):
         gated[:, h * size : (h + 1) * size] = reads[1, pl.ds(h, seqs, stride=heads), :].astype(BF16)
+
+
+def store_kernel(heads, k_in, keep, change, near, after, new_state, lefts, new, sems):
+    seqs, size = near.shape[0], near.shape[2]
+    store = lambda i: pltpu.make_async_copy(new.at[i], new_state.at[i], sems.at[i])
+    k = k_in[...]
     high = k.astype(BF16).astype(F32)
     low = (k - high).astype(BF16).astype(F32)
     lefts[:, :heads] = high.reshape(seqs, heads, size)
@@ -266,13 +281,13 @@
 
     def one(i, carry):
         at = pl.ds(pl.multiple_of(i * heads, heads), heads)
-        step = reads[0, at, :]
+        step = change[at, :]
         top = step.astype(BF16).astype(F32)
         rest = step - top
         right = jnp.concatenate([top, rest, top, jnp.zeros_like(top)], axis=0)
         right = jnp.concatenate([jnp.where(head_row == h, right, 0.0).astype(BF16) for h in range(heads)], axis=1)
         added = jnp.dot(lefts[i].T.astype(BF16), right, preferred_element_type=F32)
-        rate = rows[5, at, :]
+        rate = keep[at, :]
         for h in range(heads):
             old = near[i, h * size : (h + 1) * size, :]
             new[i, h] = rate[h : h + 1, :] * old + added[:, h * size : (h + 1) * size]
@@ -284,25 +299,39 @@
         store(i).wait()
 
 
-def run_state(came, where, pieces, beta, retain, gain, near, short, shape):
+def run_state(came, where, pieces, beta, retain, gain, short, shape):
     seqs, heads, size = shape[:3]
     count, columns = sum(map(len, came)), pieces[0].shape[-1]
     sds = jax.ShapeDtypeStruct
+    per_head = sds((seqs * heads, size), F32)
     return call(
         functools.partial(state_kernel, heads, came),
-        (sds((seqs, heads * size), BF16), sds(shape, F32)),
-        [where, *pieces, beta, retain, gain, near, short],
-        hbm_out=(1,),
+        (sds((seqs, heads * size), BF16), per_head, per_head, per_head),
+        [where, *pieces, beta, retain, gain, short],
         scratch=[
             VM((count, seqs, columns), BF16),
             VM((6, seqs * heads, size), F32),
             VM((seqs, 2 * heads, heads * size), BF16),
             VM((2, seqs * heads, size), F32),
-            VM((seqs, 4 * heads, size), F32),
-            VM(shape, F32),
-            pltpu.SemaphoreType.DMA((seqs,)),
         ],
     )
+
+
+def run_store(k, keep, change, near, after, shape):
+    seqs, heads, size = shape[:3]
+    return call(
+        functools.partial(store_kernel, heads),
+        jax.ShapeDtypeStruct(shape, F32),
+        [k, keep, change, near, after],
+        smem=(),
+        loose=(4,),
+        hbm_out=(0,),
+        scratch=[VM((seqs, 4 * heads, size), F32), VM(shape, F32), pltpu.SemaphoreType.DMA((seqs,))],
+    )
+
+
+def copy_kernel(source, out):
+    out[...] = source[...]
 
 
 def mix_kernel(masks, where, *refs):
@@ -324,24 +353,20 @@
     out[...] = (own[...].astype(F32) + other[...].astype(F32)).reshape(out.shape).astype(out.dtype)
 
 
-def resid_kernel(masks, where, *refs):
-    count = len(masks)
-    tokens, mixed, gain = refs[:count], refs[count:-4], refs[-4]
-    moe, own, resid = refs[-3:]
+def resid_kernel(masks, where, tokens, *refs):
+    mixed, (gain, moe, own, resid) = refs[:-4], refs[-4:]
     me = where[0]
-    each = own.shape[0]
-    for ref, row in zip(tokens, masks):
-        for j, mask in enumerate(row):
-            at = pl.multiple_of((me ^ mask) * each, each)
-            resid[pl.ds(at, each), :] = ref[j].astype(F32)
-    if len(mixed) == 1:
-        resid[...] = resid[...] + mixed[0][...].astype(F32)
-    for ref, row in zip(mixed, masks if len(mixed) > 1 else ()):
-        for j, mask in enumerate(row):
-            width = ref.shape[2]
-            at = pl.ds(pl.multiple_of((me ^ mask) * width, width), width)
-            resid[:, at] = resid[:, at] + ref[j].astype(F32)
-    moe[...] = scale_rows(resid[...], gain[...]).astype(BF16)
+    count, each, size = tokens.shape
+    squares = None
+    for ref, row in zip(mixed, masks):
+        for j, mask in enumerate(row):
+            wide = ref.shape[2]
+            at = pl.ds(pl.multiple_of((me ^ mask) * wide, wide), wide) if len(row) * len(mixed) > 1 else slice(None)
+            part = tokens[:, :, at].astype(F32).reshape(count * each, wide) + ref[j].astype(F32)
+            resid[:, at] = part
+            squares = part * part if squares is None else squares + part * part
+    scale = lax.rsqrt(jnp.sum(squares, axis=-1, keepdims=True) / size + EPS)
+    moe[...] = (resid[...] * scale * gain[...]).astype(BF16)
     own[...] = resid[pl.ds(pl.multiple_of(me * each, each), each), :]
 
 
@@ -417,7 +442,8 @@
 
     flat = [w.transpose(1, 2, 0).reshape(-1, width) for w in (w_query, w_key, w_value, w_zgate)]
     columns = 4 * flat[0].shape[0]
-    tok_pieces = gather_xor(tokens, digits)
+    near_tokens = call(copy_kernel, sds(tokens.shape, BF16), [tokens], smem=())
+    tok_pieces = gather_xor(tokens, digits, near_tokens)
     stacked, gain_near, near, short = call(
         load_kernel,
         (
@@ -451,13 +477,14 @@
         spare=3,
     )
     by_seq = scatter_xor(projected, order)
-    beta, retain, route, route_other = call(
-        rates_kernel,
+    beta, retain, route, route_other, ordered = call(
+        functools.partial(rates_kernel, masks),
         (
             sds((2, each, heads), F32),
             sds((2, each, heads), F32),
             sds((half, 1), F32),
             sds((half, 1), F32),
+            sds((ep_count, each, width), BF16),
         ),
         [
             where,
@@ -469,22 +496,23 @@
             decay_bias[None],
             expert_ids.T,
             route_weight.T,
+            *tok_pieces,
         ],
         scratch=[VM((ep_count, 2, each, 1), F32)],
     )
-    gated, new_state = run_state(
+    gated, k_rows, keep, change = run_state(
         came,
         where,
         by_seq,
         beta.reshape(seqs, heads),
         retain.reshape(seqs, heads),
         head_gain[None],
-        near,
         short,
         state.shape,
     )
 
     gated_pieces = gather_xor(gated, digits)
+    new_state = run_store(k_rows, keep, change, near, gated_pieces[0], state.shape)
     out_cols = w_out.shape[1]
     mixed, mixed_other = call(
         functools.partial(mix_kernel, masks),
@@ -498,11 +526,11 @@
     if out_cols % 128:
         order = jnp.argsort(me ^ jnp.array([m for row in masks for m in row], jnp.int32))
         blocks = jnp.take(jnp.concatenate(mixed_pieces, axis=0), order, axis=0)
-        mixed_pieces = [blocks.transpose(1, 0, 2).reshape(half, width)]
+        mixed_pieces = [blocks.transpose(1, 0, 2).reshape(1, half, width)]
     moe_in, resid = call(
-        functools.partial(resid_kernel, masks),
+        functools.partial(resid_kernel, masks if out_cols % 128 == 0 else [[0]]),
         (sds((half, width), BF16), sds((each, width), F32)),
-        [where, *tok_pieces, *mixed_pieces, moe_gain[None]],
+        [where, ordered, *mixed_pieces, moe_gain[None]],
         scratch=[VM((half, width), F32)],
     )
     moe_other = exchange(moe_in, 0, 1)

time: 107 us -> 99 us (0.925)
  waiting for transfers between devices: 43.6 us -> 35.8 us
    ppermute x34, waiting for transfers between devices: 43.6 us -> 35.8 us  [exchange(): return lax.ppermute(value, AXES, pairs)]
    pallas_call x15 -> x17, Pallas kernels: 19.1 us -> 19.2 us  [call(): pl.pallas_call(kernel, out_shape=out_shape, in_specs=[pl.BlockSpec(memory...]
  transfers between devices with their start and end apart: 34 -> 34, of which waited for: 24 -> 24; matrix products, arithmetic and copies ran while one was open for 0% -> 0% of each run, Pallas kernels for 7% -> 11%
where the time goes in v4:
time: 99 us; the launch traced here: 98.8 us
  starting transfers between devices  41.8 us (42%)
  waiting for transfers between devices  35.8 us (36%)
  Pallas kernels  19.2 us (19%)
  between operations  1.04 us (1%)
    ppermute x34, starting transfers between devices, exchange(): return lax.ppermute(value, AXES, pairs)  41.8 us
    ppermute x34, waiting for transfers between devices, exchange(): return lax.ppermute(value, AXES, pairs)  35.8 us
    pallas_call x17, Pallas kernels, call(): pl.pallas_call(kernel, out_shape=out_shape, in_specs=[pl.BlockSpec(memory...  19.2 us
  transfers between devices with their start and end apart: 34, of which 24 were waited for; matrix products, arithmetic and copies ran while one was open for 0% of the time, Pallas kernels for 11%

profile of v4, /device:TPU:0, one launch (start us, length us, event | category | flops | bytes accessed | tf_op | source)
XLA Modules:
  0.0 98.8 jit_solution(13839261287452041596)
XLA Ops:
  0.6 5.1 %collective-permute-start.2 = (bf16[1,8,2048]{2,1,0:T(8,128)(2,1)}, bf16[1,8,2048]{2,1,0:T(8,128)(2,1)S(1)}, u32[]{:S(2)}, u32[]{:S(2)}) collective-permute-start(bf16[1,8,2048]{2,1,0:T(8,128)(2,1)} %bitcast.55), channel_id=1, source_target_pairs={{0,24},{1,25},{2,26},{3,27},{4,28},{5,29},{6,30},{7,31},{8,16},{9,... | collective-permute-start | bytes 98312 | tf_op jit(solution)/shard_map/ppermute | solution.py:70
  5.8 0.6 collective-permute-start
  6.4 0.8 copy-done.9
  7.2 0.7 collective-permute-done.2
  7.9 2.9 %collective-permute-done.1 = bf16[1,8,2048]{2,1,0:T(8,128)(2,1)S(1)} collective-permute-done((bf16[1,8,2048]{2,1,0:T(8,128)(2,1)}, bf16[1,8,2048]{2,1,0:T(8,128)(2,1)S(1)}, u32[]{:S(2)}, u32[]{:S(2)}) %collective-permute-start.1) | collective-permute-done | bytes 32800 | tf_op jit(solution)/shard_map/ppermute | solution.py:70
  10.8 1.6 %collective-permute-start.3 = (bf16[4,8,2048]{2,1,0:T(8,128)(2,1)S(1)}, bf16[4,8,2048]{2,1,0:T(8,128)(2,1)S(1)}, u32[]{:S(2)}, u32[]{:S(2)}) collective-permute-start(bf16[4,8,2048]{2,1,0:T(8,128)(2,1)S(1)} %pad_maximum_fusion.after.refs_0_), channel_id=1, source_target_pairs={{0,2},{1,3},{2,0},{3,1},{4,6},{5,7},{6,4},{7,5},{8,10},{9,11},{10,... | collective-permute-start | bytes 393224 | tf_op jit(solution)/shard_map/ppermute | solution.py:70
  12.4 1.5 %collective-permute-start.4 = (bf16[4,8,2048]{2,1,0:T(8,128)(2,1)S(1)}, bf16[4,8,2048]{2,1,0:T(8,128)(2,1)S(1)}, u32[]{:S(2)}, u32[]{:S(2)}) collective-permute-start(bf16[4,8,2048]{2,1,0:T(8,128)(2,1)S(1)} %pad_maximum_fusion.after.refs_0_), channel_id=1, source_target_pairs={{0,4},{1,5},{2,6},{3,7},{4,0},{5,1},{6,2},{7,3},{8,12},{9,13},{10,... | collective-permute-start | bytes 393224 | tf_op jit(solution)/shard_map/ppermute | solution.py:70
  13.9 0.5 collective-permute-start.5
  14.5 4.3 %shard_map.231 = (bf16[2048,256]{1,0:T(8,128)(2,1)S(1)}, f32[1,2048]{1,0:T(1,128)S(1)}, f32[16,1024,128]{2,1,0:T(8,128)S(1)}, bf16[16,1024,128]{2,1,0:T(8,128)(2,1)S(1)}) custom-call(bf16[4,8,2048]{2,1,0:T(8,128)(2,1)S(1)} %pad_maximum_fusion.after.refs_0_, bf16[64,2048]{1,0:T(8,128)(2,1)} %bitcast.78, bf16[64,2048]{1,0:T(8,128)(2,1)} %bitcast.79, ...), custom_call_target="tpu_custom_call" | custom-call | tf_op jit(solution)/shard_map/pallas_call | solution.py:35
  18.9 0.9 collective-permute-done.5.refs_3_
  19.8 0.8 shard_map.232.own.x_ref
  20.6 0.3 shard_map.234.own
  20.9 1.6 %collective-permute-done.6.other.x_ref = bf16[16,8,2048]{2,1,0:T(8,128)(2,1)S(1)} collective-permute-done((bf16[16,8,2048]{2,1,0:T(8,128)(2,1)S(1)}, bf16[16,8,2048]{2,1,0:T(8,128)(2,1)S(1)}, u32[]{:S(2)}, u32[]{:S(2)}) %collective-permute-start.6) | collective-permute-done | bytes 524320 | tf_op jit(solution)/shard_map/ppermute | solution.py:70
  22.5 0.9 shard_map.235
  23.4 0.7 collective-permute-start.7
  24.1 1.5 %collective-permute-start.8 = (bf16[4,2,8,256]{3,2,1,0:T(8,128)(2,1)S(1)}, bf16[4,2,8,256]{3,2,1,0:T(8,128)(2,1)S(1)}, u32[]{:S(2)}, u32[]{:S(2)}) collective-permute-start(bf16[4,2,8,256]{3,2,1,0:T(8,128)(2,1)S(1)} %get-tuple-element.40), channel_id=1, source_target_pairs={{0,4},{1,5},{2,6},{3,7},{4,0},{5,1},{6,2},{7,3},{8,12},{9,13},{10,... | collective-permute-start | bytes 98312 | tf_op jit(solution)/shard_map/ppermute | solution.py:70
  25.6 1.3 %collective-permute-start.9 = (bf16[4,2,8,256]{3,2,1,0:T(8,128)(2,1)S(1)}, bf16[4,2,8,256]{3,2,1,0:T(8,128)(2,1)S(1)}, u32[]{:S(2)}, u32[]{:S(2)}) collective-permute-start(bf16[4,2,8,256]{3,2,1,0:T(8,128)(2,1)S(1)} %get-tuple-element.41), channel_id=1, source_target_pairs={{0,6},{1,7},{2,4},{3,5},{4,2},{5,3},{6,0},{7,1},{8,14},{9,15},{10,... | collective-permute-start | bytes 98312 | tf_op jit(solution)/shard_map/ppermute | solution.py:70
  26.9 0.4 collective-permute-done.7
  27.4 0.6 collective-permute-done.8
  28.0 2.4 %collective-permute-done.9 = bf16[4,2,8,256]{3,2,1,0:T(8,128)(2,1)S(1)} collective-permute-done((bf16[4,2,8,256]{3,2,1,0:T(8,128)(2,1)S(1)}, bf16[4,2,8,256]{3,2,1,0:T(8,128)(2,1)S(1)}, u32[]{:S(2)}, u32[]{:S(2)}) %collective-permute-start.9) | collective-permute-done | bytes 32800 | tf_op jit(solution)/shard_map/ppermute | solution.py:70
  30.5 2.1 %collective-permute-start.11 = (bf16[4,2,8,256]{3,2,1,0:T(8,128)(2,1)S(1)}, bf16[4,2,8,256]{3,2,1,0:T(8,128)(2,1)S(1)}, u32[]{:S(2)}, u32[]{:S(2)}) collective-permute-start(bf16[4,2,8,256]{3,2,1,0:T(8,128)(2,1)S(1)} %bitcast.75), channel_id=1, source_target_pairs={{0,16},{1,17},{2,18},{3,19},{4,20},{5,21},{6,22},{7,23},{8,24},{9,... | collective-permute-start | bytes 98312 | tf_op jit(solution)/shard_map/ppermute | solution.py:70
  32.6 2.3 %collective-permute-start.12 = (bf16[4,2,8,256]{3,2,1,0:T(8,128)(2,1)S(1)}, bf16[4,2,8,256]{3,2,1,0:T(8,128)(2,1)S(1)}, u32[]{:S(2)}, u32[]{:S(2)}) collective-permute-start(bf16[4,2,8,256]{3,2,1,0:T(8,128)(2,1)S(1)} %bitcast.74), channel_id=1, source_target_pairs={{0,24},{1,25},{2,26},{3,27},{4,28},{5,29},{6,30},{7,31},{8,16},{9,... | collective-permute-start | bytes 98312 | tf_op jit(solution)/shard_map/ppermute | solution.py:70
  35.0 0.8 shard_map.233
  35.8 2.5 %collective-permute-done.12.refs_3_ = bf16[4,2,8,256]{3,2,1,0:T(8,128)(2,1)S(1)} collective-permute-done((bf16[4,2,8,256]{3,2,1,0:T(8,128)(2,1)S(1)}, bf16[4,2,8,256]{3,2,1,0:T(8,128)(2,1)S(1)}, u32[]{:S(2)}, u32[]{:S(2)}) %collective-permute-start.12) | collective-permute-done | bytes 32800 | tf_op jit(solution)/shard_map/ppermute | solution.py:70
  38.3 1.9 %shard_map.237 = (bf16[16,1024]{1,0:T(8,128)(2,1)S(1)}, f32[128,128]{1,0:T(8,128)S(1)}, f32[128,128]{1,0:T(8,128)S(1)}, f32[128,128]{1,0:T(8,128)S(1)}) custom-call(s32[2]{0:T(128)S(1)} %pad_add_fusion.where, bf16[4,2,8,256]{3,2,1,0:T(8,128)(2,1)S(1)} %bitcast.52, bf16[4,2,8,256]{3,2,1,0:T(8,128)(2,1)S(1)} %collective-permute-done.10.refs_1_, ...), custom_call_target="tpu_custom_call" | custom-call | tf_op jit(solution)/shard_map/pallas_call | solution.py:35
  40.2 2.3 %collective-permute-start.15 = (bf16[1,16,1024]{2,1,0:T(8,128)(2,1)S(1)}, bf16[1,16,1024]{2,1,0:T(8,128)(2,1)S(1)}, u32[]{:S(2)}, u32[]{:S(2)}) collective-permute-start(bf16[1,16,1024]{2,1,0:T(8,128)(2,1)S(1)} %bitcast.62), channel_id=1, source_target_pairs={{0,24},{1,25},{2,26},{3,27},{4,28},{5,29},{6,30},{7,31},{8,16},{9,... | collective-permute-start | bytes 98312 | tf_op jit(solution)/shard_map/ppermute | solution.py:70
  42.6 2.1 %collective-permute-start.13 = (bf16[1,16,1024]{2,1,0:T(8,128)(2,1)S(1)}, bf16[1,16,1024]{2,1,0:T(8,128)(2,1)S(1)}, u32[]{:S(2)}, u32[]{:S(2)}) collective-permute-start(bf16[1,16,1024]{2,1,0:T(8,128)(2,1)S(1)} %bitcast.64), channel_id=1, source_target_pairs={{0,8},{1,9},{2,10},{3,11},{4,12},{5,13},{6,14},{7,15},{8,0},{9,1},... | collective-permute-start | bytes 98312 | tf_op jit(solution)/shard_map/ppermute | solution.py:70
  44.7 1.3 %collective-permute-done.15 = bf16[1,16,1024]{2,1,0:T(8,128)(2,1)S(1)} collective-permute-done((bf16[1,16,1024]{2,1,0:T(8,128)(2,1)S(1)}, bf16[1,16,1024]{2,1,0:T(8,128)(2,1)S(1)}, u32[]{:S(2)}, u32[]{:S(2)}) %collective-permute-start.15) | collective-permute-done | bytes 32800 | tf_op jit(solution)/shard_map/ppermute | solution.py:70
  46.0 1.4 %collective-permute-done.14 = bf16[1,16,1024]{2,1,0:T(8,128)(2,1)S(1)} collective-permute-done((bf16[1,16,1024]{2,1,0:T(8,128)(2,1)S(1)}, bf16[1,16,1024]{2,1,0:T(8,128)(2,1)S(1)}, u32[]{:S(2)}, u32[]{:S(2)}) %collective-permute-start.14) | collective-permute-done | bytes 32800 | tf_op jit(solution)/shard_map/ppermute | solution.py:70
  47.4 0.9 collective-permute-start.16
  48.3 1.1 %collective-permute-start.17 = (bf16[4,16,1024]{2,1,0:T(8,128)(2,1)S(1)}, bf16[4,16,1024]{2,1,0:T(8,128)(2,1)S(1)}, u32[]{:S(2)}, u32[]{:S(2)}) collective-permute-start(bf16[4,16,1024]{2,1,0:T(8,128)(2,1)S(1)} %pad_maximum_fusion.1.refs_0_.after), channel_id=1, source_target_pairs={{0,4},{1,5},{2,6},{3,7},{4,0},{5,1},{6,2},{7,3},{8,12},{9,13},{10,... | collective-permute-start | bytes 393224 | tf_op jit(solution)/shard_map/ppermute | solution.py:70
  49.4 1.6 %collective-permute-start.18 = (bf16[4,16,1024]{2,1,0:T(8,128)(2,1)S(1)}, bf16[4,16,1024]{2,1,0:T(8,128)(2,1)S(1)}, u32[]{:S(2)}, u32[]{:S(2)}) collective-permute-start(bf16[4,16,1024]{2,1,0:T(8,128)(2,1)S(1)} %pad_maximum_fusion.1.refs_0_.after), channel_id=1, source_target_pairs={{0,6},{1,7},{2,4},{3,5},{4,2},{5,3},{6,0},{7,1},{8,14},{9,15},{10,... | collective-permute-start | bytes 393224 | tf_op jit(solution)/shard_map/ppermute | solution.py:70
  51.0 1.5 %collective-permute-done.16.refs_1_ = bf16[4,16,1024]{2,1,0:T(8,128)(2,1)S(1)} collective-permute-done((bf16[4,16,1024]{2,1,0:T(8,128)(2,1)S(1)}, bf16[4,16,1024]{2,1,0:T(8,128)(2,1)S(1)}, u32[]{:S(2)}, u32[]{:S(2)}) %collective-permute-start.16) | collective-permute-done | bytes 131104 | tf_op jit(solution)/shard_map/ppermute | solution.py:70
  52.4 0.8 collective-permute-done.17.refs_2_
  53.3 2.0 %collective-permute-done.18.refs_3_ = bf16[4,16,1024]{2,1,0:T(8,128)(2,1)S(1)} collective-permute-done((bf16[4,16,1024]{2,1,0:T(8,128)(2,1)S(1)}, bf16[4,16,1024]{2,1,0:T(8,128)(2,1)S(1)}, u32[]{:S(2)}, u32[]{:S(2)}) %collective-permute-start.18) | collective-permute-done | bytes 131104 | tf_op jit(solution)/shard_map/ppermute | solution.py:70
  55.2 0.8 shard_map.238
  56.2 1.2 %collective-permute-done.19.other = bf16[16,8,128]{2,1,0:T(8,128)(2,1)S(1)} collective-permute-done((bf16[16,8,128]{2,1,0:T(8,128)(2,1)S(1)}, bf16[16,8,128]{2,1,0:T(8,128)(2,1)S(1)}, u32[]{:S(2)}, u32[]{:S(2)}) %collective-permute-start.19) | collective-permute-done | bytes 32800 | tf_op jit(solution)/shard_map/ppermute | solution.py:70
  57.4 1.9 %collective-permute-start.22 = (bf16[1,128,128]{2,1,0:T(8,128)(2,1)S(1)}, bf16[1,128,128]{2,1,0:T(8,128)(2,1)S(1)}, u32[]{:S(2)}, u32[]{:S(2)}) collective-permute-start(bf16[1,128,128]{2,1,0:T(8,128)(2,1)S(1)} %bitcast.47), channel_id=1, source_target_pairs={{0,24},{1,25},{2,26},{3,27},{4,28},{5,29},{6,30},{7,31},{8,16},{9,... | collective-permute-start | bytes 98312 | tf_op jit(solution)/shard_map/ppermute | solution.py:70
  59.3 1.0 %collective-permute-start.21 = (bf16[1,128,128]{2,1,0:T(8,128)(2,1)S(1)}, bf16[1,128,128]{2,1,0:T(8,128)(2,1)S(1)}, u32[]{:S(2)}, u32[]{:S(2)}) collective-permute-start(bf16[1,128,128]{2,1,0:T(8,128)(2,1)S(1)} %bitcast.48), channel_id=1, source_target_pairs={{0,16},{1,17},{2,18},{3,19},{4,20},{5,21},{6,22},{7,23},{8,24},{9,... | collective-permute-start | bytes 98312 | tf_op jit(solution)/shard_map/ppermute | solution.py:70
  60.3 1.5 %collective-permute-start.20 = (bf16[1,128,128]{2,1,0:T(8,128)(2,1)S(1)}, bf16[1,128,128]{2,1,0:T(8,128)(2,1)S(1)}, u32[]{:S(2)}, u32[]{:S(2)}) collective-permute-start(bf16[1,128,128]{2,1,0:T(8,128)(2,1)S(1)} %bitcast.49), channel_id=1, source_target_pairs={{0,8},{1,9},{2,10},{3,11},{4,12},{5,13},{6,14},{7,15},{8,0},{9,1},... | collective-permute-start | bytes 98312 | tf_op jit(solution)/shard_map/ppermute | solution.py:70
  61.8 1.6 %collective-permute-done.22 = bf16[1,128,128]{2,1,0:T(8,128)(2,1)S(1)} collective-permute-done((bf16[1,128,128]{2,1,0:T(8,128)(2,1)S(1)}, bf16[1,128,128]{2,1,0:T(8,128)(2,1)S(1)}, u32[]{:S(2)}, u32[]{:S(2)}) %collective-permute-start.22) | collective-permute-done | bytes 32800 | tf_op jit(solution)/shard_map/ppermute | solution.py:70
  63.5 0.8 collective-permute-done.21
  64.2 0.2 collective-permute-done.20
  64.5 0.7 collective-permute-start.23
  65.1 1.5 %collective-permute-start.24 = (bf16[4,128,128]{2,1,0:T(8,128)(2,1)S(1)}, bf16[4,128,128]{2,1,0:T(8,128)(2,1)S(1)}, u32[]{:S(2)}, u32[]{:S(2)}) collective-permute-start(bf16[4,128,128]{2,1,0:T(8,128)(2,1)S(1)} %pad_maximum_fusion.2.refs_0_), channel_id=1, source_target_pairs={{0,4},{1,5},{2,6},{3,7},{4,0},{5,1},{6,2},{7,3},{8,12},{9,13},{10,... | collective-permute-start | bytes 393224 | tf_op jit(solution)/shard_map/ppermute | solution.py:70
  66.6 1.4 %collective-permute-start.25 = (bf16[4,128,128]{2,1,0:T(8,128)(2,1)S(1)}, bf16[4,128,128]{2,1,0:T(8,128)(2,1)S(1)}, u32[]{:S(2)}, u32[]{:S(2)}) collective-permute-start(bf16[4,128,128]{2,1,0:T(8,128)(2,1)S(1)} %pad_maximum_fusion.2.refs_0_), channel_id=1, source_target_pairs={{0,6},{1,7},{2,4},{3,5},{4,2},{5,3},{6,0},{7,1},{8,14},{9,15},{10,... | collective-permute-start | bytes 393224 | tf_op jit(solution)/shard_map/ppermute | solution.py:70
  68.0 2.6 %collective-permute-done.23.refs_1_ = bf16[4,128,128]{2,1,0:T(8,128)(2,1)S(1)} collective-permute-done((bf16[4,128,128]{2,1,0:T(8,128)(2,1)S(1)}, bf16[4,128,128]{2,1,0:T(8,128)(2,1)S(1)}, u32[]{:S(2)}, u32[]{:S(2)}) %collective-permute-start.23) | collective-permute-done | bytes 131104 | tf_op jit(solution)/shard_map/ppermute | solution.py:70
  70.6 2.3 %collective-permute-done.24.refs_2_ = bf16[4,128,128]{2,1,0:T(8,128)(2,1)S(1)} collective-permute-done((bf16[4,128,128]{2,1,0:T(8,128)(2,1)S(1)}, bf16[4,128,128]{2,1,0:T(8,128)(2,1)S(1)}, u32[]{:S(2)}, u32[]{:S(2)}) %collective-permute-start.24) | collective-permute-done | bytes 131104 | tf_op jit(solution)/shard_map/ppermute | solution.py:70
  72.9 1.0 %shard_map.240 = (bf16[128,2048]{1,0:T(8,128)(2,1)S(1)}, f32[8,2048]{1,0:T(8,128)S(1)}) custom-call(s32[2]{0:T(128)S(1)} %pad_add_fusion.where, bf16[16,8,2048]{2,1,0:T(8,128)(2,1)S(1)} %get-tuple-element.37.tokens, bf16[4,128,128]{2,1,0:T(8,128)(2,1)S(1)} %pad_maximum_fusion.2.refs_0_, bf16[4,128,128]{2,1,0:T(8,128)(2,1)S(1)} %collective-permute-done.23.refs_1_, ...), custom_call_target="tpu_custom_call" | custom-call | tf_op jit(solution)/shard_map/pallas_call | solution.py:35
  74.0 1.9 %collective-permute-done.26.rows_in = bf16[128,2048]{1,0:T(8,128)(2,1)S(1)} collective-permute-done((bf16[128,2048]{1,0:T(8,128)(2,1)S(1)}, bf16[128,2048]{1,0:T(8,128)(2,1)S(1)}, u32[]{:S(2)}, u32[]{:S(2)}) %collective-permute-start.26) | collective-permute-done | bytes 524320 | tf_op jit(solution)/shard_map/ppermute | solution.py:70
  75.9 1.6 %shard_map.242 = bf16[128,2048]{1,0:T(8,128)(2,1)S(1)} custom-call(bf16[128,2048]{1,0:T(8,128)(2,1)S(1)} %collective-permute-done.26.rows_in, f32[128,1]{1,0:T(8,128)S(1)} %get-tuple-element.55.route, bf16[1,2048]{1,0:T(2,128)(2,1)S(1)} %broadcast_in_dim.39.mix, bf16[2048,128]{1,0:T(8,128)(2,1)S(1)} %copy-done.3, bf16[2048,128]{1,0:T(8,128)(2,1)S(1)} %copy-done.4, ...), custom_call_target="tpu_custom_call" | custom-call | tf_op jit(solution)/shard_map/pallas_call | solution.py:35
  77.8 1.6 %shard_map.241.own = f32[128,2048]{1,0:T(8,128)S(1)} custom-call(bf16[128,2048]{1,0:T(8,128)(2,1)S(1)} %get-tuple-element.53.rows_in, f32[128,1]{1,0:T(8,128)S(1)} %get-tuple-element.54.route, bf16[1,2048]{1,0:T(2,128)(2,1)S(1)} %broadcast_in_dim.39.mix, bf16[2048,128]{1,0:T(8,128)(2,1)S(1)} %copy-done.3, bf16[2048,128]{1,0:T(8,128)(2,1)S(1)} %copy-done.4, ...), custom_call_target="tpu_custom_call" | custom-call | tf_op jit(solution)/shard_map/pallas_call | solution.py:35
  79.5 0.6 shard_map.243
  80.2 1.2 %collective-permute-start.28 = (bf16[4,8,2048]{2,1,0:T(8,128)(2,1)S(1)}, bf16[4,8,2048]{2,1,0:T(8,128)(2,1)S(1)}, u32[]{:S(2)}, u32[]{:S(2)}) collective-permute-start(bf16[4,8,2048]{2,1,0:T(8,128)(2,1)S(1)} %get-tuple-element.57), channel_id=1, source_target_pairs={{0,2},{1,3},{2,0},{3,1},{4,6},{5,7},{6,4},{7,5},{8,10},{9,11},{10,... | collective-permute-start | bytes 393224 | tf_op jit(solution)/shard_map/ppermute | solution.py:70
  81.4 1.0 %collective-permute-start.29 = (bf16[4,8,2048]{2,1,0:T(8,128)(2,1)S(1)}, bf16[4,8,2048]{2,1,0:T(8,128)(2,1)S(1)}, u32[]{:S(2)}, u32[]{:S(2)}) collective-permute-start(bf16[4,8,2048]{2,1,0:T(8,128)(2,1)S(1)} %get-tuple-element.58), channel_id=1, source_target_pairs={{0,4},{1,5},{2,6},{3,7},{4,0},{5,1},{6,2},{7,3},{8,12},{9,13},{10,... | collective-permute-start | bytes 393224 | tf_op jit(solution)/shard_map/ppermute | solution.py:70
  82.4 1.3 %collective-permute-start.30 = (bf16[4,8,2048]{2,1,0:T(8,128)(2,1)S(1)}, bf16[4,8,2048]{2,1,0:T(8,128)(2,1)S(1)}, u32[]{:S(2)}, u32[]{:S(2)}) collective-permute-start(bf16[4,8,2048]{2,1,0:T(8,128)(2,1)S(1)} %get-tuple-element.59), channel_id=1, source_target_pairs={{0,6},{1,7},{2,4},{3,5},{4,2},{5,3},{6,0},{7,1},{8,14},{9,15},{10,... | collective-permute-start | bytes 393224 | tf_op jit(solution)/shard_map/ppermute | solution.py:70
  83.7 2.9 %collective-permute-done.28.refs_1_ = bf16[4,8,2048]{2,1,0:T(8,128)(2,1)S(1)} collective-permute-done((bf16[4,8,2048]{2,1,0:T(8,128)(2,1)S(1)}, bf16[4,8,2048]{2,1,0:T(8,128)(2,1)S(1)}, u32[]{:S(2)}, u32[]{:S(2)}) %collective-permute-start.28) | collective-permute-done | bytes 131104 | tf_op jit(solution)/shard_map/ppermute | solution.py:70
  86.6 3.0 %collective-permute-done.29.refs_2_ = bf16[4,8,2048]{2,1,0:T(8,128)(2,1)S(1)} collective-permute-done((bf16[4,8,2048]{2,1,0:T(8,128)(2,1)S(1)}, bf16[4,8,2048]{2,1,0:T(8,128)(2,1)S(1)}, u32[]{:S(2)}, u32[]{:S(2)}) %collective-permute-start.29) | collective-permute-done | bytes 131104 | tf_op jit(solution)/shard_map/ppermute | solution.py:70
  89.7 1.1 %collective-permute-start.31 = (bf16[8,2048]{1,0:T(8,128)(2,1)S(1)}, bf16[8,2048]{1,0:T(8,128)(2,1)S(1)}, u32[]{:S(2)}, u32[]{:S(2)}) collective-permute-start(bf16[8,2048]{1,0:T(8,128)(2,1)S(1)} %get-tuple-element.61), channel_id=1, source_target_pairs={{0,8},{1,9},{2,10},{3,11},{4,12},{5,13},{6,14},{7,15},{8,0},{9,1},... | collective-permute-start | bytes 98312 | tf_op jit(solution)/shard_map/ppermute | solution.py:70
  90.8 1.6 %collective-permute-start.32 = (bf16[8,2048]{1,0:T(8,128)(2,1)S(1)}, bf16[8,2048]{1,0:T(8,128)(2,1)S(1)}, u32[]{:S(2)}, u32[]{:S(2)}) collective-permute-start(bf16[8,2048]{1,0:T(8,128)(2,1)S(1)} %get-tuple-element.62), channel_id=1, source_target_pairs={{0,16},{1,17},{2,18},{3,19},{4,20},{5,21},{6,22},{7,23},{8,24},{9,... | collective-permute-start | bytes 98312 | tf_op jit(solution)/shard_map/ppermute | solution.py:70
  92.4 1.7 %collective-permute-start.33 = (bf16[8,2048]{1,0:T(8,128)(2,1)S(1)}, bf16[8,2048]{1,0:T(8,128)(2,1)S(1)}, u32[]{:S(2)}, u32[]{:S(2)}) collective-permute-start(bf16[8,2048]{1,0:T(8,128)(2,1)S(1)} %get-tuple-element.63), channel_id=1, source_target_pairs={{0,24},{1,25},{2,26},{3,27},{4,28},{5,29},{6,30},{7,31},{8,16},{9,... | collective-permute-start | bytes 98312 | tf_op jit(solution)/shard_map/ppermute | solution.py:70
  94.1 3.8 %shard_map.246 = f32[16,8,128,128]{3,2,1,0:T(8,128)} custom-call(f32[128,128]{1,0:T(8,128)S(1)} %get-tuple-element.64.k_in, f32[128,128]{1,0:T(8,128)S(1)} %get-tuple-element.65.keep, f32[128,128]{1,0:T(8,128)S(1)} %get-tuple-element.66.change, f32[16,1024,128]{2,1,0:T(8,128)S(1)} %get-tuple-element.67.near, ...), custom_call_target="tpu_custom_call" | custom-call | tf_op jit(solution)/shard_map/pallas_call | solution.py:35
  97.9 0.2 collective-permute-done.33.refs_3_
  98.2 0.6 shard_map.245
  (60 shorter events, 1.0 us)
Async XLA Ops:
  0.6 7.2 %collective-permute-start.2 = (bf16[1,8,2048]{2,1,0:T(8,128)(2,1)}, bf16[1,8,2048]{2,1,0:T(8,128)(2,1)S(1)}, u32[]{:S(2)}, u32[]{:S(2)}) collective-permute-start(bf16[1,8,2048]{2,1,0:T(8,128)(2,1)} %bitcast.55), channel_id=1, source_target_pairs={{0,24},{1,25},{2,26},{3,27},{4,28},{5,29},{6,30},{7,31},{8,16},{9,... | collective-permute-start | bytes 98312 | tf_op jit(solution)/shard_map/ppermute | solution.py:70
  5.8 5.0 %collective-permute-start.1 = (bf16[1,8,2048]{2,1,0:T(8,128)(2,1)}, bf16[1,8,2048]{2,1,0:T(8,128)(2,1)S(1)}, u32[]{:S(2)}, u32[]{:S(2)}) collective-permute-start(bf16[1,8,2048]{2,1,0:T(8,128)(2,1)} %bitcast.56), channel_id=1, source_target_pairs={{0,16},{1,17},{2,18},{3,19},{4,20},{5,21},{6,22},{7,23},{8,24},{9,... | collective-permute-start | bytes 98312 | tf_op jit(solution)/shard_map/ppermute | solution.py:70
  5.8 5.0 %collective-permute-start = (bf16[1,8,2048]{2,1,0:T(8,128)(2,1)}, bf16[1,8,2048]{2,1,0:T(8,128)(2,1)S(1)}, u32[]{:S(2)}, u32[]{:S(2)}) collective-permute-start(bf16[1,8,2048]{2,1,0:T(8,128)(2,1)} %bitcast.57), channel_id=1, source_target_pairs={{0,8},{1,9},{2,10},{3,11},{4,12},{5,13},{6,14},{7,15},{8,0},{9,1},... | collective-permute-start | bytes 98312 | tf_op jit(solution)/shard_map/ppermute | solution.py:70
  6.4 0.8 copy-start.9
  10.8 8.1 %collective-permute-start.3 = (bf16[4,8,2048]{2,1,0:T(8,128)(2,1)S(1)}, bf16[4,8,2048]{2,1,0:T(8,128)(2,1)S(1)}, u32[]{:S(2)}, u32[]{:S(2)}) collective-permute-start(bf16[4,8,2048]{2,1,0:T(8,128)(2,1)S(1)} %pad_maximum_fusion.after.refs_0_), channel_id=1, source_target_pairs={{0,2},{1,3},{2,0},{3,1},{4,6},{5,7},{6,4},{7,5},{8,10},{9,11},{10,... | collective-permute-start | bytes 393224 | tf_op jit(solution)/shard_map/ppermute | solution.py:70
  12.4 6.5 %collective-permute-start.4 = (bf16[4,8,2048]{2,1,0:T(8,128)(2,1)S(1)}, bf16[4,8,2048]{2,1,0:T(8,128)(2,1)S(1)}, u32[]{:S(2)}, u32[]{:S(2)}) collective-permute-start(bf16[4,8,2048]{2,1,0:T(8,128)(2,1)S(1)} %pad_maximum_fusion.after.refs_0_), channel_id=1, source_target_pairs={{0,4},{1,5},{2,6},{3,7},{4,0},{5,1},{6,2},{7,3},{8,12},{9,13},{10,... | collective-permute-start | bytes 393224 | tf_op jit(solution)/shard_map/ppermute | solution.py:70
  13.9 5.9 %collective-permute-start.5 = (bf16[4,8,2048]{2,1,0:T(8,128)(2,1)S(1)}, bf16[4,8,2048]{2,1,0:T(8,128)(2,1)S(1)}, u32[]{:S(2)}, u32[]{:S(2)}) collective-permute-start(bf16[4,8,2048]{2,1,0:T(8,128)(2,1)S(1)} %pad_maximum_fusion.after.refs_0_), channel_id=1, source_target_pairs={{0,6},{1,7},{2,4},{3,5},{4,2},{5,3},{6,0},{7,1},{8,14},{9,15},{10,... | collective-permute-start | bytes 393224 | tf_op jit(solution)/shard_map/ppermute | solution.py:70
  18.8 16.1 %copy-start.7 = (bf16[2048,8]{0,1:T(8,128)(2,1)S(1)}, bf16[2048,8]{0,1:T(8,128)(2,1)}, u32[]{:S(2)}) copy-start(bf16[2048,8]{0,1:T(8,128)(2,1)} %param.29) | copy-start | bytes 98308
  18.8 16.1 %copy-start.8 = (bf16[2048,8]{0,1:T(8,128)(2,1)S(1)}, bf16[2048,8]{0,1:T(8,128)(2,1)}, u32[]{:S(2)}) copy-start(bf16[2048,8]{0,1:T(8,128)(2,1)} %param.30) | copy-start | bytes 98308
  18.8 16.1 %copy-start.11 = (s32[256,4]{0,1:T(4,128)S(1)}, s32[256,4]{0,1:T(4,128)}, u32[]{:S(2)}) copy-start(s32[256,4]{0,1:T(4,128)} %param.44) | copy-start | bytes 12292
  18.8 16.1 %copy-start.12 = (f32[256,4]{0,1:T(4,128)S(1)}, f32[256,4]{0,1:T(4,128)}, u32[]{:S(2)}) copy-start(f32[256,4]{0,1:T(4,128)} %param.45) | copy-start | bytes 12292
  18.8 16.1 %copy-start.13 = (f32[8]{0:T(128)S(1)}, f32[8]{0:T(128)}, u32[]{:S(2)}) copy-start(f32[8]{0:T(128)} %param.31) | copy-start | bytes 100
  18.9 16.1 %copy-start.14 = (f32[8]{0:T(128)S(1)}, f32[8]{0:T(128)}, u32[]{:S(2)}) copy-start(f32[8]{0:T(128)} %param.32) | copy-start | bytes 100
  18.9 19.5 %copy-start.15 = (f32[128]{0:T(128)S(1)}, f32[128]{0:T(128)}, u32[]{:S(2)}) copy-start(f32[128]{0:T(128)} %param.33) | copy-start | bytes 1540
  20.5 2.0 %collective-permute-start.6 = (bf16[16,8,2048]{2,1,0:T(8,128)(2,1)S(1)}, bf16[16,8,2048]{2,1,0:T(8,128)(2,1)S(1)}, u32[]{:S(2)}, u32[]{:S(2)}) collective-permute-start(bf16[16,8,2048]{2,1,0:T(8,128)(2,1)S(1)} %shard_map.232.own.x_ref), channel_id=1, source_target_pairs={{0,1},{1,0},{2,3},{3,2},{4,5},{5,4},{6,7},{7,6},{8,9},{9,8},{10,11... | collective-permute-start | bytes 1572872 | tf_op jit(solution)/shard_map/ppermute | solution.py:70
  20.9 34.3 %copy-start.6 = (bf16[1024,128]{1,0:T(8,128)(2,1)S(1)}, bf16[1024,128]{1,0:T(8,128)(2,1)}, u32[]{:S(2)}) copy-start(bf16[1024,128]{1,0:T(8,128)(2,1)} %refs_4_.1) | copy-start | bytes 786436
  23.4 49.5 %copy-start.10 = (f32[2048]{0:T(1024)S(1)}, f32[2048]{0:T(1024)}, u32[]{:S(2)}) copy-start(f32[2048]{0:T(1024)} %param.36) | copy-start | bytes 24580
  23.4 4.0 %collective-permute-start.7 = (bf16[4,2,8,256]{3,2,1,0:T(8,128)(2,1)S(1)}, bf16[4,2,8,256]{3,2,1,0:T(8,128)(2,1)S(1)}, u32[]{:S(2)}, u32[]{:S(2)}) collective-permute-start(bf16[4,2,8,256]{3,2,1,0:T(8,128)(2,1)S(1)} %get-tuple-element.39), channel_id=1, source_target_pairs={{0,2},{1,3},{2,0},{3,1},{4,6},{5,7},{6,4},{7,5},{8,10},{9,11},{10,... | collective-permute-start | bytes 98312 | tf_op jit(solution)/shard_map/ppermute | solution.py:70
  24.1 3.9 %collective-permute-start.8 = (bf16[4,2,8,256]{3,2,1,0:T(8,128)(2,1)S(1)}, bf16[4,2,8,256]{3,2,1,0:T(8,128)(2,1)S(1)}, u32[]{:S(2)}, u32[]{:S(2)}) collective-permute-start(bf16[4,2,8,256]{3,2,1,0:T(8,128)(2,1)S(1)} %get-tuple-element.40), channel_id=1, source_target_pairs={{0,4},{1,5},{2,6},{3,7},{4,0},{5,1},{6,2},{7,3},{8,12},{9,13},{10,... | collective-permute-start | bytes 98312 | tf_op jit(solution)/shard_map/ppermute | solution.py:70
  25.6 4.8 %collective-permute-start.9 = (bf16[4,2,8,256]{3,2,1,0:T(8,128)(2,1)S(1)}, bf16[4,2,8,256]{3,2,1,0:T(8,128)(2,1)S(1)}, u32[]{:S(2)}, u32[]{:S(2)}) collective-permute-start(bf16[4,2,8,256]{3,2,1,0:T(8,128)(2,1)S(1)} %get-tuple-element.41), channel_id=1, source_target_pairs={{0,6},{1,7},{2,4},{3,5},{4,2},{5,3},{6,0},{7,1},{8,14},{9,15},{10,... | collective-permute-start | bytes 98312 | tf_op jit(solution)/shard_map/ppermute | solution.py:70
  30.4 5.4 %collective-permute-start.10 = (bf16[4,2,8,256]{3,2,1,0:T(8,128)(2,1)S(1)}, bf16[4,2,8,256]{3,2,1,0:T(8,128)(2,1)S(1)}, u32[]{:S(2)}, u32[]{:S(2)}) collective-permute-start(bf16[4,2,8,256]{3,2,1,0:T(8,128)(2,1)S(1)} %bitcast.76), channel_id=1, source_target_pairs={{0,8},{1,9},{2,10},{3,11},{4,12},{5,13},{6,14},{7,15},{8,0},{9,1},... | collective-permute-start | bytes 98312 | tf_op jit(solution)/shard_map/ppermute | solution.py:70
  30.5 5.3 %collective-permute-start.11 = (bf16[4,2,8,256]{3,2,1,0:T(8,128)(2,1)S(1)}, bf16[4,2,8,256]{3,2,1,0:T(8,128)(2,1)S(1)}, u32[]{:S(2)}, u32[]{:S(2)}) collective-permute-start(bf16[4,2,8,256]{3,2,1,0:T(8,128)(2,1)S(1)} %bitcast.75), channel_id=1, source_target_pairs={{0,16},{1,17},{2,18},{3,19},{4,20},{5,21},{6,22},{7,23},{8,24},{9,... | collective-permute-start | bytes 98312 | tf_op jit(solution)/shard_map/ppermute | solution.py:70
  32.6 5.7 %collective-permute-start.12 = (bf16[4,2,8,256]{3,2,1,0:T(8,128)(2,1)S(1)}, bf16[4,2,8,256]{3,2,1,0:T(8,128)(2,1)S(1)}, u32[]{:S(2)}, u32[]{:S(2)}) collective-permute-start(bf16[4,2,8,256]{3,2,1,0:T(8,128)(2,1)S(1)} %bitcast.74), channel_id=1, source_target_pairs={{0,24},{1,25},{2,26},{3,27},{4,28},{5,29},{6,30},{7,31},{8,16},{9,... | collective-permute-start | bytes 98312 | tf_op jit(solution)/shard_map/ppermute | solution.py:70
  34.9 39.1 %copy-start.16 = (bf16[2048]{0:T(1024)(128)(2,1)S(1)}, bf16[2048]{0:T(1024)(128)(2,1)}, u32[]{:S(2)}) copy-start(bf16[2048]{0:T(1024)(128)(2,1)} %param.37) | copy-start | bytes 12292
  34.9 41.0 %copy-start = (bf16[1,2048,512]{2,1,0:T(8,128)(2,1)S(1)}, bf16[1,2048,512]{2,1,0:T(8,128)(2,1)}, u32[]{:S(2)}) copy-start(bf16[1,2048,512]{2,1,0:T(8,128)(2,1)} %param.41) | copy-start | bytes 6291460
  34.9 41.0 %copy-start.1 = (bf16[1,2048,512]{2,1,0:T(8,128)(2,1)S(1)}, bf16[1,2048,512]{2,1,0:T(8,128)(2,1)}, u32[]{:S(2)}) copy-start(bf16[1,2048,512]{2,1,0:T(8,128)(2,1)} %param.42) | copy-start | bytes 6291460
  35.0 41.0 %copy-start.2 = (bf16[1,512,2048]{2,1,0:T(8,128)(2,1)S(1)}, bf16[1,512,2048]{2,1,0:T(8,128)(2,1)}, u32[]{:S(2)}) copy-start(bf16[1,512,2048]{2,1,0:T(8,128)(2,1)} %param.43) | copy-start | bytes 6291460
  35.0 40.9 %copy-start.3 = (bf16[2048,128]{1,0:T(8,128)(2,1)S(1)}, bf16[2048,128]{1,0:T(8,128)(2,1)}, u32[]{:S(2)}) copy-start(bf16[2048,128]{1,0:T(8,128)(2,1)} %d_gate.3) | copy-start | bytes 1572868
  35.0 40.9 %copy-start.4 = (bf16[2048,128]{1,0:T(8,128)(2,1)S(1)}, bf16[2048,128]{1,0:T(8,128)(2,1)}, u32[]{:S(2)}) copy-start(bf16[2048,128]{1,0:T(8,128)(2,1)} %d_up.3) | copy-start | bytes 1572868
  35.0 40.9 %copy-start.5 = (bf16[128,2048]{1,0:T(8,128)(2,1)S(1)}, bf16[128,2048]{1,0:T(8,128)(2,1)}, u32[]{:S(2)}) copy-start(bf16[128,2048]{1,0:T(8,128)(2,1)} %d_down.3) | copy-start | bytes 1572868
  40.2 5.8 %collective-permute-start.15 = (bf16[1,16,1024]{2,1,0:T(8,128)(2,1)S(1)}, bf16[1,16,1024]{2,1,0:T(8,128)(2,1)S(1)}, u32[]{:S(2)}, u32[]{:S(2)}) collective-permute-start(bf16[1,16,1024]{2,1,0:T(8,128)(2,1)S(1)} %bitcast.62), channel_id=1, source_target_pairs={{0,24},{1,25},{2,26},{3,27},{4,28},{5,29},{6,30},{7,31},{8,16},{9,... | collective-permute-start | bytes 98312 | tf_op jit(solution)/shard_map/ppermute | solution.py:70
  42.6 4.8 %collective-permute-start.14 = (bf16[1,16,1024]{2,1,0:T(8,128)(2,1)S(1)}, bf16[1,16,1024]{2,1,0:T(8,128)(2,1)S(1)}, u32[]{:S(2)}, u32[]{:S(2)}) collective-permute-start(bf16[1,16,1024]{2,1,0:T(8,128)(2,1)S(1)} %bitcast.63), channel_id=1, source_target_pairs={{0,16},{1,17},{2,18},{3,19},{4,20},{5,21},{6,22},{7,23},{8,24},{9,... | collective-permute-start | bytes 98312 | tf_op jit(solution)/shard_map/ppermute | solution.py:70
  42.6 4.8 %collective-permute-start.13 = (bf16[1,16,1024]{2,1,0:T(8,128)(2,1)S(1)}, bf16[1,16,1024]{2,1,0:T(8,128)(2,1)S(1)}, u32[]{:S(2)}, u32[]{:S(2)}) collective-permute-start(bf16[1,16,1024]{2,1,0:T(8,128)(2,1)S(1)} %bitcast.64), channel_id=1, source_target_pairs={{0,8},{1,9},{2,10},{3,11},{4,12},{5,13},{6,14},{7,15},{8,0},{9,1},... | collective-permute-start | bytes 98312 | tf_op jit(solution)/shard_map/ppermute | solution.py:70
  47.4 5.0 %collective-permute-start.16 = (bf16[4,16,1024]{2,1,0:T(8,128)(2,1)S(1)}, bf16[4,16,1024]{2,1,0:T(8,128)(2,1)S(1)}, u32[]{:S(2)}, u32[]{:S(2)}) collective-permute-start(bf16[4,16,1024]{2,1,0:T(8,128)(2,1)S(1)} %pad_maximum_fusion.1.refs_0_.after), channel_id=1, source_target_pairs={{0,2},{1,3},{2,0},{3,1},{4,6},{5,7},{6,4},{7,5},{8,10},{9,11},{10,... | collective-permute-start | bytes 393224 | tf_op jit(solution)/shard_map/ppermute | solution.py:70
  48.3 5.0 %collective-permute-start.17 = (bf16[4,16,1024]{2,1,0:T(8,128)(2,1)S(1)}, bf16[4,16,1024]{2,1,0:T(8,128)(2,1)S(1)}, u32[]{:S(2)}, u32[]{:S(2)}) collective-permute-start(bf16[4,16,1024]{2,1,0:T(8,128)(2,1)S(1)} %pad_maximum_fusion.1.refs_0_.after), channel_id=1, source_target_pairs={{0,4},{1,5},{2,6},{3,7},{4,0},{5,1},{6,2},{7,3},{8,12},{9,13},{10,... | collective-permute-start | bytes 393224 | tf_op jit(solution)/shard_map/ppermute | solution.py:70
  49.4 5.9 %collective-permute-start.18 = (bf16[4,16,1024]{2,1,0:T(8,128)(2,1)S(1)}, bf16[4,16,1024]{2,1,0:T(8,128)(2,1)S(1)}, u32[]{:S(2)}, u32[]{:S(2)}) collective-permute-start(bf16[4,16,1024]{2,1,0:T(8,128)(2,1)S(1)} %pad_maximum_fusion.1.refs_0_.after), channel_id=1, source_target_pairs={{0,6},{1,7},{2,4},{3,5},{4,2},{5,3},{6,0},{7,1},{8,14},{9,15},{10,... | collective-permute-start | bytes 393224 | tf_op jit(solution)/shard_map/ppermute | solution.py:70
  56.1 1.3 %collective-permute-start.19 = (bf16[16,8,128]{2,1,0:T(8,128)(2,1)S(1)}, bf16[16,8,128]{2,1,0:T(8,128)(2,1)S(1)}, u32[]{:S(2)}, u32[]{:S(2)}) collective-permute-start(bf16[16,8,128]{2,1,0:T(8,128)(2,1)S(1)} %get-tuple-element.51), channel_id=1, source_target_pairs={{0,1},{1,0},{2,3},{3,2},{4,5},{5,4},{6,7},{7,6},{8,9},{9,8},{10,11... | collective-permute-start | bytes 98312 | tf_op jit(solution)/shard_map/ppermute | solution.py:70
  57.4 6.1 %collective-permute-start.22 = (bf16[1,128,128]{2,1,0:T(8,128)(2,1)S(1)}, bf16[1,128,128]{2,1,0:T(8,128)(2,1)S(1)}, u32[]{:S(2)}, u32[]{:S(2)}) collective-permute-start(bf16[1,128,128]{2,1,0:T(8,128)(2,1)S(1)} %bitcast.47), channel_id=1, source_target_pairs={{0,24},{1,25},{2,26},{3,27},{4,28},{5,29},{6,30},{7,31},{8,16},{9,... | collective-permute-start | bytes 98312 | tf_op jit(solution)/shard_map/ppermute | solution.py:70
  59.3 5.0 %collective-permute-start.21 = (bf16[1,128,128]{2,1,0:T(8,128)(2,1)S(1)}, bf16[1,128,128]{2,1,0:T(8,128)(2,1)S(1)}, u32[]{:S(2)}, u32[]{:S(2)}) collective-permute-start(bf16[1,128,128]{2,1,0:T(8,128)(2,1)S(1)} %bitcast.48), channel_id=1, source_target_pairs={{0,16},{1,17},{2,18},{3,19},{4,20},{5,21},{6,22},{7,23},{8,24},{9,... | collective-permute-start | bytes 98312 | tf_op jit(solution)/shard_map/ppermute | solution.py:70
  60.3 4.1 %collective-permute-start.20 = (bf16[1,128,128]{2,1,0:T(8,128)(2,1)S(1)}, bf16[1,128,128]{2,1,0:T(8,128)(2,1)S(1)}, u32[]{:S(2)}, u32[]{:S(2)}) collective-permute-start(bf16[1,128,128]{2,1,0:T(8,128)(2,1)S(1)} %bitcast.49), channel_id=1, source_target_pairs={{0,8},{1,9},{2,10},{3,11},{4,12},{5,13},{6,14},{7,15},{8,0},{9,1},... | collective-permute-start | bytes 98312 | tf_op jit(solution)/shard_map/ppermute | solution.py:70
  64.5 6.2 %collective-permute-start.23 = (bf16[4,128,128]{2,1,0:T(8,128)(2,1)S(1)}, bf16[4,128,128]{2,1,0:T(8,128)(2,1)S(1)}, u32[]{:S(2)}, u32[]{:S(2)}) collective-permute-start(bf16[4,128,128]{2,1,0:T(8,128)(2,1)S(1)} %pad_maximum_fusion.2.refs_0_), channel_id=1, source_target_pairs={{0,2},{1,3},{2,0},{3,1},{4,6},{5,7},{6,4},{7,5},{8,10},{9,11},{10,... | collective-permute-start | bytes 393224 | tf_op jit(solution)/shard_map/ppermute | solution.py:70
  65.1 7.8 %collective-permute-start.24 = (bf16[4,128,128]{2,1,0:T(8,128)(2,1)S(1)}, bf16[4,128,128]{2,1,0:T(8,128)(2,1)S(1)}, u32[]{:S(2)}, u32[]{:S(2)}) collective-permute-start(bf16[4,128,128]{2,1,0:T(8,128)(2,1)S(1)} %pad_maximum_fusion.2.refs_0_), channel_id=1, source_target_pairs={{0,4},{1,5},{2,6},{3,7},{4,0},{5,1},{6,2},{7,3},{8,12},{9,13},{10,... | collective-permute-start | bytes 393224 | tf_op jit(solution)/shard_map/ppermute | solution.py:70
  66.6 6.3 %collective-permute-start.25 = (bf16[4,128,128]{2,1,0:T(8,128)(2,1)S(1)}, bf16[4,128,128]{2,1,0:T(8,128)(2,1)S(1)}, u32[]{:S(2)}, u32[]{:S(2)}) collective-permute-start(bf16[4,128,128]{2,1,0:T(8,128)(2,1)S(1)} %pad_maximum_fusion.2.refs_0_), channel_id=1, source_target_pairs={{0,6},{1,7},{2,4},{3,5},{4,2},{5,3},{6,0},{7,1},{8,14},{9,15},{10,... | collective-permute-start | bytes 393224 | tf_op jit(solution)/shard_map/ppermute | solution.py:70
  73.9 2.0 %collective-permute-start.26 = (bf16[128,2048]{1,0:T(8,128)(2,1)S(1)}, bf16[128,2048]{1,0:T(8,128)(2,1)S(1)}, u32[]{:S(2)}, u32[]{:S(2)}) collective-permute-start(bf16[128,2048]{1,0:T(8,128)(2,1)S(1)} %get-tuple-element.53.rows_in), channel_id=1, source_target_pairs={{0,1},{1,0},{2,3},{3,2},{4,5},{5,4},{6,7},{7,6},{8,9},{9,8},{10,11... | collective-permute-start | bytes 1572872 | tf_op jit(solution)/shard_map/ppermute | solution.py:70
  77.6 2.0 %collective-permute-start.27 = (bf16[128,2048]{1,0:T(8,128)(2,1)S(1)}, bf16[128,2048]{1,0:T(8,128)(2,1)S(1)}, u32[]{:S(2)}, u32[]{:S(2)}) collective-permute-start(bf16[128,2048]{1,0:T(8,128)(2,1)S(1)} %shard_map.242), channel_id=1, source_target_pairs={{0,1},{1,0},{2,3},{3,2},{4,5},{5,4},{6,7},{7,6},{8,9},{9,8},{10,11... | collective-permute-start | bytes 1572872 | tf_op jit(solution)/shard_map/ppermute | solution.py:70
  80.2 6.4 %collective-permute-start.28 = (bf16[4,8,2048]{2,1,0:T(8,128)(2,1)S(1)}, bf16[4,8,2048]{2,1,0:T(8,128)(2,1)S(1)}, u32[]{:S(2)}, u32[]{:S(2)}) collective-permute-start(bf16[4,8,2048]{2,1,0:T(8,128)(2,1)S(1)} %get-tuple-element.57), channel_id=1, source_target_pairs={{0,2},{1,3},{2,0},{3,1},{4,6},{5,7},{6,4},{7,5},{8,10},{9,11},{10,... | collective-permute-start | bytes 393224 | tf_op jit(solution)/shard_map/ppermute | solution.py:70
  81.4 8.2 %collective-permute-start.29 = (bf16[4,8,2048]{2,1,0:T(8,128)(2,1)S(1)}, bf16[4,8,2048]{2,1,0:T(8,128)(2,1)S(1)}, u32[]{:S(2)}, u32[]{:S(2)}) collective-permute-start(bf16[4,8,2048]{2,1,0:T(8,128)(2,1)S(1)} %get-tuple-element.58), channel_id=1, source_target_pairs={{0,4},{1,5},{2,6},{3,7},{4,0},{5,1},{6,2},{7,3},{8,12},{9,13},{10,... | collective-permute-start | bytes 393224 | tf_op jit(solution)/shard_map/ppermute | solution.py:70
  82.4 7.1 %collective-permute-start.30 = (bf16[4,8,2048]{2,1,0:T(8,128)(2,1)S(1)}, bf16[4,8,2048]{2,1,0:T(8,128)(2,1)S(1)}, u32[]{:S(2)}, u32[]{:S(2)}) collective-permute-start(bf16[4,8,2048]{2,1,0:T(8,128)(2,1)S(1)} %get-tuple-element.59), channel_id=1, source_target_pairs={{0,6},{1,7},{2,4},{3,5},{4,2},{5,3},{6,0},{7,1},{8,14},{9,15},{10,... | collective-permute-start | bytes 393224 | tf_op jit(solution)/shard_map/ppermute | solution.py:70
  89.7 8.2 %collective-permute-start.31 = (bf16[8,2048]{1,0:T(8,128)(2,1)S(1)}, bf16[8,2048]{1,0:T(8,128)(2,1)S(1)}, u32[]{:S(2)}, u32[]{:S(2)}) collective-permute-start(bf16[8,2048]{1,0:T(8,128)(2,1)S(1)} %get-tuple-element.61), channel_id=1, source_target_pairs={{0,8},{1,9},{2,10},{3,11},{4,12},{5,13},{6,14},{7,15},{8,0},{9,1},... | collective-permute-start | bytes 98312 | tf_op jit(solution)/shard_map/ppermute | solution.py:70
  90.8 7.1 %collective-permute-start.32 = (bf16[8,2048]{1,0:T(8,128)(2,1)S(1)}, bf16[8,2048]{1,0:T(8,128)(2,1)S(1)}, u32[]{:S(2)}, u32[]{:S(2)}) collective-permute-start(bf16[8,2048]{1,0:T(8,128)(2,1)S(1)} %get-tuple-element.62), channel_id=1, source_target_pairs={{0,16},{1,17},{2,18},{3,19},{4,20},{5,21},{6,22},{7,23},{8,24},{9,... | collective-permute-start | bytes 98312 | tf_op jit(solution)/shard_map/ppermute | solution.py:70
  92.4 5.7 %collective-permute-start.33 = (bf16[8,2048]{1,0:T(8,128)(2,1)S(1)}, bf16[8,2048]{1,0:T(8,128)(2,1)S(1)}, u32[]{:S(2)}, u32[]{:S(2)}) collective-permute-start(bf16[8,2048]{1,0:T(8,128)(2,1)S(1)} %get-tuple-element.63), channel_id=1, source_target_pairs={{0,24},{1,25},{2,26},{3,27},{4,28},{5,29},{6,30},{7,31},{8,16},{9,... | collective-permute-start | bytes 98312 | tf_op jit(solution)/shard_map/ppermute | solution.py:70

commit v5 on v4

--- a/solution.py
+++ b/solution.py
@@ -133,20 +133,34 @@
     copies.append(pltpu.make_async_copy(gain, gain_out, sems.at[4]))
     for c in copies:
         c.start()
-    seqs = state.shape[0]
-    fetch = lambda i: pltpu.make_async_copy(state.at[i], near.at[i], state_sems.at[i])
-    for i in range(seqs):
-        fetch(i).start()
+    first = state.shape[0] - near.shape[0]
+    begin_state(first, state, near, state_sems)
     for c in copies:
         c.wait()
     stacked[...] = rows[...].astype(F32).T.astype(BF16)
-
+    finish_state(first, state, near, short, state_sems)
+
+
+def begin_state(first, state, near, sems):
+    for i in range(near.shape[0]):
+        pltpu.make_async_copy(state.at[first + i], near.at[i], sems.at[i]).start()
+
+
+def finish_state(first, state, near, short, sems):
     def one(i, carry):
-        fetch(i).wait()
+        pltpu.make_async_copy(state.at[first + i], near.at[i], sems.at[i]).wait()
         short[i] = near[i].astype(BF16)
         return carry
 
-    lax.fori_loop(0, seqs, one, 0)
+    lax.fori_loop(0, near.shape[0], one, 0)
+
+
+def bring_kernel(after, tokens, state, tokens_out, near, short, sem, sems):
+    copy = pltpu.make_async_copy(tokens, tokens_out, sem)
+    copy.start()
+    begin_state(0, state, near, sems)
+    copy.wait()
+    finish_state(0, state, near, short, sems)
 
 
 def norm_kernel(masks, where, *refs):
@@ -218,15 +232,15 @@
 
 
 def state_kernel(heads, came, where, *refs):
-    pieces, (beta, retain, gain, short, gated, k_out, keep_out, change_out) = (
+    pieces, (beta, retain, gain, *shorts, gated, k_out, keep_out, change_out) = (
         refs[: len(came)],
-        refs[len(came) : len(came) + 8],
-    )
-    cols, rows, both, reads = refs[len(came) + 8 :]
+        refs[len(came) : -4],
+    )
+    cols, rows, both, reads = refs[-4:]
     for ref, row in zip(pieces, came):
         for j, mask in enumerate(row):
             cols[where[0] ^ mask] = ref[j].reshape(cols.shape[1:])
-    seqs, size = short.shape[0], short.shape[2]
+    seqs, size = cols.shape[1], shorts[0].shape[2]
     count, width = cols.shape[0], cols.shape[2]
     piece = width // (4 * heads)
     for first in range(0, width, size):
@@ -254,8 +268,9 @@
         at = slice(h * size, (h + 1) * size)
         both[:, :heads, at] = jnp.where(owner == h, k3, 0.0).astype(BF16)
         both[:, heads:, at] = jnp.where(owner == h, q3, 0.0).astype(BF16)
-    for i in range(seqs):
-        found = jnp.dot(both[i], short[i], preferred_element_type=F32)
+    places = [(short, i) for short in shorts for i in range(short.shape[0])]
+    for i, (short, j) in enumerate(places):
+        found = jnp.dot(both[i], short[j], preferred_element_type=F32)
         reads[0, i * heads : (i + 1) * heads, :] = found[:heads]
         reads[1, i * heads : (i + 1) * heads, :] = found[heads:]
     keep = rows[5]
@@ -267,8 +282,8 @@
         gated[:, h * size : (h + 1) * size] = reads[1, pl.ds(h, seqs, stride=heads), :].astype(BF16)
 
 
-def store_kernel(heads, k_in, keep, change, near, after, new_state, lefts, new, sems):
-    seqs, size = near.shape[0], near.shape[2]
+def store_kernel(heads, k_in, keep, change, near, near_late, after, new_state, lefts, new, sems):
+    seqs, size = new.shape[0], near.shape[2]
     store = lambda i: pltpu.make_async_copy(new.at[i], new_state.at[i], sems.at[i])
     k = k_in[...]
     high = k.astype(BF16).astype(F32)
@@ -279,7 +294,8 @@
     lefts[:, 3 * heads :] = jnp.zeros((seqs, lefts.shape[1] - 3 * heads, size), F32)
     head_row = lax.broadcasted_iota(jnp.int32, (lefts.shape[1], size), 0) % heads
 
-    def one(i, carry):
+    def one(source, first, n, carry):
+        i = first + n
         at = pl.ds(pl.multiple_of(i * heads, heads), heads)
         step = change[at, :]
         top = step.astype(BF16).astype(F32)
@@ -289,17 +305,19 @@
         added = jnp.dot(lefts[i].T.astype(BF16), right, preferred_element_type=F32)
         rate = keep[at, :]
         for h in range(heads):
-            old = near[i, h * size : (h + 1) * size, :]
+            old = source[n, h * size : (h + 1) * size, :]
             new[i, h] = rate[h : h + 1, :] * old + added[:, h * size : (h + 1) * size]
         store(i).start()
         return carry
 
-    lax.fori_loop(0, seqs, one, 0, unroll=2)
+    early = near.shape[0]
+    lax.fori_loop(0, early, functools.partial(one, near, 0), 0, unroll=2)
+    lax.fori_loop(0, seqs - early, functools.partial(one, near_late, early), 0, unroll=2)
     for i in range(seqs):
         store(i).wait()
 
 
-def run_state(came, where, pieces, beta, retain, gain, short, shape):
+def run_state(came, where, pieces, beta, retain, gain, shorts, shape):
     seqs, heads, size = shape[:3]
     count, columns = sum(map(len, came)), pieces[0].shape[-1]
     sds = jax.ShapeDtypeStruct
@@ -307,7 +325,7 @@
     return call(
         functools.partial(state_kernel, heads, came),
         (sds((seqs, heads * size), BF16), per_head, per_head, per_head),
-        [where, *pieces, beta, retain, gain, short],
+        [where, *pieces, beta, retain, gain, *shorts],
         scratch=[
             VM((count, seqs, columns), BF16),
             VM((6, seqs * heads, size), F32),
@@ -317,21 +335,17 @@
     )
 
 
-def run_store(k, keep, change, near, after, shape):
+def run_store(k, keep, change, near, near_late, after, shape):
     seqs, heads, size = shape[:3]
     return call(
         functools.partial(store_kernel, heads),
         jax.ShapeDtypeStruct(shape, F32),
-        [k, keep, change, near, after],
+        [k, keep, change, near, near_late, after],
         smem=(),
-        loose=(4,),
+        loose=(5,),
         hbm_out=(0,),
         scratch=[VM((seqs, 4 * heads, size), F32), VM(shape, F32), pltpu.SemaphoreType.DMA((seqs,))],
     )
-
-
-def copy_kernel(source, out):
-    out[...] = source[...]
 
 
 def mix_kernel(masks, where, *refs):
@@ -442,18 +456,29 @@
 
     flat = [w.transpose(1, 2, 0).reshape(-1, width) for w in (w_query, w_key, w_value, w_zgate)]
     columns = 4 * flat[0].shape[0]
-    near_tokens = call(copy_kernel, sds(tokens.shape, BF16), [tokens], smem=())
+    early = seqs * 5 // 16
+    parts = ((early, heads * size, size), (seqs - early, heads * size, size))
+    by_rows = state.reshape(seqs, heads * size, size)
+    near_tokens, near_first, short_first = call(
+        bring_kernel,
+        (sds(tokens.shape, BF16), sds(parts[0], F32), sds(parts[0], BF16)),
+        [where, tokens, by_rows],
+        smem=(),
+        hbm=(1, 2),
+        loose=(0,),
+        scratch=[pltpu.SemaphoreType.DMA, pltpu.SemaphoreType.DMA((early,))],
+    )
     tok_pieces = gather_xor(tokens, digits, near_tokens)
     stacked, gain_near, near, short = call(
         load_kernel,
         (
             sds((width, columns), BF16),
             sds((1, width), F32),
-            sds((seqs, heads * size, size), F32),
-            sds((seqs, heads * size, size), BF16),
+            sds(parts[1], F32),
+            sds(parts[1], BF16),
         ),
-        [tok_pieces[0], *flat, mix_gain[None], state.reshape(seqs, heads * size, size)],
-        scratch=[VM((columns, width), BF16), pltpu.SemaphoreType.DMA((5,)), pltpu.SemaphoreType.DMA((seqs,))],
+        [tok_pieces[0], *flat, mix_gain[None], by_rows],
+        scratch=[VM((columns, width), BF16), pltpu.SemaphoreType.DMA((5,)), pltpu.SemaphoreType.DMA((seqs - early,))],
         smem=(),
         hbm=range(1, 7),
         loose=(0,),
@@ -507,12 +532,12 @@
         beta.reshape(seqs, heads),
         retain.reshape(seqs, heads),
         head_gain[None],
-        short,
+        (short_first, short),
         state.shape,
     )
 
     gated_pieces = gather_xor(gated, digits)
-    new_state = run_store(k_rows, keep, change, near, gated_pieces[0], state.shape)
+    new_state = run_store(k_rows, keep, change, near_first, near, gated_pieces[0], state.shape)
     out_cols = w_out.shape[1]
     mixed, mixed_other = call(
         functools.partial(mix_kernel, masks),

time: 99 us -> 98.9 us (level)
  transfers between devices with their start and end apart: 34 -> 34, of which waited for: 24 -> 24; matrix products, arithmetic and copies ran while one was open for 0% -> 0% of each run, Pallas kernels for 11% -> 12%
where the time goes in v5:
time: 98.9 us; the launch traced here: 98.7 us
  starting transfers between devices  41.8 us (42%)
  waiting for transfers between devices  35.7 us (36%)
  Pallas kernels  20.1 us (20%)
  between operations  1 us (1%)
    ppermute x34, starting transfers between devices, exchange(): return lax.ppermute(value, AXES, pairs)  41.8 us
    ppermute x34, waiting for transfers between devices, exchange(): return lax.ppermute(value, AXES, pairs)  35.7 us
    pallas_call x17, Pallas kernels, call(): pl.pallas_call(kernel, out_shape=out_shape, in_specs=[pl.BlockSpec(memory...  20.1 us
  transfers between devices with their start and end apart: 34, of which 24 were waited for; matrix products, arithmetic and copies ran while one was open for 0% of the time, Pallas kernels for 12%

profile of v5, /device:TPU:0, one launch (start us, length us, event | category | flops | bytes accessed | tf_op | source)
XLA Modules:
  0.0 98.7 jit_solution(4694204586613272241)
XLA Ops:
  0.6 5.1 %collective-permute-start.2 = (bf16[1,8,2048]{2,1,0:T(8,128)(2,1)}, bf16[1,8,2048]{2,1,0:T(8,128)(2,1)S(1)}, u32[]{:S(2)}, u32[]{:S(2)}) collective-permute-start(bf16[1,8,2048]{2,1,0:T(8,128)(2,1)} %bitcast.80), channel_id=1, source_target_pairs={{0,24},{1,25},{2,26},{3,27},{4,28},{5,29},{6,30},{7,31},{8,16},{9,... | collective-permute-start | bytes 98312 | tf_op jit(solution)/shard_map/ppermute | solution.py:70
  5.8 0.6 collective-permute-start
  6.5 1.8 %shard_map.230 = (bf16[8,2048]{1,0:T(8,128)(2,1)S(1)}, f32[5,1024,128]{2,1,0:T(8,128)S(1)}, bf16[5,1024,128]{2,1,0:T(8,128)(2,1)S(1)}) custom-call(s32[2]{0:T(128)S(1)} %pad_add_fusion.after.where, bf16[8,2048]{1,0:T(8,128)(2,1)} %tokens.1, f32[16,1024,128]{2,1,0:T(8,128)} %bitcast.74), custom_call_target="tpu_custom_call" | custom-call | tf_op jit(solution)/shard_map/pallas_call | solution.py:35
  8.3 2.5 %collective-permute-done.1 = bf16[1,8,2048]{2,1,0:T(8,128)(2,1)S(1)} collective-permute-done((bf16[1,8,2048]{2,1,0:T(8,128)(2,1)}, bf16[1,8,2048]{2,1,0:T(8,128)(2,1)S(1)}, u32[]{:S(2)}, u32[]{:S(2)}) %collective-permute-start.1) | collective-permute-done | bytes 32800 | tf_op jit(solution)/shard_map/ppermute | solution.py:70
  10.8 1.6 %collective-permute-start.3 = (bf16[4,8,2048]{2,1,0:T(8,128)(2,1)S(1)}, bf16[4,8,2048]{2,1,0:T(8,128)(2,1)S(1)}, u32[]{:S(2)}, u32[]{:S(2)}) collective-permute-start(bf16[4,8,2048]{2,1,0:T(8,128)(2,1)S(1)} %pad_maximum_fusion.after.refs_0_), channel_id=1, source_target_pairs={{0,2},{1,3},{2,0},{3,1},{4,6},{5,7},{6,4},{7,5},{8,10},{9,11},{10,... | collective-permute-start | bytes 393224 | tf_op jit(solution)/shard_map/ppermute | solution.py:70
  12.4 1.5 %collective-permute-start.4 = (bf16[4,8,2048]{2,1,0:T(8,128)(2,1)S(1)}, bf16[4,8,2048]{2,1,0:T(8,128)(2,1)S(1)}, u32[]{:S(2)}, u32[]{:S(2)}) collective-permute-start(bf16[4,8,2048]{2,1,0:T(8,128)(2,1)S(1)} %pad_maximum_fusion.after.refs_0_), channel_id=1, source_target_pairs={{0,4},{1,5},{2,6},{3,7},{4,0},{5,1},{6,2},{7,3},{8,12},{9,13},{10,... | collective-permute-start | bytes 393224 | tf_op jit(solution)/shard_map/ppermute | solution.py:70
  13.9 0.5 collective-permute-start.5
  14.4 3.4 %shard_map.231 = (bf16[2048,256]{1,0:T(8,128)(2,1)S(1)}, f32[1,2048]{1,0:T(1,128)S(1)}, f32[11,1024,128]{2,1,0:T(8,128)S(1)}, bf16[11,1024,128]{2,1,0:T(8,128)(2,1)S(1)}) custom-call(bf16[4,8,2048]{2,1,0:T(8,128)(2,1)S(1)} %pad_maximum_fusion.after.refs_0_, bf16[64,2048]{1,0:T(8,128)(2,1)} %bitcast.76, bf16[64,2048]{1,0:T(8,128)(2,1)} %bitcast.77, ...), custom_call_target="tpu_custom_call" | custom-call | tf_op jit(solution)/shard_map/pallas_call | solution.py:35
  17.8 0.5 collective-permute-done.4.refs_2_
  18.3 1.5 %collective-permute-done.5.refs_3_ = bf16[4,8,2048]{2,1,0:T(8,128)(2,1)S(1)} collective-permute-done((bf16[4,8,2048]{2,1,0:T(8,128)(2,1)S(1)}, bf16[4,8,2048]{2,1,0:T(8,128)(2,1)S(1)}, u32[]{:S(2)}, u32[]{:S(2)}) %collective-permute-start.5) | collective-permute-done | bytes 131104 | tf_op jit(solution)/shard_map/ppermute | solution.py:70
  19.8 0.8 shard_map.232.own.x_ref
  20.7 0.3 shard_map.234.own
  21.0 1.6 %collective-permute-done.6.other.x_ref = bf16[16,8,2048]{2,1,0:T(8,128)(2,1)S(1)} collective-permute-done((bf16[16,8,2048]{2,1,0:T(8,128)(2,1)S(1)}, bf16[16,8,2048]{2,1,0:T(8,128)(2,1)S(1)}, u32[]{:S(2)}, u32[]{:S(2)}) %collective-permute-start.6) | collective-permute-done | bytes 524320 | tf_op jit(solution)/shard_map/ppermute | solution.py:70
  22.6 0.9 shard_map.235
  23.4 0.6 collective-permute-start.7
  24.0 0.6 collective-permute-start.8
  24.6 2.4 %collective-permute-start.9 = (bf16[4,2,8,256]{3,2,1,0:T(8,128)(2,1)S(1)}, bf16[4,2,8,256]{3,2,1,0:T(8,128)(2,1)S(1)}, u32[]{:S(2)}, u32[]{:S(2)}) collective-permute-start(bf16[4,2,8,256]{3,2,1,0:T(8,128)(2,1)S(1)} %get-tuple-element.45), channel_id=1, source_target_pairs={{0,6},{1,7},{2,4},{3,5},{4,2},{5,3},{6,0},{7,1},{8,14},{9,15},{10,... | collective-permute-start | bytes 98312 | tf_op jit(solution)/shard_map/ppermute | solution.py:70
  27.0 0.4 collective-permute-done.7
  27.4 0.5 collective-permute-done.8
  28.0 1.4 %collective-permute-done.9 = bf16[4,2,8,256]{3,2,1,0:T(8,128)(2,1)S(1)} collective-permute-done((bf16[4,2,8,256]{3,2,1,0:T(8,128)(2,1)S(1)}, bf16[4,2,8,256]{3,2,1,0:T(8,128)(2,1)S(1)}, u32[]{:S(2)}, u32[]{:S(2)}) %collective-permute-start.9) | collective-permute-done | bytes 32800 | tf_op jit(solution)/shard_map/ppermute | solution.py:70
  29.5 2.3 %collective-permute-start.11 = (bf16[4,2,8,256]{3,2,1,0:T(8,128)(2,1)S(1)}, bf16[4,2,8,256]{3,2,1,0:T(8,128)(2,1)S(1)}, u32[]{:S(2)}, u32[]{:S(2)}) collective-permute-start(bf16[4,2,8,256]{3,2,1,0:T(8,128)(2,1)S(1)} %bitcast.72), channel_id=1, source_target_pairs={{0,16},{1,17},{2,18},{3,19},{4,20},{5,21},{6,22},{7,23},{8,24},{9,... | collective-permute-start | bytes 98312 | tf_op jit(solution)/shard_map/ppermute | solution.py:70
  31.9 2.0 %collective-permute-start.12 = (bf16[4,2,8,256]{3,2,1,0:T(8,128)(2,1)S(1)}, bf16[4,2,8,256]{3,2,1,0:T(8,128)(2,1)S(1)}, u32[]{:S(2)}, u32[]{:S(2)}) collective-permute-start(bf16[4,2,8,256]{3,2,1,0:T(8,128)(2,1)S(1)} %bitcast.71), channel_id=1, source_target_pairs={{0,24},{1,25},{2,26},{3,27},{4,28},{5,29},{6,30},{7,31},{8,16},{9,... | collective-permute-start | bytes 98312 | tf_op jit(solution)/shard_map/ppermute | solution.py:70
  34.0 0.8 shard_map.233
  34.8 2.8 %collective-permute-done.12.refs_3_ = bf16[4,2,8,256]{3,2,1,0:T(8,128)(2,1)S(1)} collective-permute-done((bf16[4,2,8,256]{3,2,1,0:T(8,128)(2,1)S(1)}, bf16[4,2,8,256]{3,2,1,0:T(8,128)(2,1)S(1)}, u32[]{:S(2)}, u32[]{:S(2)}) %collective-permute-start.12) | collective-permute-done | bytes 32800 | tf_op jit(solution)/shard_map/ppermute | solution.py:70
  37.6 1.9 %shard_map.237 = (bf16[16,1024]{1,0:T(8,128)(2,1)S(1)}, f32[128,128]{1,0:T(8,128)S(1)}, f32[128,128]{1,0:T(8,128)S(1)}, f32[128,128]{1,0:T(8,128)S(1)}) custom-call(s32[2]{0:T(128)S(1)} %pad_add_fusion.after.where, bf16[4,2,8,256]{3,2,1,0:T(8,128)(2,1)S(1)} %bitcast.51, bf16[4,2,8,256]{3,2,1,0:T(8,128)(2,1)S(1)} %collective-permute-done.10.refs_1_, ...), custom_call_target="tpu_custom_call" | custom-call | tf_op jit(solution)/shard_map/pallas_call | solution.py:35
  39.5 2.1 %collective-permute-start.15 = (bf16[1,16,1024]{2,1,0:T(8,128)(2,1)S(1)}, bf16[1,16,1024]{2,1,0:T(8,128)(2,1)S(1)}, u32[]{:S(2)}, u32[]{:S(2)}) collective-permute-start(bf16[1,16,1024]{2,1,0:T(8,128)(2,1)S(1)} %bitcast.58), channel_id=1, source_target_pairs={{0,24},{1,25},{2,26},{3,27},{4,28},{5,29},{6,30},{7,31},{8,16},{9,... | collective-permute-start | bytes 98312 | tf_op jit(solution)/shard_map/ppermute | solution.py:70
  41.6 2.4 %collective-permute-start.13 = (bf16[1,16,1024]{2,1,0:T(8,128)(2,1)S(1)}, bf16[1,16,1024]{2,1,0:T(8,128)(2,1)S(1)}, u32[]{:S(2)}, u32[]{:S(2)}) collective-permute-start(bf16[1,16,1024]{2,1,0:T(8,128)(2,1)S(1)} %bitcast.60), channel_id=1, source_target_pairs={{0,8},{1,9},{2,10},{3,11},{4,12},{5,13},{6,14},{7,15},{8,0},{9,1},... | collective-permute-start | bytes 98312 | tf_op jit(solution)/shard_map/ppermute | solution.py:70
  44.0 1.3 %collective-permute-done.15 = bf16[1,16,1024]{2,1,0:T(8,128)(2,1)S(1)} collective-permute-done((bf16[1,16,1024]{2,1,0:T(8,128)(2,1)S(1)}, bf16[1,16,1024]{2,1,0:T(8,128)(2,1)S(1)}, u32[]{:S(2)}, u32[]{:S(2)}) %collective-permute-start.15) | collective-permute-done | bytes 32800 | tf_op jit(solution)/shard_map/ppermute | solution.py:70
  45.3 1.1 %collective-permute-done.14 = bf16[1,16,1024]{2,1,0:T(8,128)(2,1)S(1)} collective-permute-done((bf16[1,16,1024]{2,1,0:T(8,128)(2,1)S(1)}, bf16[1,16,1024]{2,1,0:T(8,128)(2,1)S(1)}, u32[]{:S(2)}, u32[]{:S(2)}) %collective-permute-start.14) | collective-permute-done | bytes 32800 | tf_op jit(solution)/shard_map/ppermute | solution.py:70
  46.4 2.0 %collective-permute-start.16 = (bf16[4,16,1024]{2,1,0:T(8,128)(2,1)S(1)}, bf16[4,16,1024]{2,1,0:T(8,128)(2,1)S(1)}, u32[]{:S(2)}, u32[]{:S(2)}) collective-permute-start(bf16[4,16,1024]{2,1,0:T(8,128)(2,1)S(1)} %pad_maximum_fusion.1.refs_0_.after), channel_id=1, source_target_pairs={{0,2},{1,3},{2,0},{3,1},{4,6},{5,7},{6,4},{7,5},{8,10},{9,11},{10,... | collective-permute-start | bytes 393224 | tf_op jit(solution)/shard_map/ppermute | solution.py:70
  48.4 1.0 %collective-permute-start.17 = (bf16[4,16,1024]{2,1,0:T(8,128)(2,1)S(1)}, bf16[4,16,1024]{2,1,0:T(8,128)(2,1)S(1)}, u32[]{:S(2)}, u32[]{:S(2)}) collective-permute-start(bf16[4,16,1024]{2,1,0:T(8,128)(2,1)S(1)} %pad_maximum_fusion.1.refs_0_.after), channel_id=1, source_target_pairs={{0,4},{1,5},{2,6},{3,7},{4,0},{5,1},{6,2},{7,3},{8,12},{9,13},{10,... | collective-permute-start | bytes 393224 | tf_op jit(solution)/shard_map/ppermute | solution.py:70
  49.4 0.5 collective-permute-start.18
  50.0 1.5 %collective-permute-done.16.refs_1_ = bf16[4,16,1024]{2,1,0:T(8,128)(2,1)S(1)} collective-permute-done((bf16[4,16,1024]{2,1,0:T(8,128)(2,1)S(1)}, bf16[4,16,1024]{2,1,0:T(8,128)(2,1)S(1)}, u32[]{:S(2)}, u32[]{:S(2)}) %collective-permute-start.16) | collective-permute-done | bytes 131104 | tf_op jit(solution)/shard_map/ppermute | solution.py:70
  51.5 1.9 %collective-permute-done.17.refs_2_ = bf16[4,16,1024]{2,1,0:T(8,128)(2,1)S(1)} collective-permute-done((bf16[4,16,1024]{2,1,0:T(8,128)(2,1)S(1)}, bf16[4,16,1024]{2,1,0:T(8,128)(2,1)S(1)}, u32[]{:S(2)}, u32[]{:S(2)}) %collective-permute-start.17) | collective-permute-done | bytes 131104 | tf_op jit(solution)/shard_map/ppermute | solution.py:70
  53.4 1.9 %collective-permute-done.18.refs_3_ = bf16[4,16,1024]{2,1,0:T(8,128)(2,1)S(1)} collective-permute-done((bf16[4,16,1024]{2,1,0:T(8,128)(2,1)S(1)}, bf16[4,16,1024]{2,1,0:T(8,128)(2,1)S(1)}, u32[]{:S(2)}, u32[]{:S(2)}) %collective-permute-start.18) | collective-permute-done | bytes 131104 | tf_op jit(solution)/shard_map/ppermute | solution.py:70
  55.3 0.8 shard_map.238
  56.2 1.2 %collective-permute-done.19.other = bf16[16,8,128]{2,1,0:T(8,128)(2,1)S(1)} collective-permute-done((bf16[16,8,128]{2,1,0:T(8,128)(2,1)S(1)}, bf16[16,8,128]{2,1,0:T(8,128)(2,1)S(1)}, u32[]{:S(2)}, u32[]{:S(2)}) %collective-permute-start.19) | collective-permute-done | bytes 32800 | tf_op jit(solution)/shard_map/ppermute | solution.py:70
  57.4 1.9 %collective-permute-start.22 = (bf16[1,128,128]{2,1,0:T(8,128)(2,1)S(1)}, bf16[1,128,128]{2,1,0:T(8,128)(2,1)S(1)}, u32[]{:S(2)}, u32[]{:S(2)}) collective-permute-start(bf16[1,128,128]{2,1,0:T(8,128)(2,1)S(1)} %bitcast.47), channel_id=1, source_target_pairs={{0,24},{1,25},{2,26},{3,27},{4,28},{5,29},{6,30},{7,31},{8,16},{9,... | collective-permute-start | bytes 98312 | tf_op jit(solution)/shard_map/ppermute | solution.py:70
  59.3 1.0 %collective-permute-start.21 = (bf16[1,128,128]{2,1,0:T(8,128)(2,1)S(1)}, bf16[1,128,128]{2,1,0:T(8,128)(2,1)S(1)}, u32[]{:S(2)}, u32[]{:S(2)}) collective-permute-start(bf16[1,128,128]{2,1,0:T(8,128)(2,1)S(1)} %bitcast.48), channel_id=1, source_target_pairs={{0,16},{1,17},{2,18},{3,19},{4,20},{5,21},{6,22},{7,23},{8,24},{9,... | collective-permute-start | bytes 98312 | tf_op jit(solution)/shard_map/ppermute | solution.py:70
  60.4 1.5 %collective-permute-start.20 = (bf16[1,128,128]{2,1,0:T(8,128)(2,1)S(1)}, bf16[1,128,128]{2,1,0:T(8,128)(2,1)S(1)}, u32[]{:S(2)}, u32[]{:S(2)}) collective-permute-start(bf16[1,128,128]{2,1,0:T(8,128)(2,1)S(1)} %bitcast.49), channel_id=1, source_target_pairs={{0,8},{1,9},{2,10},{3,11},{4,12},{5,13},{6,14},{7,15},{8,0},{9,1},... | collective-permute-start | bytes 98312 | tf_op jit(solution)/shard_map/ppermute | solution.py:70
  61.9 1.6 %collective-permute-done.22 = bf16[1,128,128]{2,1,0:T(8,128)(2,1)S(1)} collective-permute-done((bf16[1,128,128]{2,1,0:T(8,128)(2,1)S(1)}, bf16[1,128,128]{2,1,0:T(8,128)(2,1)S(1)}, u32[]{:S(2)}, u32[]{:S(2)}) %collective-permute-start.22) | collective-permute-done | bytes 32800 | tf_op jit(solution)/shard_map/ppermute | solution.py:70
  63.5 0.8 collective-permute-done.21
  64.3 0.2 collective-permute-done.20
  64.5 0.6 collective-permute-start.23
  65.1 0.6 collective-permute-start.24
  65.7 2.4 %collective-permute-start.25 = (bf16[4,128,128]{2,1,0:T(8,128)(2,1)S(1)}, bf16[4,128,128]{2,1,0:T(8,128)(2,1)S(1)}, u32[]{:S(2)}, u32[]{:S(2)}) collective-permute-start(bf16[4,128,128]{2,1,0:T(8,128)(2,1)S(1)} %pad_maximum_fusion.2.refs_0_), channel_id=1, source_target_pairs={{0,6},{1,7},{2,4},{3,5},{4,2},{5,3},{6,0},{7,1},{8,14},{9,15},{10,... | collective-permute-start | bytes 393224 | tf_op jit(solution)/shard_map/ppermute | solution.py:70
  68.1 2.5 %collective-permute-done.23.refs_1_ = bf16[4,128,128]{2,1,0:T(8,128)(2,1)S(1)} collective-permute-done((bf16[4,128,128]{2,1,0:T(8,128)(2,1)S(1)}, bf16[4,128,128]{2,1,0:T(8,128)(2,1)S(1)}, u32[]{:S(2)}, u32[]{:S(2)}) %collective-permute-start.23) | collective-permute-done | bytes 131104 | tf_op jit(solution)/shard_map/ppermute | solution.py:70
  70.6 0.4 collective-permute-done.24.refs_2_
  71.0 1.4 %collective-permute-done.25.refs_3_ = bf16[4,128,128]{2,1,0:T(8,128)(2,1)S(1)} collective-permute-done((bf16[4,128,128]{2,1,0:T(8,128)(2,1)S(1)}, bf16[4,128,128]{2,1,0:T(8,128)(2,1)S(1)}, u32[]{:S(2)}, u32[]{:S(2)}) %collective-permute-start.25) | collective-permute-done | bytes 131104 | tf_op jit(solution)/shard_map/ppermute | solution.py:70
  72.4 1.0 %shard_map.240 = (bf16[128,2048]{1,0:T(8,128)(2,1)S(1)}, f32[8,2048]{1,0:T(8,128)S(1)}) custom-call(s32[2]{0:T(128)S(1)} %pad_add_fusion.after.where, bf16[16,8,2048]{2,1,0:T(8,128)(2,1)S(1)} %get-tuple-element.41.tokens, bf16[4,128,128]{2,1,0:T(8,128)(2,1)S(1)} %pad_maximum_fusion.2.refs_0_, bf16[4,128,128]{2,1,0:T(8,128)(2,1)S(1)} %collective-permute-done.23.refs_1_, ...), custom_call_target="tpu_custom_call" | custom-call | tf_op jit(solution)/shard_map/pallas_call | solution.py:35
  73.6 1.9 %collective-permute-done.26.rows_in = bf16[128,2048]{1,0:T(8,128)(2,1)S(1)} collective-permute-done((bf16[128,2048]{1,0:T(8,128)(2,1)S(1)}, bf16[128,2048]{1,0:T(8,128)(2,1)S(1)}, u32[]{:S(2)}, u32[]{:S(2)}) %collective-permute-start.26) | collective-permute-done | bytes 524320 | tf_op jit(solution)/shard_map/ppermute | solution.py:70
  75.5 1.6 %shard_map.242 = bf16[128,2048]{1,0:T(8,128)(2,1)S(1)} custom-call(bf16[128,2048]{1,0:T(8,128)(2,1)S(1)} %collective-permute-done.26.rows_in, f32[128,1]{1,0:T(8,128)S(1)} %get-tuple-element.60.route, bf16[1,2048]{1,0:T(2,128)(2,1)S(1)} %broadcast_in_dim.39.mix, bf16[2048,128]{1,0:T(8,128)(2,1)S(1)} %copy-done.3, bf16[2048,128]{1,0:T(8,128)(2,1)S(1)} %copy-done.4, ...), custom_call_target="tpu_custom_call" | custom-call | tf_op jit(solution)/shard_map/pallas_call | solution.py:35
  77.3 1.6 %shard_map.241.own = f32[128,2048]{1,0:T(8,128)S(1)} custom-call(bf16[128,2048]{1,0:T(8,128)(2,1)S(1)} %get-tuple-element.58.rows_in, f32[128,1]{1,0:T(8,128)S(1)} %get-tuple-element.59.route, bf16[1,2048]{1,0:T(2,128)(2,1)S(1)} %broadcast_in_dim.39.mix, bf16[2048,128]{1,0:T(8,128)(2,1)S(1)} %copy-done.3, bf16[2048,128]{1,0:T(8,128)(2,1)S(1)} %copy-done.4, ...), custom_call_target="tpu_custom_call" | custom-call | tf_op jit(solution)/shard_map/pallas_call | solution.py:35
  79.1 0.6 shard_map.243
  79.7 1.8 %collective-permute-start.28 = (bf16[4,8,2048]{2,1,0:T(8,128)(2,1)S(1)}, bf16[4,8,2048]{2,1,0:T(8,128)(2,1)S(1)}, u32[]{:S(2)}, u32[]{:S(2)}) collective-permute-start(bf16[4,8,2048]{2,1,0:T(8,128)(2,1)S(1)} %get-tuple-element.62), channel_id=1, source_target_pairs={{0,2},{1,3},{2,0},{3,1},{4,6},{5,7},{6,4},{7,5},{8,10},{9,11},{10,... | collective-permute-start | bytes 393224 | tf_op jit(solution)/shard_map/ppermute | solution.py:70
  81.5 1.0 %collective-permute-start.29 = (bf16[4,8,2048]{2,1,0:T(8,128)(2,1)S(1)}, bf16[4,8,2048]{2,1,0:T(8,128)(2,1)S(1)}, u32[]{:S(2)}, u32[]{:S(2)}) collective-permute-start(bf16[4,8,2048]{2,1,0:T(8,128)(2,1)S(1)} %get-tuple-element.63), channel_id=1, source_target_pairs={{0,4},{1,5},{2,6},{3,7},{4,0},{5,1},{6,2},{7,3},{8,12},{9,13},{10,... | collective-permute-start | bytes 393224 | tf_op jit(solution)/shard_map/ppermute | solution.py:70
  82.5 0.8 collective-permute-start.30
  83.2 2.3 %collective-permute-done.28.refs_1_ = bf16[4,8,2048]{2,1,0:T(8,128)(2,1)S(1)} collective-permute-done((bf16[4,8,2048]{2,1,0:T(8,128)(2,1)S(1)}, bf16[4,8,2048]{2,1,0:T(8,128)(2,1)S(1)}, u32[]{:S(2)}, u32[]{:S(2)}) %collective-permute-start.28) | collective-permute-done | bytes 131104 | tf_op jit(solution)/shard_map/ppermute | solution.py:70
  85.5 4.1 %collective-permute-done.29.refs_2_ = bf16[4,8,2048]{2,1,0:T(8,128)(2,1)S(1)} collective-permute-done((bf16[4,8,2048]{2,1,0:T(8,128)(2,1)S(1)}, bf16[4,8,2048]{2,1,0:T(8,128)(2,1)S(1)}, u32[]{:S(2)}, u32[]{:S(2)}) %collective-permute-start.29) | collective-permute-done | bytes 131104 | tf_op jit(solution)/shard_map/ppermute | solution.py:70
  89.7 1.3 %collective-permute-start.31 = (bf16[8,2048]{1,0:T(8,128)(2,1)S(1)}, bf16[8,2048]{1,0:T(8,128)(2,1)S(1)}, u32[]{:S(2)}, u32[]{:S(2)}) collective-permute-start(bf16[8,2048]{1,0:T(8,128)(2,1)S(1)} %get-tuple-element.66), channel_id=1, source_target_pairs={{0,8},{1,9},{2,10},{3,11},{4,12},{5,13},{6,14},{7,15},{8,0},{9,1},... | collective-permute-start | bytes 98312 | tf_op jit(solution)/shard_map/ppermute | solution.py:70
  91.0 1.4 %collective-permute-start.32 = (bf16[8,2048]{1,0:T(8,128)(2,1)S(1)}, bf16[8,2048]{1,0:T(8,128)(2,1)S(1)}, u32[]{:S(2)}, u32[]{:S(2)}) collective-permute-start(bf16[8,2048]{1,0:T(8,128)(2,1)S(1)} %get-tuple-element.67), channel_id=1, source_target_pairs={{0,16},{1,17},{2,18},{3,19},{4,20},{5,21},{6,22},{7,23},{8,24},{9,... | collective-permute-start | bytes 98312 | tf_op jit(solution)/shard_map/ppermute | solution.py:70
  92.4 1.8 %collective-permute-start.33 = (bf16[8,2048]{1,0:T(8,128)(2,1)S(1)}, bf16[8,2048]{1,0:T(8,128)(2,1)S(1)}, u32[]{:S(2)}, u32[]{:S(2)}) collective-permute-start(bf16[8,2048]{1,0:T(8,128)(2,1)S(1)} %get-tuple-element.68), channel_id=1, source_target_pairs={{0,24},{1,25},{2,26},{3,27},{4,28},{5,29},{6,30},{7,31},{8,16},{9,... | collective-permute-start | bytes 98312 | tf_op jit(solution)/shard_map/ppermute | solution.py:70
  94.1 3.9 %shard_map.246 = f32[16,8,128,128]{3,2,1,0:T(8,128)} custom-call(f32[128,128]{1,0:T(8,128)S(1)} %get-tuple-element.69.k_in, f32[128,128]{1,0:T(8,128)S(1)} %get-tuple-element.70.keep, f32[128,128]{1,0:T(8,128)S(1)} %get-tuple-element.71.change, f32[5,1024,128]{2,1,0:T(8,128)S(1)} %get-tuple-element.72.near, ...), custom_call_target="tpu_custom_call" | custom-call | tf_op jit(solution)/shard_map/pallas_call | solution.py:35
  98.1 0.6 shard_map.245
  (58 shorter events, 1.1 us)
Async XLA Ops:
  0.6 7.6 %collective-permute-start.2 = (bf16[1,8,2048]{2,1,0:T(8,128)(2,1)}, bf16[1,8,2048]{2,1,0:T(8,128)(2,1)S(1)}, u32[]{:S(2)}, u32[]{:S(2)}) collective-permute-start(bf16[1,8,2048]{2,1,0:T(8,128)(2,1)} %bitcast.80), channel_id=1, source_target_pairs={{0,24},{1,25},{2,26},{3,27},{4,28},{5,29},{6,30},{7,31},{8,16},{9,... | collective-permute-start | bytes 98312 | tf_op jit(solution)/shard_map/ppermute | solution.py:70
  5.8 5.0 %collective-permute-start.1 = (bf16[1,8,2048]{2,1,0:T(8,128)(2,1)}, bf16[1,8,2048]{2,1,0:T(8,128)(2,1)S(1)}, u32[]{:S(2)}, u32[]{:S(2)}) collective-permute-start(bf16[1,8,2048]{2,1,0:T(8,128)(2,1)} %bitcast.81), channel_id=1, source_target_pairs={{0,16},{1,17},{2,18},{3,19},{4,20},{5,21},{6,22},{7,23},{8,24},{9,... | collective-permute-start | bytes 98312 | tf_op jit(solution)/shard_map/ppermute | solution.py:70
  5.8 5.0 %collective-permute-start = (bf16[1,8,2048]{2,1,0:T(8,128)(2,1)}, bf16[1,8,2048]{2,1,0:T(8,128)(2,1)S(1)}, u32[]{:S(2)}, u32[]{:S(2)}) collective-permute-start(bf16[1,8,2048]{2,1,0:T(8,128)(2,1)} %bitcast.82), channel_id=1, source_target_pairs={{0,8},{1,9},{2,10},{3,11},{4,12},{5,13},{6,14},{7,15},{8,0},{9,1},... | collective-permute-start | bytes 98312 | tf_op jit(solution)/shard_map/ppermute | solution.py:70
  10.8 7.0 %collective-permute-start.3 = (bf16[4,8,2048]{2,1,0:T(8,128)(2,1)S(1)}, bf16[4,8,2048]{2,1,0:T(8,128)(2,1)S(1)}, u32[]{:S(2)}, u32[]{:S(2)}) collective-permute-start(bf16[4,8,2048]{2,1,0:T(8,128)(2,1)S(1)} %pad_maximum_fusion.after.refs_0_), channel_id=1, source_target_pairs={{0,2},{1,3},{2,0},{3,1},{4,6},{5,7},{6,4},{7,5},{8,10},{9,11},{10,... | collective-permute-start | bytes 393224 | tf_op jit(solution)/shard_map/ppermute | solution.py:70
  12.4 5.9 %collective-permute-start.4 = (bf16[4,8,2048]{2,1,0:T(8,128)(2,1)S(1)}, bf16[4,8,2048]{2,1,0:T(8,128)(2,1)S(1)}, u32[]{:S(2)}, u32[]{:S(2)}) collective-permute-start(bf16[4,8,2048]{2,1,0:T(8,128)(2,1)S(1)} %pad_maximum_fusion.after.refs_0_), channel_id=1, source_target_pairs={{0,4},{1,5},{2,6},{3,7},{4,0},{5,1},{6,2},{7,3},{8,12},{9,13},{10,... | collective-permute-start | bytes 393224 | tf_op jit(solution)/shard_map/ppermute | solution.py:70
  13.9 5.9 %collective-permute-start.5 = (bf16[4,8,2048]{2,1,0:T(8,128)(2,1)S(1)}, bf16[4,8,2048]{2,1,0:T(8,128)(2,1)S(1)}, u32[]{:S(2)}, u32[]{:S(2)}) collective-permute-start(bf16[4,8,2048]{2,1,0:T(8,128)(2,1)S(1)} %pad_maximum_fusion.after.refs_0_), channel_id=1, source_target_pairs={{0,6},{1,7},{2,4},{3,5},{4,2},{5,3},{6,0},{7,1},{8,14},{9,15},{10,... | collective-permute-start | bytes 393224 | tf_op jit(solution)/shard_map/ppermute | solution.py:70
  19.8 14.1 %copy-start.7 = (bf16[2048,8]{0,1:T(8,128)(2,1)S(1)}, bf16[2048,8]{0,1:T(8,128)(2,1)}, u32[]{:S(2)}) copy-start(bf16[2048,8]{0,1:T(8,128)(2,1)} %param.29) | copy-start | bytes 98308
  19.8 14.1 %copy-start.8 = (bf16[2048,8]{0,1:T(8,128)(2,1)S(1)}, bf16[2048,8]{0,1:T(8,128)(2,1)}, u32[]{:S(2)}) copy-start(bf16[2048,8]{0,1:T(8,128)(2,1)} %param.30) | copy-start | bytes 98308
  19.8 14.1 %copy-start.10 = (s32[256,4]{0,1:T(4,128)S(1)}, s32[256,4]{0,1:T(4,128)}, u32[]{:S(2)}) copy-start(s32[256,4]{0,1:T(4,128)} %param.44) | copy-start | bytes 12292
  19.8 14.1 %copy-start.11 = (f32[256,4]{0,1:T(4,128)S(1)}, f32[256,4]{0,1:T(4,128)}, u32[]{:S(2)}) copy-start(f32[256,4]{0,1:T(4,128)} %param.45) | copy-start | bytes 12292
  19.8 14.1 %copy-start.12 = (f32[8]{0:T(128)S(1)}, f32[8]{0:T(128)}, u32[]{:S(2)}) copy-start(f32[8]{0:T(128)} %param.31) | copy-start | bytes 100
  19.8 14.1 %copy-start.13 = (f32[8]{0:T(128)S(1)}, f32[8]{0:T(128)}, u32[]{:S(2)}) copy-start(f32[8]{0:T(128)} %param.32) | copy-start | bytes 100
  20.6 17.0 %copy-start.14 = (f32[128]{0:T(128)S(1)}, f32[128]{0:T(128)}, u32[]{:S(2)}) copy-start(f32[128]{0:T(128)} %param.33) | copy-start | bytes 1540
  20.6 2.0 %collective-permute-start.6 = (bf16[16,8,2048]{2,1,0:T(8,128)(2,1)S(1)}, bf16[16,8,2048]{2,1,0:T(8,128)(2,1)S(1)}, u32[]{:S(2)}, u32[]{:S(2)}) collective-permute-start(bf16[16,8,2048]{2,1,0:T(8,128)(2,1)S(1)} %shard_map.232.own.x_ref), channel_id=1, source_target_pairs={{0,1},{1,0},{2,3},{3,2},{4,5},{5,4},{6,7},{7,6},{8,9},{9,8},{10,11... | collective-permute-start | bytes 1572872 | tf_op jit(solution)/shard_map/ppermute | solution.py:70
  23.4 4.0 %collective-permute-start.7 = (bf16[4,2,8,256]{3,2,1,0:T(8,128)(2,1)S(1)}, bf16[4,2,8,256]{3,2,1,0:T(8,128)(2,1)S(1)}, u32[]{:S(2)}, u32[]{:S(2)}) collective-permute-start(bf16[4,2,8,256]{3,2,1,0:T(8,128)(2,1)S(1)} %get-tuple-element.43), channel_id=1, source_target_pairs={{0,2},{1,3},{2,0},{3,1},{4,6},{5,7},{6,4},{7,5},{8,10},{9,11},{10,... | collective-permute-start | bytes 98312 | tf_op jit(solution)/shard_map/ppermute | solution.py:70
  24.0 3.9 %collective-permute-start.8 = (bf16[4,2,8,256]{3,2,1,0:T(8,128)(2,1)S(1)}, bf16[4,2,8,256]{3,2,1,0:T(8,128)(2,1)S(1)}, u32[]{:S(2)}, u32[]{:S(2)}) collective-permute-start(bf16[4,2,8,256]{3,2,1,0:T(8,128)(2,1)S(1)} %get-tuple-element.44), channel_id=1, source_target_pairs={{0,4},{1,5},{2,6},{3,7},{4,0},{5,1},{6,2},{7,3},{8,12},{9,13},{10,... | collective-permute-start | bytes 98312 | tf_op jit(solution)/shard_map/ppermute | solution.py:70
  24.6 4.8 %collective-permute-start.9 = (bf16[4,2,8,256]{3,2,1,0:T(8,128)(2,1)S(1)}, bf16[4,2,8,256]{3,2,1,0:T(8,128)(2,1)S(1)}, u32[]{:S(2)}, u32[]{:S(2)}) collective-permute-start(bf16[4,2,8,256]{3,2,1,0:T(8,128)(2,1)S(1)} %get-tuple-element.45), channel_id=1, source_target_pairs={{0,6},{1,7},{2,4},{3,5},{4,2},{5,3},{6,0},{7,1},{8,14},{9,15},{10,... | collective-permute-start | bytes 98312 | tf_op jit(solution)/shard_map/ppermute | solution.py:70
  29.4 5.4 %collective-permute-start.10 = (bf16[4,2,8,256]{3,2,1,0:T(8,128)(2,1)S(1)}, bf16[4,2,8,256]{3,2,1,0:T(8,128)(2,1)S(1)}, u32[]{:S(2)}, u32[]{:S(2)}) collective-permute-start(bf16[4,2,8,256]{3,2,1,0:T(8,128)(2,1)S(1)} %bitcast.73), channel_id=1, source_target_pairs={{0,8},{1,9},{2,10},{3,11},{4,12},{5,13},{6,14},{7,15},{8,0},{9,1},... | collective-permute-start | bytes 98312 | tf_op jit(solution)/shard_map/ppermute | solution.py:70
  29.5 5.3 %collective-permute-start.11 = (bf16[4,2,8,256]{3,2,1,0:T(8,128)(2,1)S(1)}, bf16[4,2,8,256]{3,2,1,0:T(8,128)(2,1)S(1)}, u32[]{:S(2)}, u32[]{:S(2)}) collective-permute-start(bf16[4,2,8,256]{3,2,1,0:T(8,128)(2,1)S(1)} %bitcast.72), channel_id=1, source_target_pairs={{0,16},{1,17},{2,18},{3,19},{4,20},{5,21},{6,22},{7,23},{8,24},{9,... | collective-permute-start | bytes 98312 | tf_op jit(solution)/shard_map/ppermute | solution.py:70
  31.9 5.7 %collective-permute-start.12 = (bf16[4,2,8,256]{3,2,1,0:T(8,128)(2,1)S(1)}, bf16[4,2,8,256]{3,2,1,0:T(8,128)(2,1)S(1)}, u32[]{:S(2)}, u32[]{:S(2)}) collective-permute-start(bf16[4,2,8,256]{3,2,1,0:T(8,128)(2,1)S(1)} %bitcast.71), channel_id=1, source_target_pairs={{0,24},{1,25},{2,26},{3,27},{4,28},{5,29},{6,30},{7,31},{8,16},{9,... | collective-permute-start | bytes 98312 | tf_op jit(solution)/shard_map/ppermute | solution.py:70
  33.9 21.4 %copy-start.6 = (bf16[1024,128]{1,0:T(8,128)(2,1)S(1)}, bf16[1024,128]{1,0:T(8,128)(2,1)}, u32[]{:S(2)}) copy-start(bf16[1024,128]{1,0:T(8,128)(2,1)} %refs_4_.1) | copy-start | bytes 786436
  33.9 38.5 %copy-start.9 = (f32[2048]{0:T(1024)S(1)}, f32[2048]{0:T(1024)}, u32[]{:S(2)}) copy-start(f32[2048]{0:T(1024)} %param.36) | copy-start | bytes 24580
  33.9 41.5 %copy-start.4 = (bf16[2048,128]{1,0:T(8,128)(2,1)S(1)}, bf16[2048,128]{1,0:T(8,128)(2,1)}, u32[]{:S(2)}) copy-start(bf16[2048,128]{1,0:T(8,128)(2,1)} %d_up.3) | copy-start | bytes 1572868
  33.9 41.5 %copy-start.5 = (bf16[128,2048]{1,0:T(8,128)(2,1)S(1)}, bf16[128,2048]{1,0:T(8,128)(2,1)}, u32[]{:S(2)}) copy-start(bf16[128,2048]{1,0:T(8,128)(2,1)} %d_down.3) | copy-start | bytes 1572868
  37.6 36.0 %copy-start.15 = (bf16[2048]{0:T(1024)(128)(2,1)S(1)}, bf16[2048]{0:T(1024)(128)(2,1)}, u32[]{:S(2)}) copy-start(bf16[2048]{0:T(1024)(128)(2,1)} %param.37) | copy-start | bytes 12292
  37.6 37.9 %copy-start = (bf16[1,2048,512]{2,1,0:T(8,128)(2,1)S(1)}, bf16[1,2048,512]{2,1,0:T(8,128)(2,1)}, u32[]{:S(2)}) copy-start(bf16[1,2048,512]{2,1,0:T(8,128)(2,1)} %param.41) | copy-start | bytes 6291460
  37.6 37.9 %copy-start.1 = (bf16[1,2048,512]{2,1,0:T(8,128)(2,1)S(1)}, bf16[1,2048,512]{2,1,0:T(8,128)(2,1)}, u32[]{:S(2)}) copy-start(bf16[1,2048,512]{2,1,0:T(8,128)(2,1)} %param.42) | copy-start | bytes 6291460
  37.6 37.9 %copy-start.2 = (bf16[1,512,2048]{2,1,0:T(8,128)(2,1)S(1)}, bf16[1,512,2048]{2,1,0:T(8,128)(2,1)}, u32[]{:S(2)}) copy-start(bf16[1,512,2048]{2,1,0:T(8,128)(2,1)} %param.43) | copy-start | bytes 6291460
  37.6 37.9 %copy-start.3 = (bf16[2048,128]{1,0:T(8,128)(2,1)S(1)}, bf16[2048,128]{1,0:T(8,128)(2,1)}, u32[]{:S(2)}) copy-start(bf16[2048,128]{1,0:T(8,128)(2,1)} %d_gate.3) | copy-start | bytes 1572868
  39.5 5.8 %collective-permute-start.15 = (bf16[1,16,1024]{2,1,0:T(8,128)(2,1)S(1)}, bf16[1,16,1024]{2,1,0:T(8,128)(2,1)S(1)}, u32[]{:S(2)}, u32[]{:S(2)}) collective-permute-start(bf16[1,16,1024]{2,1,0:T(8,128)(2,1)S(1)} %bitcast.58), channel_id=1, source_target_pairs={{0,24},{1,25},{2,26},{3,27},{4,28},{5,29},{6,30},{7,31},{8,16},{9,... | collective-permute-start | bytes 98312 | tf_op jit(solution)/shard_map/ppermute | solution.py:70
  41.6 4.8 %collective-permute-start.14 = (bf16[1,16,1024]{2,1,0:T(8,128)(2,1)S(1)}, bf16[1,16,1024]{2,1,0:T(8,128)(2,1)S(1)}, u32[]{:S(2)}, u32[]{:S(2)}) collective-permute-start(bf16[1,16,1024]{2,1,0:T(8,128)(2,1)S(1)} %bitcast.59), channel_id=1, source_target_pairs={{0,16},{1,17},{2,18},{3,19},{4,20},{5,21},{6,22},{7,23},{8,24},{9,... | collective-permute-start | bytes 98312 | tf_op jit(solution)/shard_map/ppermute | solution.py:70
  41.6 4.8 %collective-permute-start.13 = (bf16[1,16,1024]{2,1,0:T(8,128)(2,1)S(1)}, bf16[1,16,1024]{2,1,0:T(8,128)(2,1)S(1)}, u32[]{:S(2)}, u32[]{:S(2)}) collective-permute-start(bf16[1,16,1024]{2,1,0:T(8,128)(2,1)S(1)} %bitcast.60), channel_id=1, source_target_pairs={{0,8},{1,9},{2,10},{3,11},{4,12},{5,13},{6,14},{7,15},{8,0},{9,1},... | collective-permute-start | bytes 98312 | tf_op jit(solution)/shard_map/ppermute | solution.py:70
  46.4 5.0 %collective-permute-start.16 = (bf16[4,16,1024]{2,1,0:T(8,128)(2,1)S(1)}, bf16[4,16,1024]{2,1,0:T(8,128)(2,1)S(1)}, u32[]{:S(2)}, u32[]{:S(2)}) collective-permute-start(bf16[4,16,1024]{2,1,0:T(8,128)(2,1)S(1)} %pad_maximum_fusion.1.refs_0_.after), channel_id=1, source_target_pairs={{0,2},{1,3},{2,0},{3,1},{4,6},{5,7},{6,4},{7,5},{8,10},{9,11},{10,... | collective-permute-start | bytes 393224 | tf_op jit(solution)/shard_map/ppermute | solution.py:70
  48.4 5.0 %collective-permute-start.17 = (bf16[4,16,1024]{2,1,0:T(8,128)(2,1)S(1)}, bf16[4,16,1024]{2,1,0:T(8,128)(2,1)S(1)}, u32[]{:S(2)}, u32[]{:S(2)}) collective-permute-start(bf16[4,16,1024]{2,1,0:T(8,128)(2,1)S(1)} %pad_maximum_fusion.1.refs_0_.after), channel_id=1, source_target_pairs={{0,4},{1,5},{2,6},{3,7},{4,0},{5,1},{6,2},{7,3},{8,12},{9,13},{10,... | collective-permute-start | bytes 393224 | tf_op jit(solution)/shard_map/ppermute | solution.py:70
  49.4 5.9 %collective-permute-start.18 = (bf16[4,16,1024]{2,1,0:T(8,128)(2,1)S(1)}, bf16[4,16,1024]{2,1,0:T(8,128)(2,1)S(1)}, u32[]{:S(2)}, u32[]{:S(2)}) collective-permute-start(bf16[4,16,1024]{2,1,0:T(8,128)(2,1)S(1)} %pad_maximum_fusion.1.refs_0_.after), channel_id=1, source_target_pairs={{0,6},{1,7},{2,4},{3,5},{4,2},{5,3},{6,0},{7,1},{8,14},{9,15},{10,... | collective-permute-start | bytes 393224 | tf_op jit(solution)/shard_map/ppermute | solution.py:70
  56.2 1.3 %collective-permute-start.19 = (bf16[16,8,128]{2,1,0:T(8,128)(2,1)S(1)}, bf16[16,8,128]{2,1,0:T(8,128)(2,1)S(1)}, u32[]{:S(2)}, u32[]{:S(2)}) collective-permute-start(bf16[16,8,128]{2,1,0:T(8,128)(2,1)S(1)} %get-tuple-element.56), channel_id=1, source_target_pairs={{0,1},{1,0},{2,3},{3,2},{4,5},{5,4},{6,7},{7,6},{8,9},{9,8},{10,11... | collective-permute-start | bytes 98312 | tf_op jit(solution)/shard_map/ppermute | solution.py:70
  57.4 6.1 %collective-permute-start.22 = (bf16[1,128,128]{2,1,0:T(8,128)(2,1)S(1)}, bf16[1,128,128]{2,1,0:T(8,128)(2,1)S(1)}, u32[]{:S(2)}, u32[]{:S(2)}) collective-permute-start(bf16[1,128,128]{2,1,0:T(8,128)(2,1)S(1)} %bitcast.47), channel_id=1, source_target_pairs={{0,24},{1,25},{2,26},{3,27},{4,28},{5,29},{6,30},{7,31},{8,16},{9,... | collective-permute-start | bytes 98312 | tf_op jit(solution)/shard_map/ppermute | solution.py:70
  59.3 5.0 %collective-permute-start.21 = (bf16[1,128,128]{2,1,0:T(8,128)(2,1)S(1)}, bf16[1,128,128]{2,1,0:T(8,128)(2,1)S(1)}, u32[]{:S(2)}, u32[]{:S(2)}) collective-permute-start(bf16[1,128,128]{2,1,0:T(8,128)(2,1)S(1)} %bitcast.48), channel_id=1, source_target_pairs={{0,16},{1,17},{2,18},{3,19},{4,20},{5,21},{6,22},{7,23},{8,24},{9,... | collective-permute-start | bytes 98312 | tf_op jit(solution)/shard_map/ppermute | solution.py:70
  60.4 4.1 %collective-permute-start.20 = (bf16[1,128,128]{2,1,0:T(8,128)(2,1)S(1)}, bf16[1,128,128]{2,1,0:T(8,128)(2,1)S(1)}, u32[]{:S(2)}, u32[]{:S(2)}) collective-permute-start(bf16[1,128,128]{2,1,0:T(8,128)(2,1)S(1)} %bitcast.49), channel_id=1, source_target_pairs={{0,8},{1,9},{2,10},{3,11},{4,12},{5,13},{6,14},{7,15},{8,0},{9,1},... | collective-permute-start | bytes 98312 | tf_op jit(solution)/shard_map/ppermute | solution.py:70
  64.5 6.1 %collective-permute-start.23 = (bf16[4,128,128]{2,1,0:T(8,128)(2,1)S(1)}, bf16[4,128,128]{2,1,0:T(8,128)(2,1)S(1)}, u32[]{:S(2)}, u32[]{:S(2)}) collective-permute-start(bf16[4,128,128]{2,1,0:T(8,128)(2,1)S(1)} %pad_maximum_fusion.2.refs_0_), channel_id=1, source_target_pairs={{0,2},{1,3},{2,0},{3,1},{4,6},{5,7},{6,4},{7,5},{8,10},{9,11},{10,... | collective-permute-start | bytes 393224 | tf_op jit(solution)/shard_map/ppermute | solution.py:70
  65.1 5.9 %collective-permute-start.24 = (bf16[4,128,128]{2,1,0:T(8,128)(2,1)S(1)}, bf16[4,128,128]{2,1,0:T(8,128)(2,1)S(1)}, u32[]{:S(2)}, u32[]{:S(2)}) collective-permute-start(bf16[4,128,128]{2,1,0:T(8,128)(2,1)S(1)} %pad_maximum_fusion.2.refs_0_), channel_id=1, source_target_pairs={{0,4},{1,5},{2,6},{3,7},{4,0},{5,1},{6,2},{7,3},{8,12},{9,13},{10,... | collective-permute-start | bytes 393224 | tf_op jit(solution)/shard_map/ppermute | solution.py:70
  65.7 6.7 %collective-permute-start.25 = (bf16[4,128,128]{2,1,0:T(8,128)(2,1)S(1)}, bf16[4,128,128]{2,1,0:T(8,128)(2,1)S(1)}, u32[]{:S(2)}, u32[]{:S(2)}) collective-permute-start(bf16[4,128,128]{2,1,0:T(8,128)(2,1)S(1)} %pad_maximum_fusion.2.refs_0_), channel_id=1, source_target_pairs={{0,6},{1,7},{2,4},{3,5},{4,2},{5,3},{6,0},{7,1},{8,14},{9,15},{10,... | collective-permute-start | bytes 393224 | tf_op jit(solution)/shard_map/ppermute | solution.py:70
  73.5 2.0 %collective-permute-start.26 = (bf16[128,2048]{1,0:T(8,128)(2,1)S(1)}, bf16[128,2048]{1,0:T(8,128)(2,1)S(1)}, u32[]{:S(2)}, u32[]{:S(2)}) collective-permute-start(bf16[128,2048]{1,0:T(8,128)(2,1)S(1)} %get-tuple-element.58.rows_in), channel_id=1, source_target_pairs={{0,1},{1,0},{2,3},{3,2},{4,5},{5,4},{6,7},{7,6},{8,9},{9,8},{10,11... | collective-permute-start | bytes 1572872 | tf_op jit(solution)/shard_map/ppermute | solution.py:70
  77.1 2.0 %collective-permute-start.27 = (bf16[128,2048]{1,0:T(8,128)(2,1)S(1)}, bf16[128,2048]{1,0:T(8,128)(2,1)S(1)}, u32[]{:S(2)}, u32[]{:S(2)}) collective-permute-start(bf16[128,2048]{1,0:T(8,128)(2,1)S(1)} %shard_map.242), channel_id=1, source_target_pairs={{0,1},{1,0},{2,3},{3,2},{4,5},{5,4},{6,7},{7,6},{8,9},{9,8},{10,11... | collective-permute-start | bytes 1572872 | tf_op jit(solution)/shard_map/ppermute | solution.py:70
  79.7 5.8 %collective-permute-start.28 = (bf16[4,8,2048]{2,1,0:T(8,128)(2,1)S(1)}, bf16[4,8,2048]{2,1,0:T(8,128)(2,1)S(1)}, u32[]{:S(2)}, u32[]{:S(2)}) collective-permute-start(bf16[4,8,2048]{2,1,0:T(8,128)(2,1)S(1)} %get-tuple-element.62), channel_id=1, source_target_pairs={{0,2},{1,3},{2,0},{3,1},{4,6},{5,7},{6,4},{7,5},{8,10},{9,11},{10,... | collective-permute-start | bytes 393224 | tf_op jit(solution)/shard_map/ppermute | solution.py:70
  81.5 8.1 %collective-permute-start.29 = (bf16[4,8,2048]{2,1,0:T(8,128)(2,1)S(1)}, bf16[4,8,2048]{2,1,0:T(8,128)(2,1)S(1)}, u32[]{:S(2)}, u32[]{:S(2)}) collective-permute-start(bf16[4,8,2048]{2,1,0:T(8,128)(2,1)S(1)} %get-tuple-element.63), channel_id=1, source_target_pairs={{0,4},{1,5},{2,6},{3,7},{4,0},{5,1},{6,2},{7,3},{8,12},{9,13},{10,... | collective-permute-start | bytes 393224 | tf_op jit(solution)/shard_map/ppermute | solution.py:70
  82.5 7.1 %collective-permute-start.30 = (bf16[4,8,2048]{2,1,0:T(8,128)(2,1)S(1)}, bf16[4,8,2048]{2,1,0:T(8,128)(2,1)S(1)}, u32[]{:S(2)}, u32[]{:S(2)}) collective-permute-start(bf16[4,8,2048]{2,1,0:T(8,128)(2,1)S(1)} %get-tuple-element.64), channel_id=1, source_target_pairs={{0,6},{1,7},{2,4},{3,5},{4,2},{5,3},{6,0},{7,1},{8,14},{9,15},{10,... | collective-permute-start | bytes 393224 | tf_op jit(solution)/shard_map/ppermute | solution.py:70
  89.7 8.3 %collective-permute-start.31 = (bf16[8,2048]{1,0:T(8,128)(2,1)S(1)}, bf16[8,2048]{1,0:T(8,128)(2,1)S(1)}, u32[]{:S(2)}, u32[]{:S(2)}) collective-permute-start(bf16[8,2048]{1,0:T(8,128)(2,1)S(1)} %get-tuple-element.66), channel_id=1, source_target_pairs={{0,8},{1,9},{2,10},{3,11},{4,12},{5,13},{6,14},{7,15},{8,0},{9,1},... | collective-permute-start | bytes 98312 | tf_op jit(solution)/shard_map/ppermute | solution.py:70
  91.0 7.1 %collective-permute-start.32 = (bf16[8,2048]{1,0:T(8,128)(2,1)S(1)}, bf16[8,2048]{1,0:T(8,128)(2,1)S(1)}, u32[]{:S(2)}, u32[]{:S(2)}) collective-permute-start(bf16[8,2048]{1,0:T(8,128)(2,1)S(1)} %get-tuple-element.67), channel_id=1, source_target_pairs={{0,16},{1,17},{2,18},{3,19},{4,20},{5,21},{6,22},{7,23},{8,24},{9,... | collective-permute-start | bytes 98312 | tf_op jit(solution)/shard_map/ppermute | solution.py:70
  92.4 5.7 %collective-permute-start.33 = (bf16[8,2048]{1,0:T(8,128)(2,1)S(1)}, bf16[8,2048]{1,0:T(8,128)(2,1)S(1)}, u32[]{:S(2)}, u32[]{:S(2)}) collective-permute-start(bf16[8,2048]{1,0:T(8,128)(2,1)S(1)} %get-tuple-element.68), channel_id=1, source_target_pairs={{0,24},{1,25},{2,26},{3,27},{4,28},{5,29},{6,30},{7,31},{8,16},{9,... | collective-permute-start | bytes 98312 | tf_op jit(solution)/shard_map/ppermute | solution.py:70
